TPU v7x, 512 devices: a whole 4x4x16 slice. The times are simulated.
512 devices in a mesh: ep: 32 (over z, core), tp: 16 (over y, x).
Axes of the slice: x: 4, y: 4, z: 16, core: 2. Of those that a mesh axis runs over, the one named last changes fastest.
Arguments:
- query_maps: bfloat16 [4096, 16, 128], P('ep', 'tp'), may hold values from -6 to 6
- key_maps: bfloat16 [4096, 16, 128], P('ep', 'tp'), may hold values from -6 to 6
- value_rows: bfloat16 [4096, 16, 128], P('ep', 'tp'), may hold values from -6 to 6
- head_lambda: float32 [16], P('tp'), may hold values from 0.3 to 0.8
- head_gain: float32 [128], replicated, may hold values from 0.1 to 1.9
- out_weight: bfloat16 [2048, 2048], P('tp'), may hold values from -0.125 to 0.125
- token_rows: bfloat16 [4096, 2048], P('ep'), may hold values from -36 to 36
- norm_gain: float32 [2048], replicated, may hold values from 0.1 to 1.9
- expert_ids: int32 [4096, 4], P('ep'), may hold values from 0 to 31, all different within a row; in each aligned block of 128 rows (0 to 127, 128 to 255, ...) at most 20 rows name the same one
- route_weights: float32 [4096, 4], P('ep'), may hold values from 0.1 to 0.5
- gate_weight: bfloat16 [32, 2048, 4096], P('ep', None, 'tp'), may hold values from -0.82864076 to 0.82864076
- up_weight: bfloat16 [32, 2048, 4096], P('ep', None, 'tp'), may hold values from -0.82864076 to 0.82864076
- down_weight: bfloat16 [32, 4096, 2048], P('ep', 'tp'), may hold values from -0.03125 to 0.03125
Outputs:
- mixed_rows: bfloat16 [4096, 2048], P(('ep', 'tp'))
- mixed_experts: bfloat16 [4096, 2048], P('ep', 'tp')
Inputs may be any that keep to these rules, and one draw needn't show every extreme that they name: `expert_ids`: each row names 4 different experts. Among the rows of one index of ep no expert is named more than 20 times, and in every draw some expert is named exactly 20 times there.
All inputs are finite; a program needn't handle non-finite values.
Results may differ from a plain program's by a relative error of at most 0.015.
Values may be sent and summed in bfloat16 or wider, within the bound.
No kernel may reach another device: no remote copies, remote signals or barrier semaphores. Data moves between devices by JAX's collectives and lax.ppermute only.
A program may use at most 64 MiB of HBM per device.

v0:
```python
import jax
import jax.numpy as jnp
from jax import lax
from jax.sharding import PartitionSpec as P

NORM_EPS = 1e-05
CLAMP_LIMIT = 7.0
GATE_SLOPE = 1.702


def sent_together(arrays, axis, dim, along):
    ends, at = ([], 0)
    for a in arrays[:-1]:
        at += a.shape[along]
        ends.append(at)
    both = jnp.concatenate(arrays, axis=along)
    return tuple(jnp.split(lax.all_gather(both, axis, axis=dim, tiled=True), ends, axis=along))


def in_blocks(array, dim, length):
    lengths = array.shape
    tiles = array.reshape(*lengths[:dim], length, lengths[dim] // length, *lengths[dim + 1 :])
    return jnp.moveaxis(tiles, dim, 0)


def sum_at_owner(array, axis, dim):
    tiles = in_blocks(array, dim, lax.axis_size(axis))
    arrived = lax.all_to_all(tiles, axis, split_axis=0, concat_axis=0, tiled=True)
    return arrived.astype(jnp.float32).sum(axis=0)


def sent_to_all(array, axis):
    length = lax.axis_size(axis)
    return lax.all_to_all(
        jnp.broadcast_to(array[None], (length, *array.shape)), axis, 0, 0, tiled=True
    )


def laid_out(tiles, dim):
    tiles = jnp.moveaxis(tiles, 0, dim)
    lengths = tiles.shape
    return tiles.reshape(*lengths[:dim], lengths[dim] * lengths[dim + 1], *lengths[dim + 2 :])


def collect(array, axis, dim):
    tiles = sent_to_all(array, axis)
    return laid_out(tiles, dim)


def fold_rows(queries, positions, running, key_block, value_block, offset, head_width, score_scale):
    key_pos = jnp.arange(key_block.shape[0], dtype=jnp.int32)
    causal = key_pos[None, None, :] <= positions[None, :, None]

    def update(running_state):
        fresh = []
        for map_index in range(2):
            row_max, denominator, numerator = running_state[map_index]
            col_low = map_index * head_width
            col_high = col_low + head_width
            scores = (
                jnp.einsum(
                    "qhd,khd->hqk",
                    queries[:, :, col_low:col_high],
                    key_block[:, :, col_low:col_high],
                    preferred_element_type=jnp.float32,
                )
                * score_scale
            )
            scores = jnp.where(causal, scores, -jnp.inf)
            new_max = jnp.maximum(row_max, jnp.max(scores, axis=-1))
            exp_terms = jnp.exp(scores - new_max[:, :, None])
            denominator = jnp.sum(exp_terms, axis=-1)
            numerator = jnp.einsum(
                "hqk,khd->qhd",
                exp_terms.astype(jnp.bfloat16),
                value_block,
                preferred_element_type=jnp.float32,
            )
            fresh.append((new_max, denominator, numerator))
        return tuple(fresh)

    def unchanged(running_state):
        return running_state

    return lax.cond(offset <= positions[positions.shape[0] - 1], update, unchanged, running)


def finish_rows(state, head_lambda, head_gain):
    first_map, second_map = state
    attended = first_map[2] / jnp.transpose(first_map[1])[:, :, None] - head_lambda[
        None, :, None
    ] * (second_map[2] / jnp.transpose(second_map[1])[:, :, None])
    mean_sq = jnp.mean(attended * attended, axis=-1, keepdims=True)
    return (attended * lax.rsqrt(mean_sq + NORM_EPS) * head_gain).astype(jnp.bfloat16)


def mixer_half(query_maps, key_maps, value_rows, head_lambda, head_gain, out_weight):
    local_rows = query_maps.shape[0]
    local_heads = query_maps.shape[1]
    head_width = query_maps.shape[2] // 2
    score_scale = head_width ** (-0.5)
    half_rows = local_rows // 2
    ep_index = lax.axis_index("ep")
    early_queries = query_maps[:half_rows]
    late_queries = query_maps[half_rows:]
    early_pos = ep_index * local_rows + jnp.arange(half_rows, dtype=jnp.int32)
    late_pos = ep_index * local_rows + half_rows + jnp.arange(half_rows, dtype=jnp.int32)
    one_map = (
        jnp.full((local_heads, half_rows), -1e30, jnp.float32),
        jnp.zeros((local_heads, half_rows), jnp.float32),
        jnp.zeros((half_rows, local_heads, 2 * head_width), jnp.float32),
    )
    offset = jnp.int32(0)
    key_block, value_block = sent_together((key_maps, value_rows), "ep", 0, 1)
    early_state = fold_rows(
        early_queries,
        early_pos,
        (one_map, one_map),
        key_block,
        value_block,
        offset,
        head_width,
        score_scale,
    )
    late_state = fold_rows(
        late_queries,
        late_pos,
        (one_map, one_map),
        key_block,
        value_block,
        offset,
        head_width,
        score_scale,
    )
    early_state, late_state = (early_state, late_state)
    early_rows = finish_rows(early_state, head_lambda, head_gain)
    late_rows = finish_rows(late_state, head_lambda, head_gain)
    head_rows = jnp.concatenate([early_rows, late_rows], axis=0).reshape(
        local_rows, local_heads * 2 * head_width
    )
    product = jnp.dot(head_rows, out_weight, preferred_element_type=jnp.float32)
    summed = sum_at_owner(
        lax.optimization_barrier(product.astype(jnp.bfloat16))
        .astype(jnp.float32)
        .astype(jnp.bfloat16),
        "tp",
        0,
    )
    return summed.astype(jnp.bfloat16)


def complete_experts(gate_pre, up_pre, down_matrix):
    gated = jnp.minimum(gate_pre, CLAMP_LIMIT)
    clipped = jnp.clip(up_pre, -CLAMP_LIMIT, CLAMP_LIMIT)
    active = ((clipped + 1.0) * gated * jax.nn.sigmoid(GATE_SLOPE * gated)).astype(jnp.bfloat16)
    partial_value = jnp.einsum(
        "scf,fd->scd", active, down_matrix, preferred_element_type=jnp.float32
    )
    partial_value = lax.optimization_barrier(partial_value.astype(jnp.bfloat16)).astype(jnp.float32)
    summed = sum_at_owner(partial_value.astype(jnp.bfloat16), "tp", 2)
    return lax.all_to_all(
        summed.astype(jnp.bfloat16), "ep", split_axis=0, concat_axis=0, tiled=True
    )


def expert_half(
    token_rows, norm_gain, expert_ids, route_weights, gate_weight, up_weight, down_weight
):
    local_rows, model_width = token_rows.shape
    route_count = expert_ids.shape[1]
    expert_count = lax.axis_size("ep")
    capacity = 5 * local_rows * route_count // (4 * expert_count)
    gate_matrix = gate_weight[0]
    up_matrix = up_weight[0]
    down_matrix = down_weight[0]
    rows_float = token_rows.astype(jnp.float32)
    mean_sq = jnp.mean(rows_float * rows_float, axis=-1, keepdims=True)
    normed = (rows_float * lax.rsqrt(mean_sq + NORM_EPS) * norm_gain).astype(jnp.bfloat16)
    flat_ids = expert_ids.reshape(-1)
    onehot = (flat_ids[:, None] == jnp.arange(expert_count, dtype=jnp.int32)[None, :]).astype(
        jnp.int32
    )
    rank_before = jnp.cumsum(onehot, axis=0) - onehot
    slot_of = jnp.sum(rank_before * onehot, axis=1)
    target = flat_ids * capacity + slot_of
    token_of = jnp.arange(local_rows * route_count, dtype=jnp.int32) // route_count
    slot_table = (
        jnp.full((expert_count * capacity,), local_rows, jnp.int32).at[target].set(token_of)
    )
    padded = jnp.concatenate([normed, jnp.zeros((1, model_width), jnp.bfloat16)], axis=0)
    outgoing = padded[slot_table].reshape(expert_count, capacity, model_width)
    feature_width = model_width // lax.axis_size("tp")
    outgoing_part = lax.dynamic_slice_in_dim(
        outgoing, lax.axis_index("tp") * feature_width, feature_width, 2
    )
    feature_block = collect(
        lax.all_to_all(outgoing_part, "ep", split_axis=0, concat_axis=0, tiled=True), "tp", 2
    )
    gate_sum = jnp.einsum(
        "scd,df->scf", feature_block, gate_matrix, preferred_element_type=jnp.float32
    )
    up_sum = jnp.einsum("scd,df->scf", feature_block, up_matrix, preferred_element_type=jnp.float32)
    returned = complete_experts(gate_sum, up_sum, down_matrix)
    result_width = returned.shape[2]
    picked = returned.reshape(expert_count * capacity, result_width)[target].astype(jnp.float32)
    weighted = picked * route_weights.reshape(-1)[:, None]
    combined = jnp.sum(weighted.reshape(local_rows, route_count, result_width), axis=1)
    return combined.astype(jnp.bfloat16)


def body(
    query_maps,
    key_maps,
    value_rows,
    head_lambda,
    head_gain,
    out_weight,
    token_rows,
    norm_gain,
    expert_ids,
    route_weights,
    gate_weight,
    up_weight,
    down_weight,
):
    mixed_rows = mixer_half(query_maps, key_maps, value_rows, head_lambda, head_gain, out_weight)
    mixed_experts = expert_half(
        token_rows, norm_gain, expert_ids, route_weights, gate_weight, up_weight, down_weight
    )
    return (mixed_rows, mixed_experts)


def solution(mesh):
    placed = (
        P("ep", "tp", None),
        P("ep", "tp", None),
        P("ep", "tp", None),
        P("tp"),
        P(),
        P("tp", None),
        P("ep", None),
        P(),
        P("ep", None),
        P("ep", None),
        P("ep", None, "tp"),
        P("ep", None, "tp"),
        P("ep", "tp", None),
    )
    return jax.shard_map(
        body,
        mesh=mesh,
        in_specs=placed,
        out_specs=(P(("ep", "tp"), None), P("ep", "tp")),
        check_vma=False,
    )
```

profile of v0, /device:TPU:1, one launch (start us, length us, event | category | flops | bytes accessed | tf_op | source)
XLA Modules:
  0.0 208.6 jit_solution(8947306529190692896)
XLA Ops:
  7.2 0.8 broadcast_multiply_fusion
  8.0 0.8 copy.44
  9.0 1.2 fusion.66
  10.5 1.2 reduce-window.6
  12.0 2.4 %scatter_custom_fusion = s32[640]{0:T(1024)S(1)} fusion(s32[512]{0:T(512)S(1)} %bitcast.195, s32[512]{0:T(512)S(1)} %add_select_fusion, s32[]{:T(128)} %constant.42.clone.1), kind=kCustom, calls=%fused_computation.126 | custom fusion | bytes 2564 | tf_op jit(solution)/shard_map/scatter | solution.py:188
  14.5 1.2 fusion.68
  15.8 4.1 %gather_fusion = bf16[640,2048]{1,0:T(8,128)(2,1)} fusion(bf16[129,2048]{1,0:T(8,128)(2,1)S(1)} %concatenate.11, s32[1024]{0:T(1024)S(1)} %pad_clamp_fusion.1), kind=kCustom, calls=%fused_computation | custom fusion | bytes 5245440 | tf_op jit(solution)/shard_map/gather | solution.py:191
  19.9 5.2 %reshape.273 = bf16[32,20,2048]{2,1,0:T(8,128)(2,1)} reshape(bf16[640,2048]{1,0:T(8,128)(2,1)} %gather_fusion) | data formatting | bytes 5242880 | tf_op jit(solution)/shard_map/reshape | solution.py:191
  25.1 1.6 constant_dynamic-slice_fusion
  26.7 16.7 %all-to-all-start.1 = ((bf16[32,20,128]{2,1,0:T(8,128)(2,1)}), bf16[32,20,128]{2,1,0:T(8,128)(2,1)S(1)}, u32[]{:S(2)}, u32[]{:S(2)}) async-start(bf16[32,20,128]{2,1,0:T(8,128)(2,1)} %constant_dynamic-slice_fusion), calls=%async_computation.1 | async-start | bytes 393216 | tf_op jit(solution)/shard_map/all_to_all | solution.py:197
  43.5 0.6 pad_maximum_fusion
  44.2 18.0 %all-to-all-done.1 = bf16[32,20,128]{2,1,0:T(8,128)(2,1)S(1)} async-done(((bf16[32,20,128]{2,1,0:T(8,128)(2,1)}), bf16[32,20,128]{2,1,0:T(8,128)(2,1)S(1)}, u32[]{:S(2)}, u32[]{:S(2)}) %all-to-all-start.1) | async-done | bytes 163872 | tf_op jit(solution)/shard_map/all_to_all | solution.py:197
  62.3 0.5 broadcast_in_dim.39
  62.8 39.4 %all_to_all.25 = bf16[16,32,20,128]{3,1,2,0:T(8,128)(2,1)S(1)} all-to-all(bf16[16,32,20,128]{3,1,2,0:T(8,128)(2,1)S(1)} %broadcast_in_dim.39), channel_id=1, replica_groups=mesh['ep'=32,'tp'=16] {'tp'}, dimensions={0} | all-to-all | bytes 5242880 | tf_op jit(solution)/shard_map/all_to_all | solution.py:34
  102.2 1.5 copy-done.3
  103.7 0.8 fusion.49
  104.9 6.1 %convolution_convert_fusion = bf16[32,20,2048]{2,0,1:T(8,128)(2,1)} fusion(f32[32,20,256]{2,0,1:T(8,128)S(1)} %fusion.49, bf16[1,256,2048]{2,1,0:T(8,128)(2,1)S(1)} %copy-done, bf16[1,2048,256]{2,1,0:T(8,128)(2,1)S(1)} %copy-done.10, bf16[16,32,20,128]{3,1,2,0:T(8,128)(2,1)} %copy-done.3), kind=kOutput, calls=%fused_computation.63 | convolution fusion | flops 1344962560 | bytes 7995392 | tf_op jit(solution)/shard_map/scf,fd->scd/dot_general | solution.py:156
  111.0 3.9 %bitcast_bitcast_fusion = bf16[16,32,20,128]{3,1,2,0:T(8,128)(2,1)} fusion(bf16[32,20,2048]{2,0,1:T(8,128)(2,1)} %convolution_convert_fusion), kind=kLoop, calls=%fused_computation.68 | loop fusion | bytes 5242880 | tf_op jit(solution)/shard_map/transpose | solution.py:23
  114.9 4.4 %all-to-all-start.3 = ((bf16[16,32,20,128]{3,1,2,0:T(8,128)(2,1)}), bf16[16,32,20,128]{3,1,2,0:T(8,128)(2,1)}, u32[]{:S(2)}, u32[]{:S(2)}) async-start(bf16[16,32,20,128]{3,1,2,0:T(8,128)(2,1)} %bitcast_bitcast_fusion), calls=%async_computation.3 | async-start | bytes 5242880 | tf_op jit(solution)/shard_map/all_to_all | solution.py:28
  119.4 0.7 slice.45
  121.4 0.6 slice.44
  122.6 1.7 fusion.103
  124.4 0.6 iota.36
  125.0 1.1 le.45
  126.1 5.0 %conditional.3 = (f32[1,64]{1,0:T(1,128)S(1)}, f32[64,1,128]{2,0,1:T(8,128)S(1)}, f32[1,64]{1,0:T(1,128)S(1)}, f32[64,1,128]{2,0,1:T(8,128)S(1)}) conditional(s32[]{:T(128)} %bitcast.40, () %tuple.26, (s32[]{:T(128)}, s32[1,64,1]{1,2,0:T(1,128)S(1)}, s32[1,64,4096]{2,1,0:T(8,128)S(1)}, bf16[128,1,128]{2,0,1:T(8,128)(2,1)S(1)}, ...), branch_computations={%region_7.8_spmd, %region_8.13_spmd} | conditional | flops 205258688 | bytes 17665856 | solution.py:85
  126.3 1.3 copy.42
  127.6 1.5 fusion.101
  129.9 0.5 fusion.102
  131.1 8.8 %conditional.2 = (f32[1,64]{1,0:T(1,128)}, f32[64,1,128]{2,0,1:T(8,128)S(1)}, f32[1,64]{1,0:T(1,128)}, f32[64,1,128]{2,0,1:T(8,128)}) conditional(s32[]{:T(128)} %bitcast.36, () %tuple.24, (s32[]{:T(128)}, s32[1,64,1]{1,2,0:T(1,128)}, s32[1,64,4096]{2,1,0:T(8,128)}, bf16[128,1,128]{2,0,1:T(8,128)(2,1)S(1)}, bf16[4096,1,128]{2,0,1:T(8,128)(2,1)S(1)}, ...), branch_computations={%region_0.0_spmd, %region_1.6_spmd} | conditional | flops 205258688 | bytes 17665856 | solution.py:85
  131.3 0.7 add_bitcast_fusion
  132.0 1.4 broadcast_compare_fusion
  133.4 1.3 copy.41
  134.8 1.5 fusion.99
  136.3 0.9 fusion.7
  138.0 0.9 fusion.9
  138.9 1.0 convolution_bitcast_fusion
  139.9 1.0 multiply_reduce_fusion
  141.0 2.1 %convolution_convert_fusion.1 = bf16[128,2048]{1,0:T(8,128)(2,1)} fusion(bf16[128,2048]{1,0:T(8,128)(2,1)} %param.22, bf16[64,1,128]{2,0,1:T(8,128)(2,1)S(1)} %get-tuple-element.129, bf16[64,1,128]{2,0,1:T(8,128)(2,1)S(1)} %get-tuple-element.128), kind=kOutput, calls=%fused_computation.69 | convolution fusion | flops 67436544 | bytes 1081344 | tf_op jit(solution)/shard_map/dot_general | solution.py:141
  143.1 10.3 %all-to-all-done.3 = bf16[16,32,20,128]{3,1,2,0:T(8,128)(2,1)} async-done(((bf16[16,32,20,128]{3,1,2,0:T(8,128)(2,1)}), bf16[16,32,20,128]{3,1,2,0:T(8,128)(2,1)}, u32[]{:S(2)}, u32[]{:S(2)}) %all-to-all-start.3) | async-done | bytes 2621472 | tf_op jit(solution)/shard_map/all_to_all | solution.py:28
  153.5 6.1 %all-to-all-start = ((bf16[16,8,2048]{2,1,0:T(8,128)(2,1)}), bf16[16,8,2048]{2,1,0:T(8,128)(2,1)S(1)}, u32[]{:S(2)}, u32[]{:S(2)}) async-start(bf16[16,8,2048]{2,1,0:T(8,128)(2,1)} %bitcast.44), calls=%async_computation | async-start | bytes 1048576 | tf_op jit(solution)/shard_map/all_to_all | solution.py:28
  159.6 2.1 %reduce_sum.121 = bf16[32,20,128]{2,0,1:T(8,128)(2,1)S(1)} reduce(bf16[16,32,20,128]{3,1,2,0:T(8,128)(2,1)} %all-to-all-done.3, bf16[]{:T(256)} %constant.81.clone.1), dimensions={0}, to_apply=%region_20.21 | reduce | flops 1228800 | bytes 2785282 | tf_op jit(solution)/shard_map/reduce_sum | solution.py:29
  161.7 0.7 copy.51
  162.4 7.4 %all-to-all-done = bf16[16,8,2048]{2,1,0:T(8,128)(2,1)S(1)} async-done(((bf16[16,8,2048]{2,1,0:T(8,128)(2,1)}), bf16[16,8,2048]{2,1,0:T(8,128)(2,1)S(1)}, u32[]{:S(2)}, u32[]{:S(2)}) %all-to-all-start) | async-done | bytes 524320 | tf_op jit(solution)/shard_map/all_to_all | solution.py:28
  169.8 10.9 %all-to-all-start.4 = ((bf16[32,20,128]{2,1,0:T(8,128)(2,1)}), bf16[32,20,128]{2,1,0:T(8,128)(2,1)S(1)}, u32[]{:S(2)}, u32[]{:S(2)}) async-start(bf16[32,20,128]{2,1,0:T(8,128)(2,1)} %copy.51), calls=%async_computation.4 | async-start | bytes 393216 | tf_op jit(solution)/shard_map/all_to_all | solution.py:161
  180.8 0.7 reduce_sum.117
  181.5 18.0 %all-to-all-done.4 = bf16[32,20,128]{2,1,0:T(8,128)(2,1)S(1)} async-done(((bf16[32,20,128]{2,1,0:T(8,128)(2,1)}), bf16[32,20,128]{2,1,0:T(8,128)(2,1)S(1)}, u32[]{:S(2)}, u32[]{:S(2)}) %all-to-all-start.4) | async-done | bytes 163872 | tf_op jit(solution)/shard_map/all_to_all | solution.py:161
  199.5 1.3 gather_fusion.1
  200.9 0.9 fusion.82
  (62 shorter events, 4.2 us)
Async XLA Ops:
  7.2 97.4 %copy-start = (bf16[1,256,2048]{2,1,0:T(8,128)(2,1)S(1)}, bf16[1,256,2048]{2,1,0:T(8,128)(2,1)}, u32[]{:S(2)}) copy-start(bf16[1,256,2048]{2,1,0:T(8,128)(2,1)} %param.29) | copy-start | bytes 3145732
  19.9 23.6 %copy-start.5 = (bf16[128,1,128]{2,0,1:T(8,128)(2,1)S(1)}, bf16[128,1,128]{2,0,1:T(8,128)(2,1)}, u32[]{:S(2)}) copy-start(bf16[128,1,128]{2,0,1:T(8,128)(2,1)} %param.19) | copy-start | bytes 98308
  19.9 23.6 %copy-start.6 = (bf16[128,1,128]{2,0,1:T(8,128)(2,1)S(1)}, bf16[128,1,128]{2,0,1:T(8,128)(2,1)}, u32[]{:S(2)}) copy-start(bf16[128,1,128]{2,0,1:T(8,128)(2,1)} %param.18) | copy-start | bytes 98308
  26.7 35.5 %all-to-all-start.1 = ((bf16[32,20,128]{2,1,0:T(8,128)(2,1)}), bf16[32,20,128]{2,1,0:T(8,128)(2,1)S(1)}, u32[]{:S(2)}, u32[]{:S(2)}) async-start(bf16[32,20,128]{2,1,0:T(8,128)(2,1)} %constant_dynamic-slice_fusion), calls=%async_computation.1 | async-start | bytes 393216 | tf_op jit(solution)/shard_map/all_to_all | solution.py:197
  43.4 79.2 %all-gather.2.cloned.1.call-start = ((), (), s32[]{:S(2)}) async-start(), calls=%async_computation.5 | async-start | bytes 2162688 | tf_op jit(solution)/shard_map/all_gather | solution.py:17
  62.8 40.9 %copy-start.9 = (bf16[1,2048,256]{2,1,0:T(8,128)(2,1)S(1)}, bf16[1,2048,256]{2,1,0:T(8,128)(2,1)}, u32[]{:S(2)}) copy-start(bf16[1,2048,256]{2,1,0:T(8,128)(2,1)} %param.27) | copy-start | bytes 3145732
  102.2 1.5 copy-start.3
  103.7 1.2 copy-start.10
  114.9 38.5 %all-to-all-start.3 = ((bf16[16,32,20,128]{3,1,2,0:T(8,128)(2,1)}), bf16[16,32,20,128]{3,1,2,0:T(8,128)(2,1)}, u32[]{:S(2)}, u32[]{:S(2)}) async-start(bf16[16,32,20,128]{3,1,2,0:T(8,128)(2,1)} %bitcast_bitcast_fusion), calls=%async_computation.3 | async-start | bytes 5242880 | tf_op jit(solution)/shard_map/all_to_all | solution.py:28
  122.6 3.5 %copy-start.4 = (bf16[128,1,128]{2,0,1:T(8,128)(2,1)S(1)}, bf16[128,1,128]{2,0,1:T(8,128)(2,1)}, u32[]{:S(2)}) copy-start(bf16[128,1,128]{2,0,1:T(8,128)(2,1)} %param.17) | copy-start | bytes 98308
  127.6 2.3 %copy-start.1 = (bf16[4096,1,128]{0,2,1:T(8,128)(2,1)S(1)}, bf16[4096,1,128]{0,2,1:T(8,128)(2,1)}, u32[]{:S(2)}) copy-start(bf16[4096,1,128]{0,2,1:T(8,128)(2,1)} %copy.42) | copy-start | bytes 3145732 | tf_op jit(solution)/shard_map/cond
  131.1 9.8 %copy-start.8 = (f32[128]{0:T(128)S(1)}, f32[128]{0:T(128)}, u32[]{:S(2)}) copy-start(f32[128]{0:T(128)} %param.21) | copy-start | bytes 1540
  134.8 2.8 %copy-start.2 = (bf16[4096,1,128]{0,2,1:T(8,128)(2,1)S(1)}, bf16[4096,1,128]{0,2,1:T(8,128)(2,1)}, u32[]{:S(2)}) copy-start(bf16[4096,1,128]{0,2,1:T(8,128)(2,1)} %copy.41) | copy-start | bytes 3145732 | tf_op jit(solution)/shard_map/cond
  141.0 39.7 %copy-start.7 = (f32[128,4]{0,1:T(4,128)S(1)}, f32[128,4]{0,1:T(4,128)}, u32[]{:S(2)}) copy-start(f32[128,4]{0,1:T(4,128)} %param.26) | copy-start | bytes 6148
  153.5 16.3 %all-to-all-start = ((bf16[16,8,2048]{2,1,0:T(8,128)(2,1)}), bf16[16,8,2048]{2,1,0:T(8,128)(2,1)S(1)}, u32[]{:S(2)}, u32[]{:S(2)}) async-start(bf16[16,8,2048]{2,1,0:T(8,128)(2,1)} %bitcast.44), calls=%async_computation | async-start | bytes 1048576 | tf_op jit(solution)/shard_map/all_to_all | solution.py:28
  169.8 29.7 %all-to-all-start.4 = ((bf16[32,20,128]{2,1,0:T(8,128)(2,1)}), bf16[32,20,128]{2,1,0:T(8,128)(2,1)S(1)}, u32[]{:S(2)}, u32[]{:S(2)}) async-start(bf16[32,20,128]{2,1,0:T(8,128)(2,1)} %copy.51), calls=%async_computation.4 | async-start | bytes 393216 | tf_op jit(solution)/shard_map/all_to_all | solution.py:161
Sparse Core Ops, SparseCore 0:
  46.4 72.5 all-gather.1
where the time goes:
time: 210 us; the launch traced here: 209 us
  waiting for transfers between devices  53.7 us (26%)
  blocking collectives  39.4 us (19%)
  starting transfers between devices  38.2 us (18%)
  local copies, waits for them, and re-layouts  30.8 us (15%)
  between operations  16.3 us (8%)
  matrix products  15.2 us (7%)
  other arithmetic  14.7 us (7%)
    all_to_all x1, blocking collectives, sent_to_all(): lax.all_to_all(jnp.broadcast_to(array[None], (length, *array.shape)), axi...  39.4 us
    all_to_all x1, waiting for transfers between devices, expert_half(): lax.all_to_all(outgoing_part, 'ep', split_axis=0, concat_axis=0, tiled=True)  18 us
    all_to_all x1, waiting for transfers between devices, complete_experts(): lax.all_to_all(summed.astype(jnp.bfloat16), 'ep', split_axis=0, concat_ax...  18 us
    all_to_all x2, waiting for transfers between devices, sum_at_owner(): lax.all_to_all(tiles, axis, split_axis=0, concat_axis=0, tiled=True)  17.7 us
    all_to_all x1, starting transfers between devices, expert_half(): lax.all_to_all(outgoing_part, 'ep', split_axis=0, concat_axis=0, tiled=True)  16.7 us
    all_to_all x1, starting transfers between devices, complete_experts(): lax.all_to_all(summed.astype(jnp.bfloat16), 'ep', split_axis=0, concat_ax...  10.9 us
    all_to_all x2, starting transfers between devices, sum_at_owner(): lax.all_to_all(tiles, axis, split_axis=0, concat_axis=0, tiled=True)  10.5 us
    dot_general x1, matrix products, complete_experts(): jnp.einsum('scf,fd->scd', active, down_matrix, preferred_element_type=jnp...  6.09 us
  transfers between devices with their start and end apart: 5, of which 4 were waited for; matrix products, arithmetic and copies ran while one was open for 18% of the time, Pallas kernels for 0%

commit v1 on v0

v1 whole, which is shorter than its diff:
```python
import jax
import jax.numpy as jnp
from jax import lax
from jax.experimental import pallas as pl
from jax.experimental.pallas import tpu as pltpu
from jax.sharding import Mesh, PartitionSpec as P

NORM_EPS = 1e-05
CLAMP_LIMIT = 7.0
GATE_SLOPE = 1.702
BF16 = jnp.bfloat16
F32 = jnp.float32

Z, CORE, Y, X = 16, 2, 4, 4
EP = ("z", "core")
TP = ("y", "x")
N_EP = Z * CORE
N_TP = Y * X
TOK = 128
CAP = 20
PAD = 24
ROWS = N_EP * CAP
PADDED = N_EP * PAD
WIDE = 128
MODEL = N_TP * WIDE
OUT_ROWS = ROWS + TOK

LANE_OFFSETS = (-4, 0, 4, 8, -5, -1, 3, 7, -3, 1, 5, 9, -6, -2, 2, 6)


def routing(ids, values=None):
    expert = lax.broadcasted_iota(jnp.int32, (N_EP, TOK), 0)
    named = jnp.zeros((N_EP, TOK), F32)
    weight = jnp.zeros((N_EP, TOK), F32)
    for k in range(ids.shape[0]):
        hit = ids[k : k + 1, :] == expert
        named = named + jnp.where(hit, 1.0, 0.0)
        if values is not None:
            weight = weight + jnp.where(hit, values[k : k + 1, :], 0.0)
    earlier = lax.broadcasted_iota(jnp.int32, (TOK, TOK), 0) < lax.broadcasted_iota(
        jnp.int32, (TOK, TOK), 1
    )
    rank = jnp.dot(
        named.astype(BF16),
        jnp.where(earlier, 1.0, 0.0).astype(BF16),
        preferred_element_type=F32,
    )
    slot = jnp.where(named > 0.5, rank.astype(jnp.int32), -1)
    place = lax.broadcasted_iota(jnp.int32, (PAD, TOK), 0)
    pieces = []
    for e in range(N_EP):
        here = slot[e : e + 1, :] == place
        pieces.append(jnp.where(here, 1.0 if values is None else weight[e : e + 1, :], 0.0))
    return jnp.concatenate(pieces, axis=0)


def dispatch_kernel(at_ref, rows_ref, part_ref, gain_ref, ids_ref, out_ref):
    rows = rows_ref[...].astype(F32)
    mean_sq = jnp.mean(rows * rows, axis=-1, keepdims=True)
    part = part_ref[...].astype(F32) * lax.rsqrt(mean_sq + NORM_EPS) * gain_ref[...]
    chosen = routing(ids_ref[...]).astype(BF16)
    packed = jnp.dot(chosen, part.astype(BF16), preferred_element_type=F32)
    out_ref[...] = packed.astype(BF16).reshape(N_EP, PAD, WIDE)


def dispatch(at, token_rows, gain, ids):
    return pl.pallas_call(
        dispatch_kernel,
        out_shape=jax.ShapeDtypeStruct((N_EP, PAD, WIDE), BF16),
        grid_spec=pltpu.PrefetchScalarGridSpec(
            num_scalar_prefetch=1,
            grid=(1,),
            in_specs=[
                pl.BlockSpec((TOK, MODEL), lambda i, at: (0, 0)),
                pl.BlockSpec((TOK, WIDE), lambda i, at: (0, at[0])),
                pl.BlockSpec((1, WIDE), lambda i, at: (0, at[0])),
                pl.BlockSpec((4, TOK), lambda i, at: (0, 0)),
            ],
            out_specs=pl.BlockSpec((N_EP, PAD, WIDE), lambda i, at: (0, 0, 0)),
        ),
        name="dispatch",
    )(at, token_rows, token_rows, gain, ids)


def compact_kernel(in_ref, out_ref):
    to = lax.broadcasted_iota(jnp.int32, (2 * CAP, 2 * PAD), 0)
    src = lax.broadcasted_iota(jnp.int32, (2 * CAP, 2 * PAD), 1)
    pick = jnp.where(src == jnp.where(to < CAP, to, to + (PAD - CAP)), 1.0, 0.0).astype(BF16)
    for g in range(N_EP // 2):
        block = in_ref[2 * g : 2 * g + 2].reshape(2 * PAD, WIDE)
        kept = jnp.dot(pick, block, preferred_element_type=F32).astype(BF16)
        for t in range(N_TP):
            out_ref[t, 2 * CAP * g : 2 * CAP * (g + 1), :] = kept


def compact(arrived):
    return pl.pallas_call(
        compact_kernel,
        out_shape=jax.ShapeDtypeStruct((N_TP, ROWS, WIDE), BF16),
        name="compact",
    )(arrived)


SPLIT = OUT_ROWS // 2


def ffn_rows(x_ref, wg_ref, wu_ref, wd_ref, out_ref, count):
    rows = jnp.concatenate([x_ref[t, :count, :] for t in range(N_TP)], axis=-1)
    gate = jnp.dot(rows, wg_ref[...], preferred_element_type=F32)
    up = jnp.dot(rows, wu_ref[...], preferred_element_type=F32)
    gated = jnp.minimum(gate, CLAMP_LIMIT)
    clipped = jnp.clip(up, -CLAMP_LIMIT, CLAMP_LIMIT)
    active = ((clipped + 1.0) * gated * jax.nn.sigmoid(GATE_SLOPE * gated)).astype(BF16)
    terms = jnp.dot(active, wd_ref[...], preferred_element_type=F32).astype(BF16)
    for t in range(N_TP):
        out_ref[t, :count, :] = terms[:, t * WIDE : (t + 1) * WIDE]


def ffn_kernel(x_ref, wg_ref, wu_ref, wd_ref, proj_ref, out_ref):
    step = pl.program_id(0)

    @pl.when(step == 0)
    def _():
        ffn_rows(x_ref, wg_ref, wu_ref, wd_ref, out_ref, SPLIT)

    @pl.when(step == 1)
    def _():
        ffn_rows(x_ref, wg_ref, wu_ref, wd_ref, out_ref, ROWS - SPLIT)
        out_ref[:, ROWS - SPLIT :, :] = proj_ref[...]


def ffn(x, wg, wu, wd, proj):
    whole = lambda *shape: pl.BlockSpec(shape, lambda i: (0,) * len(shape))
    return pl.pallas_call(
        ffn_kernel,
        out_shape=jax.ShapeDtypeStruct((N_TP, OUT_ROWS, WIDE), BF16),
        grid=(2,),
        in_specs=[
            pl.BlockSpec((N_TP, SPLIT, WIDE), lambda i: (0, i, 0)),
            whole(*wg.shape),
            whole(*wu.shape),
            whole(*wd.shape),
            whole(*proj.shape),
        ],
        out_specs=pl.BlockSpec((N_TP, SPLIT, WIDE), lambda i: (0, i, 0)),
        name="ffn",
    )(x, wg, wu, wd, proj)


REDUCE_STEPS = 4
REDUCE_ROWS = ROWS // REDUCE_STEPS
REDUCE_SRC = N_EP // REDUCE_STEPS


def reduce_kernel(in_ref, pack_ref, mixed_ref):
    step = pl.program_id(0)
    summed = in_ref[0].astype(F32)
    for t in range(1, N_TP):
        summed = summed + in_ref[t].astype(F32)
    summed = summed.astype(BF16)

    @pl.when(step < REDUCE_STEPS)
    def _():
        to = lax.broadcasted_iota(jnp.int32, (2 * PAD, 2 * CAP), 0)
        src = lax.broadcasted_iota(jnp.int32, (2 * PAD, 2 * CAP), 1)
        hit = to == jnp.where(src < CAP, src, src + (PAD - CAP))
        place = jnp.where(hit, 1.0, 0.0).astype(BF16)
        for g in range(REDUCE_SRC // 2):
            block = summed[2 * CAP * g : 2 * CAP * (g + 1)]
            spread = jnp.dot(place, block, preferred_element_type=F32).astype(BF16)
            pack_ref[2 * g : 2 * g + 2] = spread.reshape(2, PAD, WIDE)

    @pl.when(step == REDUCE_STEPS)
    def _():
        for c in range(N_TP):
            mixed_ref[:, c * WIDE : (c + 1) * WIDE] = summed[8 * c : 8 * (c + 1)]


def reduce_terms(y):
    return pl.pallas_call(
        reduce_kernel,
        out_shape=(
            jax.ShapeDtypeStruct((N_EP, PAD, WIDE), BF16),
            jax.ShapeDtypeStruct((TOK // N_TP, MODEL), BF16),
        ),
        grid=(REDUCE_STEPS + 1,),
        in_specs=[pl.BlockSpec((N_TP, REDUCE_ROWS, WIDE), lambda i: (0, i, 0))],
        out_specs=(
            pl.BlockSpec(
                (REDUCE_SRC, PAD, WIDE), lambda i: (jnp.minimum(i, REDUCE_STEPS - 1), 0, 0)
            ),
            pl.BlockSpec((TOK // N_TP, MODEL), lambda i: (0, 0)),
        ),
        name="reduce_terms",
    )(y)


def combine_kernel(back_ref, ids_ref, weights_ref, out_ref):
    spread = routing(ids_ref[...], weights_ref[...])
    high = spread.astype(BF16)
    low = (spread - high.astype(F32)).astype(BF16)
    back = back_ref[...].reshape(PADDED, WIDE)
    over = (((0,), (0,)), ((), ()))
    mixed = lax.dot_general(high, back, over, preferred_element_type=F32)
    mixed = mixed + lax.dot_general(low, back, over, preferred_element_type=F32)
    out_ref[...] = mixed.astype(BF16)


def combine(back, ids, weights):
    return pl.pallas_call(
        combine_kernel,
        out_shape=jax.ShapeDtypeStruct((TOK, WIDE), BF16),
        name="combine",
    )(back, ids, weights)


def attend_kernel(
    place_ref, lam_ref, q_ref, own_ref, other_ref, gain_ref, w_ref, out_ref, score_ref
):
    q = q_ref[...]
    q = (q.astype(F32) * (64**-0.5)).astype(BF16)
    lane = lax.broadcasted_iota(jnp.int32, (TOK, WIDE), 1)
    zero = jnp.zeros_like(q)
    both = jnp.concatenate(
        [jnp.where(lane < 64, q, zero), jnp.where(lane < 64, zero, q)], axis=0
    )
    row = lax.broadcasted_iota(jnp.int32, (2 * TOK, TOK), 0)
    row = jnp.where(row < TOK, row, row - TOK)
    ahead = lax.broadcasted_iota(jnp.int32, (2 * TOK, TOK), 1) - row
    me = place_ref[N_EP]
    top = jnp.full((2 * TOK, TOK), -1e30, F32)
    for b in range(N_EP):
        ref = own_ref if b < Z else other_ref
        keys = ref[b % Z, :, :WIDE]
        scores = lax.dot_general(
            both, keys, (((1,), (1,)), ((), ())), preferred_element_type=F32
        )
        scores = jnp.where(ahead <= (me - place_ref[b]) * TOK, scores, -1e30)
        score_ref[b] = scores
        top = jnp.maximum(top, scores)
    row_max = jnp.max(top, axis=-1, keepdims=True)
    total = jnp.zeros((2 * TOK, TOK), F32)
    value_sum = jnp.zeros((2 * TOK, WIDE), F32)
    for b in range(N_EP):
        ref = own_ref if b < Z else other_ref
        terms = jnp.exp(score_ref[b] - row_max)
        total = total + terms
        value_sum = value_sum + jnp.dot(
            terms.astype(BF16), ref[b % Z, :, WIDE:], preferred_element_type=F32
        )
    ratio = value_sum / jnp.sum(total, axis=-1, keepdims=True)
    attended = ratio[:TOK] - lam_ref[0] * ratio[TOK:]
    mean_sq = jnp.mean(attended * attended, axis=-1, keepdims=True)
    head_rows = (attended * lax.rsqrt(mean_sq + NORM_EPS) * gain_ref[...]).astype(BF16)
    product = jnp.dot(head_rows, w_ref[...], preferred_element_type=F32).astype(BF16)
    for c in range(N_TP):
        piece = product[:, c * WIDE : (c + 1) * WIDE].reshape(N_TP, TOK // N_TP, WIDE)
        out_ref[:, 8 * c : 8 * (c + 1), :] = piece


def attend(place, lam, q, own, other, gain, w):
    vmem = pl.BlockSpec(memory_space=pltpu.VMEM)
    smem = pl.BlockSpec(memory_space=pltpu.SMEM)
    return pl.pallas_call(
        attend_kernel,
        out_shape=jax.ShapeDtypeStruct((N_TP, TOK, WIDE), BF16),
        in_specs=[smem, smem, vmem, vmem, vmem, vmem, vmem],
        out_specs=vmem,
        scratch_shapes=[pltpu.VMEM((N_EP, 2 * TOK, TOK), F32)],
        name="attend",
    )(place, lam, q, own, other, gain, w)


def shifted(array, axis, by):
    length = lax.axis_size(axis)
    return lax.ppermute(array, axis, [(i, (i + by) % length) for i in range(length)])


def exchanged(array, axes):
    return lax.all_to_all(array, axes, split_axis=0, concat_axis=0, tiled=True)


def collect_keys(keys, values):
    mine = jnp.concatenate([keys, values], axis=-1)
    far = jnp.stack(
        [shifted(mine, "z", 4), mine, shifted(mine, "z", -4), shifted(mine, "z", 8)]
    )
    near = [
        shifted(far, "z", 1),
        shifted(far, "z", -1),
        shifted(far[0:2], "z", 2),
        shifted(far[1:3], "z", -2),
    ]
    return jnp.concatenate([far, *near], axis=0)


def body(
    query_maps,
    key_maps,
    value_rows,
    head_lambda,
    head_gain,
    out_weight,
    token_rows,
    norm_gain,
    expert_ids,
    route_weights,
    gate_weight,
    up_weight,
    down_weight,
):
    z_at = lax.axis_index("z").astype(jnp.int32)
    core_at = lax.axis_index("core").astype(jnp.int32)
    tp_at = lax.axis_index(TP).astype(jnp.int32)
    ids = expert_ids.T
    packed = dispatch(tp_at.reshape(1), token_rows, norm_gain.reshape(1, MODEL), ids)
    arrived = exchanged(packed, EP)

    own = collect_keys(key_maps.reshape(TOK, WIDE), value_rows.reshape(TOK, WIDE))
    other = shifted(own, "core", 1)
    chips = (z_at + jnp.array(LANE_OFFSETS, jnp.int32) + Z) % Z
    place = jnp.concatenate(
        [chips * CORE + core_at, chips * CORE + 1 - core_at, (z_at * CORE + core_at).reshape(1)]
    )
    proj = attend(
        place,
        head_lambda,
        query_maps.reshape(TOK, WIDE),
        own,
        other,
        head_gain.reshape(1, WIDE),
        out_weight,
    )

    x = exchanged(compact(arrived), TP)
    terms = ffn(x, gate_weight[0], up_weight[0], down_weight[0], proj)
    back, mixed_rows = reduce_terms(exchanged(terms, TP))
    mixed_experts = combine(exchanged(back, EP), ids, route_weights.T)
    return (mixed_rows, mixed_experts)


def solution(mesh):
    fine = Mesh(mesh.devices.reshape(Z, CORE, Y, X), ("z", "core", "y", "x"))
    placed = (
        P(EP, TP, None),
        P(EP, TP, None),
        P(EP, TP, None),
        P(TP),
        P(),
        P(TP, None),
        P(EP, None),
        P(),
        P(EP, None),
        P(EP, None),
        P(EP, None, TP),
        P(EP, None, TP),
        P(EP, TP, None),
    )
    return jax.shard_map(
        body,
        mesh=fine,
        in_specs=placed,
        out_specs=(P((*EP, *TP), None), P(EP, TP)),
        check_vma=False,
    )
```

time: 210 us -> 173 us (0.82)
  waiting for transfers between devices: 53.7 us -> 5.13 us
  blocking collectives: 39.4 us -> 68.5 us
  starting transfers between devices: 38.2 us -> 63.8 us
  Pallas kernels: 0 us -> 23.9 us
  local copies, waits for them, and re-layouts: 30.8 us -> 6.91 us
  matrix products: 15.2 us -> 0 us
  between operations: 16.3 us -> 1.46 us
  other arithmetic: 14.7 us -> 2.1 us
    all_to_all x4 -> x2, waiting for transfers between devices: 53.7 us -> 3.57 us  [exchanged(): return lax.all_to_all(array, axes, split_axis=0, concat_axis=0, tiled=True)]
    ppermute x0 -> x8, starting transfers between devices: none -> 40.1 us  [shifted(): lax.ppermute(array, axis, [(i, (i + by) % length) for i in range(length)])]
    all_to_all x1 -> x2, blocking collectives: 39.4 us -> 68.5 us  [exchanged(): return lax.all_to_all(array, axes, split_axis=0, concat_axis=0, tiled=True)]
    pallas_call x0 -> x6, Pallas kernels: none -> 23.9 us  [the longest x1 6.21 us: ffn(): pl.pallas_call(ffn_kernel, out_shape=jax.ShapeDtypeStruct((N_TP, OUT_ROWS...]
    dot_general x11 -> x0, matrix products: 15.2 us -> none  [the longest x1 6.09 us: complete_experts(): jnp.einsum('scf,fd->scd', active, down_matrix, preferred_element_type=jnp...]
    all_to_all x4 -> x2, starting transfers between devices: 38.2 us -> 23.6 us  [exchanged(): return lax.all_to_all(array, axes, split_axis=0, concat_axis=0, tiled=True)]
    reduce_sum x10 -> x0, other arithmetic: 8.38 us -> none  [the longest x2 2.81 us: sum_at_owner(): return arrived.astype(jnp.float32).sum(axis=0)]
    gather x2 -> x0, local copies, waits for them, and re-layouts: 5.43 us -> none  [the longest x1 4.09 us: expert_half(): outgoing = padded[slot_table].reshape(expert_count, capacity, model_width)]
  transfers between devices with their start and end apart: 5 -> 10, of which waited for: 4 -> 3; matrix products, arithmetic and copies ran while one was open for 18% -> 4% of each run, Pallas kernels for 0% -> 5%
where the time goes in v1:
time: 173 us; the launch traced here: 172 us
  blocking collectives  68.5 us (40%)
  starting transfers between devices  63.8 us (37%)
  Pallas kernels  23.9 us (14%)
  local copies, waits for them, and re-layouts  6.91 us (4%)
  waiting for transfers between devices  5.13 us (3%)
  other arithmetic  2.1 us (1%)
    all_to_all x2, blocking collectives, exchanged(): return lax.all_to_all(array, axes, split_axis=0, concat_axis=0, tiled=True)  68.5 us
    ppermute x8, starting transfers between devices, shifted(): lax.ppermute(array, axis, [(i, (i + by) % length) for i in range(length)])  40.1 us
    all_to_all x2, starting transfers between devices, exchanged(): return lax.all_to_all(array, axes, split_axis=0, concat_axis=0, tiled=True)  23.6 us
    unnamed x16, local copies, waits for them, and re-layouts  6.23 us
    pallas_call x1, Pallas kernels, ffn(): pl.pallas_call(ffn_kernel, out_shape=jax.ShapeDtypeStruct((N_TP, OUT_ROWS...  6.21 us
    pallas_call x1, Pallas kernels, attend(): pl.pallas_call(attend_kernel, out_shape=jax.ShapeDtypeStruct((N_TP, TOK,...  6.09 us
    pallas_call x1, Pallas kernels, reduce_terms(): pl.pallas_call(reduce_kernel, out_shape=(jax.ShapeDtypeStruct((N_EP, PAD,...  4.52 us
    all_to_all x2, waiting for transfers between devices, exchanged(): return lax.all_to_all(array, axes, split_axis=0, concat_axis=0, tiled=True)  3.57 us
  transfers between devices with their start and end apart: 10, of which 3 were waited for; matrix products, arithmetic and copies ran while one was open for 4% of the time, Pallas kernels for 5%

profile of v1, /device:TPU:1, one launch (start us, length us, event | category | flops | bytes accessed | tf_op | source)
XLA Modules:
  0.0 171.7 jit_solution(17779416363124037385)
XLA Ops:
  0.6 2.2 %dispatch.1 = bf16[32,24,128]{2,1,0:T(8,128)(2,1)} custom-call(s32[1]{0:T(128)} %bitcast.at_ref, bf16[128,2048]{1,0:T(8,128)(2,1)} %part_ref.1, bf16[128,2048]{1,0:T(8,128)(2,1)} %part_ref.1, f32[1,2048]{1,0:T(1,128)} %bitcast.34, s32[4,128]{1,0:T(4,128)} %bitcast.35), custom_call_target="tpu_custom_call" | custom-call | tf_op jit(solution)/shard_map/dispatch/pallas_call | solution.py:67
  2.8 16.7 %all-to-all-start = ((bf16[32,24,128]{2,1,0:T(8,128)(2,1)}), bf16[32,24,128]{2,1,0:T(8,128)(2,1)S(1)}, u32[]{:S(2)}, u32[]{:S(2)}) async-start(bf16[32,24,128]{2,1,0:T(8,128)(2,1)} %dispatch.1), calls=%async_computation | async-start | bytes 393216 | tf_op jit(solution)/shard_map/all_to_all | solution.py:280
  19.6 0.8 fusion.2
  20.4 7.2 %collective-permute-start.1 = (bf16[128,256]{1,0:T(8,128)(2,1)S(1)}, bf16[128,256]{1,0:T(8,128)(2,1)S(1)}, u32[]{:S(2)}, u32[]{:S(2)}) collective-permute-start(bf16[128,256]{1,0:T(8,128)(2,1)S(1)} %get-tuple-element.11), channel_id=1, source_target_pairs={{0,384},{32,416},{64,448},{96,480},{128,0},{160,32},{192,64},{224,... | collective-permute-start | bytes 196616 | tf_op jit(solution)/shard_map/ppermute | solution.py:276
  27.6 7.0 %collective-permute-start.2 = (bf16[128,256]{1,0:T(8,128)(2,1)S(1)}, bf16[128,256]{1,0:T(8,128)(2,1)S(1)}, u32[]{:S(2)}, u32[]{:S(2)}) collective-permute-start(bf16[128,256]{1,0:T(8,128)(2,1)S(1)} %get-tuple-element.11), channel_id=1, source_target_pairs={{0,256},{32,288},{64,320},{96,352},{128,384},{160,416},{192,448},{... | collective-permute-start | bytes 196616 | tf_op jit(solution)/shard_map/ppermute | solution.py:276
  34.5 7.0 %collective-permute-start = (bf16[128,256]{1,0:T(8,128)(2,1)S(1)}, bf16[128,256]{1,0:T(8,128)(2,1)S(1)}, u32[]{:S(2)}, u32[]{:S(2)}) collective-permute-start(bf16[128,256]{1,0:T(8,128)(2,1)S(1)} %get-tuple-element.11), channel_id=1, source_target_pairs={{0,128},{32,160},{64,192},{96,224},{128,256},{160,288},{192,320},{... | collective-permute-start | bytes 196616 | tf_op jit(solution)/shard_map/ppermute | solution.py:276
  41.6 0.0 all-to-all-done.in_ref
  41.6 0.0 copy-start.1
  41.6 0.7 copy-done.1
  42.3 2.8 %compact.1 = bf16[16,640,128]{2,1,0:T(8,128)(2,1)} custom-call(bf16[32,24,128]{2,1,0:T(8,128)(2,1)} %copy-done.1), custom_call_target="tpu_custom_call" | custom-call | tf_op jit(solution)/shard_map/compact/pallas_call | solution.py:97
  45.1 0.0 copy-start.2
  45.1 0.0 copy-start.3
  45.1 0.0 copy-start.4
  45.1 6.9 %all-to-all-start.1 = ((bf16[16,640,128]{2,1,0:T(8,128)(2,1)}), bf16[16,640,128]{2,1,0:T(8,128)(2,1)S(1)}, u32[]{:S(2)}, u32[]{:S(2)}) async-start(bf16[16,640,128]{2,1,0:T(8,128)(2,1)} %compact.1), calls=%async_computation.1 | async-start | bytes 5242880 | tf_op jit(solution)/shard_map/all_to_all | solution.py:280
  52.0 0.0 collective-permute-done.1
  52.0 0.0 collective-permute-done.2
  52.0 0.0 collective-permute-done
  52.1 2.2 %collective-permute-start.4 = (bf16[4,128,256]{2,1,0:T(8,128)(2,1)S(1)}, bf16[4,128,256]{2,1,0:T(8,128)(2,1)S(1)}, u32[]{:S(2)}, u32[]{:S(2)}) collective-permute-start(bf16[4,128,256]{2,1,0:T(8,128)(2,1)S(1)} %pad_maximum_fusion), channel_id=1, source_target_pairs={{0,480},{32,0},{64,32},{96,64},{128,96},{160,128},{192,160},{224,1... | collective-permute-start | bytes 786440 | tf_op jit(solution)/shard_map/ppermute | solution.py:276
  54.3 3.1 %collective-permute-start.3 = (bf16[4,128,256]{2,1,0:T(8,128)(2,1)S(1)}, bf16[4,128,256]{2,1,0:T(8,128)(2,1)S(1)}, u32[]{:S(2)}, u32[]{:S(2)}) collective-permute-start(bf16[4,128,256]{2,1,0:T(8,128)(2,1)S(1)} %pad_maximum_fusion), channel_id=1, source_target_pairs={{0,32},{32,64},{64,96},{96,128},{128,160},{160,192},{192,224},{224... | collective-permute-start | bytes 786440 | tf_op jit(solution)/shard_map/ppermute | solution.py:276
  57.4 2.2 %collective-permute-start.6 = (bf16[2,128,256]{2,1,0:T(8,128)(2,1)S(1)}, bf16[2,128,256]{2,1,0:T(8,128)(2,1)S(1)}, u32[]{:S(2)}, u32[]{:S(2)}) collective-permute-start(bf16[2,128,256]{2,1,0:T(8,128)(2,1)S(1)} %get-tuple-element.8), channel_id=1, source_target_pairs={{0,448},{32,480},{64,0},{96,32},{128,64},{160,96},{192,128},{224,1... | collective-permute-start | bytes 393224 | tf_op jit(solution)/shard_map/ppermute | solution.py:276
  59.6 4.0 %collective-permute-start.5 = (bf16[2,128,256]{2,1,0:T(8,128)(2,1)S(1)}, bf16[2,128,256]{2,1,0:T(8,128)(2,1)S(1)}, u32[]{:S(2)}, u32[]{:S(2)}) collective-permute-start(bf16[2,128,256]{2,1,0:T(8,128)(2,1)S(1)} %get-tuple-element.9), channel_id=1, source_target_pairs={{0,64},{32,96},{64,128},{96,160},{128,192},{160,224},{192,256},{22... | collective-permute-start | bytes 393224 | tf_op jit(solution)/shard_map/ppermute | solution.py:276
  63.6 0.6 constant_dynamic-update-slice_fusion.7
  64.3 0.0 copy-done.2
  64.3 0.0 copy-done.3
  64.3 0.6 constant_dynamic-update-slice_fusion.6
  64.9 0.6 constant_dynamic-update-slice_fusion.5
  65.5 0.6 constant_dynamic-update-slice_fusion.4
  66.2 0.0 collective-permute-done.3
  66.2 0.7 constant_dynamic-update-slice_fusion.3
  66.9 0.0 collective-permute-done.4
  66.9 0.7 constant_dynamic-update-slice_fusion.2
  67.6 0.2 collective-permute-done.5
  67.8 0.6 constant_dynamic-update-slice_fusion.1
  68.5 0.0 collective-permute-done.6
  68.5 0.7 constant_dynamic-update-slice_fusion.own_ref
  69.2 7.5 %collective-permute-start.7 = (bf16[16,128,256]{2,1,0:T(8,128)(2,1)}, bf16[16,128,256]{2,1,0:T(8,128)(2,1)}, u32[]{:S(2)}, u32[]{:S(2)}) collective-permute-start(bf16[16,128,256]{2,1,0:T(8,128)(2,1)} %constant_dynamic-update-slice_fusion.own_ref), channel_id=1, source_target_pairs={{0,16},{16,0},{1,17},{17,1},{2,18},{18,2},{3,19},{19,3},{4,20},{20... | collective-permute-start | bytes 3145736 | tf_op jit(solution)/shard_map/ppermute | solution.py:276
  77.3 0.0 copy-done.4
  77.4 0.6 pad_add_fusion.place_ref
  78.0 1.3 collective-permute-done.7.other_ref
  79.3 6.1 %attend.1.proj_ref = bf16[16,128,128]{2,1,0:T(8,128)(2,1)} custom-call(s32[33]{0:T(128)} %pad_add_fusion.place_ref, f32[1]{0:T(128)S(6)} %copy.23.lam_ref, bf16[128,128]{1,0:T(8,128)(2,1)} %bitcast.33, bf16[16,128,256]{2,1,0:T(8,128)(2,1)} %constant_dynamic-update-slice_fusion.own_ref, bf16[16,128,256]{2,1,0:T(8,128)(2,1)} %collective-permute-done.7.other_ref, ...), custom_call_target="tpu_custom_call" | custom-call | tf_op jit(solution)/shard_map/attend/pallas_call | solution.py:264
  85.4 3.6 %all-to-all-done.1.x_ref = bf16[16,640,128]{2,1,0:T(8,128)(2,1)S(1)} async-done(((bf16[16,640,128]{2,1,0:T(8,128)(2,1)}), bf16[16,640,128]{2,1,0:T(8,128)(2,1)S(1)}, u32[]{:S(2)}, u32[]{:S(2)}) %all-to-all-start.1) | async-done | bytes 2621472 | tf_op jit(solution)/shard_map/all_to_all | solution.py:280
  89.0 0.0 copy-start
  89.0 1.5 copy-done
  90.5 6.2 %ffn.1 = bf16[16,768,128]{2,1,0:T(8,128)(2,1)} custom-call(bf16[16,640,128]{2,1,0:T(8,128)(2,1)} %copy-done, bf16[2048,256]{1,0:T(8,128)(2,1)} %bitcast.21, bf16[2048,256]{1,0:T(8,128)(2,1)} %bitcast.22, bf16[256,2048]{1,0:T(8,128)(2,1)} %bitcast.23, bf16[16,128,128]{2,1,0:T(8,128)(2,1)} %attend.1.proj_ref), custom_call_target="tpu_custom_call" | custom-call | tf_op jit(solution)/shard_map/ffn/pallas_call | solution.py:134
  96.7 41.9 %all_to_all.20.in_ref = bf16[16,768,128]{2,1,0:T(8,128)(2,1)} all-to-all(bf16[16,768,128]{2,1,0:T(8,128)(2,1)} %ffn.1), channel_id=1, replica_groups=mesh['z'=16,'core'=2,'y'=4,'x'=4] {'y','x'}, dimensions={0} | all-to-all | bytes 6291456 | tf_op jit(solution)/shard_map/all_to_all | solution.py:280
  138.6 4.5 %reduce_terms.1 = (bf16[32,24,128]{2,1,0:T(8,128)(2,1)}, bf16[8,2048]{1,0:T(8,128)(2,1)}) custom-call(bf16[16,768,128]{2,1,0:T(8,128)(2,1)} %all_to_all.20.in_ref), custom_call_target="tpu_custom_call" | custom-call | tf_op jit(solution)/shard_map/reduce_terms/pallas_call | solution.py:180
  143.1 26.7 %all_to_all.21.back_ref = bf16[32,24,128]{2,1,0:T(8,128)(2,1)} all-to-all(bf16[32,24,128]{2,1,0:T(8,128)(2,1)} %get-tuple-element.5), channel_id=1, replica_groups=mesh['z'=16,'core'=2,'y'=4,'x'=4] {'z','core'}, dimensions={0} | all-to-all | bytes 393216 | tf_op jit(solution)/shard_map/all_to_all | solution.py:280
  169.7 2.0 %combine.1 = bf16[128,128]{1,0:T(8,128)(2,1)} custom-call(bf16[32,24,128]{2,1,0:T(8,128)(2,1)} %all_to_all.21.back_ref, s32[4,128]{1,0:T(4,128)} %bitcast.36, f32[4,128]{1,0:T(4,128)} %bitcast.37), custom_call_target="tpu_custom_call" | custom-call | tf_op jit(solution)/shard_map/combine/pallas_call | solution.py:210
  (4 shorter events, 0.1 us)
Async XLA Ops:
  2.8 38.7 %all-to-all-start = ((bf16[32,24,128]{2,1,0:T(8,128)(2,1)}), bf16[32,24,128]{2,1,0:T(8,128)(2,1)S(1)}, u32[]{:S(2)}, u32[]{:S(2)}) async-start(bf16[32,24,128]{2,1,0:T(8,128)(2,1)} %dispatch.1), calls=%async_computation | async-start | bytes 393216 | tf_op jit(solution)/shard_map/all_to_all | solution.py:280
  20.4 31.7 %collective-permute-start.1 = (bf16[128,256]{1,0:T(8,128)(2,1)S(1)}, bf16[128,256]{1,0:T(8,128)(2,1)S(1)}, u32[]{:S(2)}, u32[]{:S(2)}) collective-permute-start(bf16[128,256]{1,0:T(8,128)(2,1)S(1)} %get-tuple-element.11), channel_id=1, source_target_pairs={{0,384},{32,416},{64,448},{96,480},{128,0},{160,32},{192,64},{224,... | collective-permute-start | bytes 196616 | tf_op jit(solution)/shard_map/ppermute | solution.py:276
  27.6 24.4 %collective-permute-start.2 = (bf16[128,256]{1,0:T(8,128)(2,1)S(1)}, bf16[128,256]{1,0:T(8,128)(2,1)S(1)}, u32[]{:S(2)}, u32[]{:S(2)}) collective-permute-start(bf16[128,256]{1,0:T(8,128)(2,1)S(1)} %get-tuple-element.11), channel_id=1, source_target_pairs={{0,256},{32,288},{64,320},{96,352},{128,384},{160,416},{192,448},{... | collective-permute-start | bytes 196616 | tf_op jit(solution)/shard_map/ppermute | solution.py:276
  34.5 17.5 %collective-permute-start = (bf16[128,256]{1,0:T(8,128)(2,1)S(1)}, bf16[128,256]{1,0:T(8,128)(2,1)S(1)}, u32[]{:S(2)}, u32[]{:S(2)}) collective-permute-start(bf16[128,256]{1,0:T(8,128)(2,1)S(1)} %get-tuple-element.11), channel_id=1, source_target_pairs={{0,128},{32,160},{64,192},{96,224},{128,256},{160,288},{192,320},{... | collective-permute-start | bytes 196616 | tf_op jit(solution)/shard_map/ppermute | solution.py:276
  41.6 0.7 copy-start.1
  45.1 19.1 %copy-start.2 = (bf16[128,1,128]{2,0,1:T(8,128)(2,1)S(1)}, bf16[128,1,128]{2,0,1:T(8,128)(2,1)}, u32[]{:S(2)}) copy-start(bf16[128,1,128]{2,0,1:T(8,128)(2,1)} %param.16) | copy-start | bytes 98308
  45.1 19.1 %copy-start.3 = (bf16[128,1,128]{2,0,1:T(8,128)(2,1)S(1)}, bf16[128,1,128]{2,0,1:T(8,128)(2,1)}, u32[]{:S(2)}) copy-start(bf16[128,1,128]{2,0,1:T(8,128)(2,1)} %param.15) | copy-start | bytes 98308
  45.1 32.2 %copy-start.4 = (s32[16]{0:T(128)S(1)}, s32[16]{0:T(128)}, u32[]{:S(2)}) copy-start(s32[16]{0:T(128)} %constant.43.clone) | copy-start | bytes 196
  45.1 43.8 %all-to-all-start.1 = ((bf16[16,640,128]{2,1,0:T(8,128)(2,1)}), bf16[16,640,128]{2,1,0:T(8,128)(2,1)S(1)}, u32[]{:S(2)}, u32[]{:S(2)}) async-start(bf16[16,640,128]{2,1,0:T(8,128)(2,1)} %compact.1), calls=%async_computation.1 | async-start | bytes 5242880 | tf_op jit(solution)/shard_map/all_to_all | solution.py:280
  52.1 14.8 %collective-permute-start.4 = (bf16[4,128,256]{2,1,0:T(8,128)(2,1)S(1)}, bf16[4,128,256]{2,1,0:T(8,128)(2,1)S(1)}, u32[]{:S(2)}, u32[]{:S(2)}) collective-permute-start(bf16[4,128,256]{2,1,0:T(8,128)(2,1)S(1)} %pad_maximum_fusion), channel_id=1, source_target_pairs={{0,480},{32,0},{64,32},{96,64},{128,96},{160,128},{192,160},{224,1... | collective-permute-start | bytes 786440 | tf_op jit(solution)/shard_map/ppermute | solution.py:276
  54.3 11.9 %collective-permute-start.3 = (bf16[4,128,256]{2,1,0:T(8,128)(2,1)S(1)}, bf16[4,128,256]{2,1,0:T(8,128)(2,1)S(1)}, u32[]{:S(2)}, u32[]{:S(2)}) collective-permute-start(bf16[4,128,256]{2,1,0:T(8,128)(2,1)S(1)} %pad_maximum_fusion), channel_id=1, source_target_pairs={{0,32},{32,64},{64,96},{96,128},{128,160},{160,192},{192,224},{224... | collective-permute-start | bytes 786440 | tf_op jit(solution)/shard_map/ppermute | solution.py:276
  57.4 11.1 %collective-permute-start.6 = (bf16[2,128,256]{2,1,0:T(8,128)(2,1)S(1)}, bf16[2,128,256]{2,1,0:T(8,128)(2,1)S(1)}, u32[]{:S(2)}, u32[]{:S(2)}) collective-permute-start(bf16[2,128,256]{2,1,0:T(8,128)(2,1)S(1)} %get-tuple-element.8), channel_id=1, source_target_pairs={{0,448},{32,480},{64,0},{96,32},{128,64},{160,96},{192,128},{224,1... | collective-permute-start | bytes 393224 | tf_op jit(solution)/shard_map/ppermute | solution.py:276
  59.6 8.2 %collective-permute-start.5 = (bf16[2,128,256]{2,1,0:T(8,128)(2,1)S(1)}, bf16[2,128,256]{2,1,0:T(8,128)(2,1)S(1)}, u32[]{:S(2)}, u32[]{:S(2)}) collective-permute-start(bf16[2,128,256]{2,1,0:T(8,128)(2,1)S(1)} %get-tuple-element.9), channel_id=1, source_target_pairs={{0,64},{32,96},{64,128},{96,160},{128,192},{160,224},{192,256},{22... | collective-permute-start | bytes 393224 | tf_op jit(solution)/shard_map/ppermute | solution.py:276
  69.2 10.1 %collective-permute-start.7 = (bf16[16,128,256]{2,1,0:T(8,128)(2,1)}, bf16[16,128,256]{2,1,0:T(8,128)(2,1)}, u32[]{:S(2)}, u32[]{:S(2)}) collective-permute-start(bf16[16,128,256]{2,1,0:T(8,128)(2,1)} %constant_dynamic-update-slice_fusion.own_ref), channel_id=1, source_target_pairs={{0,16},{16,0},{1,17},{17,1},{2,18},{18,2},{3,19},{19,3},{4,20},{20... | collective-permute-start | bytes 3145736 | tf_op jit(solution)/shard_map/ppermute | solution.py:276
  89.0 1.5 copy-start

commit v2 on v1

v2 whole, which is shorter than its diff:
```python
import jax
import jax.numpy as jnp
from jax import lax
from jax.experimental import pallas as pl
from jax.experimental.pallas import tpu as pltpu
from jax.sharding import Mesh, PartitionSpec as P


NORM_EPS = 1e-05
CLAMP_LIMIT = 7.0
GATE_SLOPE = 1.702
BF16 = jnp.bfloat16
F32 = jnp.float32

Z, CORE, Y, X = 16, 2, 4, 4
EP = ("z", "core")
TP = ("y", "x")
N_EP = Z * CORE
N_TP = Y * X
TOK = 128
CAP = 20
PAD = 24
ROWS = N_EP * CAP
PADDED = N_EP * PAD
WIDE = 128
MODEL = N_TP * WIDE
OUT_ROWS = ROWS + TOK

STEPS = (0, 4, 2, 6, 1, 5, 3, 7)
MIB = 1 << 20


def in_vmem(array):
    return pltpu.with_memory_space_constraint(array, pltpu.VMEM)


def params(mib):
    return pltpu.CompilerParams(vmem_limit_bytes=mib * MIB)


def routing(ids, values=None):
    expert = lax.broadcasted_iota(jnp.int32, (N_EP, TOK), 0)
    named = jnp.zeros((N_EP, TOK), F32)
    weight = jnp.zeros((N_EP, TOK), F32)
    for k in range(ids.shape[0]):
        hit = ids[k : k + 1, :] == expert
        named = named + jnp.where(hit, 1.0, 0.0)
        if values is not None:
            weight = weight + jnp.where(hit, values[k : k + 1, :], 0.0)
    earlier = lax.broadcasted_iota(jnp.int32, (TOK, TOK), 0) < lax.broadcasted_iota(
        jnp.int32, (TOK, TOK), 1
    )
    rank = jnp.dot(
        named.astype(BF16),
        jnp.where(earlier, 1.0, 0.0).astype(BF16),
        preferred_element_type=F32,
    )
    slot = jnp.where(named > 0.5, rank.astype(jnp.int32), -1)
    place = lax.broadcasted_iota(jnp.int32, (PAD, TOK), 0)
    pieces = []
    for e in range(N_EP):
        here = slot[e : e + 1, :] == place
        pieces.append(jnp.where(here, 1.0 if values is None else weight[e : e + 1, :], 0.0))
    return jnp.concatenate(pieces, axis=0)


def dispatch_kernel(at_ref, rows_ref, part_ref, gain_ref, ids_ref, out_ref):
    rows = rows_ref[...].astype(F32)
    mean_sq = jnp.mean(rows * rows, axis=-1, keepdims=True)
    part = part_ref[...].astype(F32) * lax.rsqrt(mean_sq + NORM_EPS) * gain_ref[...]
    chosen = routing(ids_ref[...]).astype(BF16)
    packed = jnp.dot(chosen, part.astype(BF16), preferred_element_type=F32)
    out_ref[...] = packed.astype(BF16).reshape(N_EP, PAD, WIDE)


def dispatch(at, token_rows, gain, ids):
    return pl.pallas_call(
        dispatch_kernel,
        out_shape=jax.ShapeDtypeStruct((N_EP, PAD, WIDE), BF16),
        grid_spec=pltpu.PrefetchScalarGridSpec(
            num_scalar_prefetch=1,
            grid=(1,),
            in_specs=[
                pl.BlockSpec((TOK, MODEL), lambda i, at: (0, 0)),
                pl.BlockSpec((TOK, WIDE), lambda i, at: (0, at[0])),
                pl.BlockSpec((1, WIDE), lambda i, at: (0, at[0])),
                pl.BlockSpec((4, TOK), lambda i, at: (0, 0)),
            ],
            out_specs=pl.BlockSpec((N_EP, PAD, WIDE), lambda i, at: (0, 0, 0)),
        ),
        compiler_params=params(8),
        name="dispatch",
    )(at, token_rows, token_rows, gain, ids)


COMPACT_STEPS = 4
COMPACT_SRC = N_EP // COMPACT_STEPS


def compact_kernel(in_ref, out_ref):
    to = lax.broadcasted_iota(jnp.int32, (2 * CAP, 2 * PAD), 0)
    src = lax.broadcasted_iota(jnp.int32, (2 * CAP, 2 * PAD), 1)
    pick = jnp.where(src == jnp.where(to < CAP, to, to + (PAD - CAP)), 1.0, 0.0).astype(BF16)
    for g in range(0, COMPACT_SRC, 2):
        block = in_ref[g : g + 2].reshape(2 * PAD, WIDE)
        kept = jnp.dot(pick, block, preferred_element_type=F32).astype(BF16)
        for t in range(N_TP):
            out_ref[t, CAP * g : CAP * (g + 2), :] = kept


def compact(arrived):
    return pl.pallas_call(
        compact_kernel,
        out_shape=pltpu.HBM((N_TP, ROWS, WIDE), BF16),
        grid=(COMPACT_STEPS,),
        in_specs=[pl.BlockSpec((COMPACT_SRC, PAD, WIDE), lambda i: (i, 0, 0))],
        out_specs=pl.BlockSpec((N_TP, COMPACT_SRC * CAP, WIDE), lambda i: (0, i, 0)),
        compiler_params=params(8),
        name="compact",
    )(arrived)


FFN_ROWS = ROWS // 2


def ffn_kernel(x_ref, wg_hbm, wu_hbm, wd_hbm, proj_ref, out_ref, wg_ref, wu_ref, wd_ref, sems):
    loads = [
        pltpu.make_async_copy(src, dst, sems.at[n])
        for n, (src, dst) in enumerate(((wg_hbm, wg_ref), (wu_hbm, wu_ref), (wd_hbm, wd_ref)))
    ]
    for load in loads:
        load.start()
    out_ref[:, ROWS:, :] = proj_ref[...]
    for low in range(0, ROWS, FFN_ROWS):
        here = slice(low, low + FFN_ROWS)
        rows = jnp.concatenate([x_ref[t, here, :] for t in range(N_TP)], axis=-1)
        if low == 0:
            loads[0].wait()
        gate = jnp.dot(rows, wg_ref[...], preferred_element_type=F32)
        if low == 0:
            loads[1].wait()
        up = jnp.dot(rows, wu_ref[...], preferred_element_type=F32)
        gated = jnp.minimum(gate, CLAMP_LIMIT)
        clipped = jnp.clip(up, -CLAMP_LIMIT, CLAMP_LIMIT)
        active = ((clipped + 1.0) * gated * jax.nn.sigmoid(GATE_SLOPE * gated)).astype(BF16)
        if low == 0:
            loads[2].wait()
        terms = jnp.dot(active, wd_ref[...], preferred_element_type=F32).astype(BF16)
        for t in range(N_TP):
            out_ref[t, here, :] = terms[:, t * WIDE : (t + 1) * WIDE]


def ffn(x, wg, wu, wd, proj):
    vmem = pl.BlockSpec(memory_space=pltpu.VMEM)
    hbm = pl.BlockSpec(memory_space=pl.ANY)
    return pl.pallas_call(
        ffn_kernel,
        out_shape=pltpu.VMEM((N_TP, OUT_ROWS, WIDE), BF16),
        in_specs=[vmem, hbm, hbm, hbm, vmem],
        out_specs=vmem,
        scratch_shapes=[
            pltpu.VMEM(wg.shape, BF16),
            pltpu.VMEM(wu.shape, BF16),
            pltpu.VMEM(wd.shape, BF16),
            pltpu.SemaphoreType.DMA((3,)),
        ],
        compiler_params=params(16),
        name="ffn",
    )(
        in_vmem(x),
        *(pltpu.with_memory_space_constraint(w, pltpu.HBM) for w in (wg, wu, wd)),
        in_vmem(proj),
    )


def summed_rows(in_ref, low, count):
    total = in_ref[0, low : low + count, :].astype(F32)
    for t in range(1, N_TP):
        total = total + in_ref[t, low : low + count, :].astype(F32)
    return total.astype(BF16)


def reduce_kernel(in_ref, pack_ref, mixed_ref):
    to = lax.broadcasted_iota(jnp.int32, (2 * PAD, 2 * CAP), 0)
    src = lax.broadcasted_iota(jnp.int32, (2 * PAD, 2 * CAP), 1)
    hit = to == jnp.where(src < CAP, src, src + (PAD - CAP))
    place = jnp.where(hit, 1.0, 0.0).astype(BF16)
    for g in range(0, N_EP, 2):
        block = summed_rows(in_ref, CAP * g, 2 * CAP)
        spread = jnp.dot(place, block, preferred_element_type=F32).astype(BF16)
        pack_ref[g : g + 2] = spread.reshape(2, PAD, WIDE)
    for c in range(N_TP):
        mixed_ref[:, c * WIDE : (c + 1) * WIDE] = summed_rows(in_ref, ROWS + 8 * c, 8)


def reduce_terms(y):
    vmem = pl.BlockSpec(memory_space=pltpu.VMEM)
    return pl.pallas_call(
        reduce_kernel,
        out_shape=(
            pltpu.VMEM((N_EP, PAD, WIDE), BF16),
            jax.ShapeDtypeStruct((TOK // N_TP, MODEL), BF16),
        ),
        in_specs=[vmem],
        out_specs=(vmem, vmem),
        compiler_params=params(8),
        name="reduce_terms",
    )(in_vmem(y))


def weigh_kernel(ids_ref, weights_ref, high_ref, low_ref):
    spread = routing(ids_ref[...], weights_ref[...]).T
    high = spread.astype(BF16)
    high_ref[...] = high
    low_ref[...] = (spread - high.astype(F32)).astype(BF16)


def weigh(ids, weights):
    vmem = pl.BlockSpec(memory_space=pltpu.VMEM)
    return pl.pallas_call(
        weigh_kernel,
        out_shape=(pltpu.VMEM((TOK, PADDED), BF16),) * 2,
        in_specs=[vmem] * 2,
        out_specs=(vmem, vmem),
        compiler_params=params(8),
        name="weigh",
    )(ids, weights)


def combine_kernel(back_ref, high_ref, low_ref, out_ref):
    back = back_ref[...].reshape(PADDED, WIDE)
    mixed = jnp.dot(high_ref[...], back, preferred_element_type=F32)
    mixed = mixed + jnp.dot(low_ref[...], back, preferred_element_type=F32)
    out_ref[...] = mixed.astype(BF16)


def combine(back, high, low):
    vmem = pl.BlockSpec(memory_space=pltpu.VMEM)
    return pl.pallas_call(
        combine_kernel,
        out_shape=jax.ShapeDtypeStruct((TOK, WIDE), BF16),
        in_specs=[vmem] * 3,
        out_specs=vmem,
        compiler_params=params(8),
        name="combine",
    )(*(in_vmem(a) for a in (back, high, low)))


def attend_kernel(
    z_ref, core_ref, lam_ref, q_ref, a_ref, b_ref, c_ref, d_ref, gain_ref, w_ref, out_ref, score_ref
):
    q = q_ref[...]
    q = (q.astype(F32) * (64**-0.5)).astype(BF16)
    lane = lax.broadcasted_iota(jnp.int32, (TOK, WIDE), 1)
    zero = jnp.zeros_like(q)
    both = jnp.concatenate(
        [jnp.where(lane < 64, q, zero), jnp.where(lane < 64, zero, q)], axis=0
    )
    row = lax.broadcasted_iota(jnp.int32, (2 * TOK, TOK), 0)
    row = jnp.where(row < TOK, row, row - TOK)
    ahead = lax.broadcasted_iota(jnp.int32, (2 * TOK, TOK), 1) - row
    z, core = z_ref[0], core_ref[0]
    me = CORE * z + core
    chips = []
    for half, refs in ((core, (a_ref, b_ref)), (1 - core, (c_ref, d_ref))):
        for n, step in enumerate(STEPS):
            down = CORE * ((z - step) & (Z - 1))
            up = CORE * ((z + 1 + step) & (Z - 1))
            first = jnp.where(half == 0, down + 1, up)
            second = jnp.where(half == 0, down, up + 1)
            chips.append((refs[n // 4], 2 * (n % 4), (first, second)))
    top = jnp.full((2 * TOK, TOK), -1e30, F32)
    for n, (ref, low, blocks) in enumerate(chips):
        keys = ref[low : low + 2, :, :WIDE].reshape(2 * TOK, WIDE)
        scores = lax.dot_general(
            both, keys, (((1,), (1,)), ((), ())), preferred_element_type=F32
        )
        for h in range(2):
            part = scores[:, h * TOK : (h + 1) * TOK]
            part = jnp.where(ahead <= (me - blocks[h]) * TOK, part, -1e30)
            score_ref[n, :, h * TOK : (h + 1) * TOK] = part
            top = jnp.maximum(top, part)
    row_max = jnp.max(top, axis=-1, keepdims=True)
    total = jnp.zeros((2 * TOK, 2 * TOK), F32)
    value_sum = jnp.zeros((2 * TOK, WIDE), F32)
    for n, (ref, low, _) in enumerate(chips):
        terms = jnp.exp(score_ref[n] - row_max)
        total = total + terms
        values = ref[low : low + 2, :, WIDE:].reshape(2 * TOK, WIDE)
        value_sum = value_sum + jnp.dot(terms.astype(BF16), values, preferred_element_type=F32)
    ratio = value_sum / jnp.sum(total, axis=-1, keepdims=True)
    attended = ratio[:TOK] - lam_ref[0] * ratio[TOK:]
    mean_sq = jnp.mean(attended * attended, axis=-1, keepdims=True)
    head_rows = (attended * lax.rsqrt(mean_sq + NORM_EPS) * gain_ref[...]).astype(BF16)
    product = jnp.dot(head_rows, w_ref[...], preferred_element_type=F32).astype(BF16)
    for c in range(N_TP):
        piece = product[:, c * WIDE : (c + 1) * WIDE].reshape(N_TP, TOK // N_TP, WIDE)
        out_ref[:, 8 * c : 8 * (c + 1), :] = piece


def attend(z_at, core_at, lam, q, blocks, gain, w):
    vmem = pl.BlockSpec(memory_space=pltpu.VMEM)
    smem = pl.BlockSpec(memory_space=pltpu.SMEM)
    return pl.pallas_call(
        attend_kernel,
        out_shape=pltpu.VMEM((N_TP, TOK, WIDE), BF16),
        in_specs=[smem] * 3 + [vmem] * 7,
        out_specs=vmem,
        scratch_shapes=[pltpu.VMEM((Z, 2 * TOK, 2 * TOK), F32)],
        compiler_params=params(16),
        name="attend",
    )(z_at, core_at, lam, q, *blocks, gain, w)


def moved(array, source):
    pairs = []
    for z in range(Z):
        for core in range(CORE):
            sender = source(z, core)
            if sender is not None:
                pairs.append((sender[0] % Z * CORE + sender[1], z * CORE + core))
    return lax.ppermute(array, EP, pairs)


def along(array, by):
    return moved(array, lambda z, core: (z + by if core else z - by, core))


def across(array):
    return moved(array, lambda z, core: (z, 1 - core))


def exchanged(array, axes):
    return lax.all_to_all(array, axes, split_axis=0, concat_axis=0, tiled=True)


def collect_keys(keys, values, core_at):
    mine = jnp.concatenate([keys, values], axis=-1)
    first = moved(mine, lambda z, core: (z + 1, 0) if core else (z, 1))
    second = moved(mine, lambda z, core: (z + 1, 1) if core else None)
    pair = jnp.stack([first, jnp.where(core_at == 0, mine, second)])
    two = jnp.concatenate([pair, along(pair, 4)], axis=0)
    four = jnp.concatenate([two, along(two, 2)], axis=0)
    rest = along(four, 1)
    other = across(four)
    return four, rest, other, across(rest)


def body(
    query_maps,
    key_maps,
    value_rows,
    head_lambda,
    head_gain,
    out_weight,
    token_rows,
    norm_gain,
    expert_ids,
    route_weights,
    gate_weight,
    up_weight,
    down_weight,
):
    z_at = lax.axis_index("z").astype(jnp.int32)
    core_at = lax.axis_index("core").astype(jnp.int32)
    tp_at = lax.axis_index(TP).astype(jnp.int32)
    ids = expert_ids.T
    packed = dispatch(tp_at.reshape(1), token_rows, norm_gain.reshape(1, MODEL), ids)
    arrived = exchanged(packed, EP)
    blocks = collect_keys(
        key_maps.reshape(TOK, WIDE), value_rows.reshape(TOK, WIDE), core_at
    )
    proj = attend(
        z_at.reshape(1),
        core_at.reshape(1),
        head_lambda,
        query_maps.reshape(TOK, WIDE),
        blocks,
        head_gain.reshape(1, WIDE),
        out_weight,
    )
    high, low = weigh(ids, route_weights.T)
    spread = compact(arrived)
    x = exchanged(spread, TP)
    terms = ffn(x, gate_weight[0], up_weight[0], down_weight[0], proj)
    y = exchanged(terms, TP)
    back, mixed_rows = reduce_terms(y)
    returned = exchanged(back, EP)
    mixed_experts = combine(returned, high, low)
    return (mixed_rows, mixed_experts)


def solution(mesh):
    fine = Mesh(mesh.devices.reshape(Z, CORE, Y, X), ("z", "core", "y", "x"))
    placed = (
        P(EP, TP, None),
        P(EP, TP, None),
        P(EP, TP, None),
        P(TP),
        P(),
        P(TP, None),
        P(EP, None),
        P(),
        P(EP, None),
        P(EP, None),
        P(EP, None, TP),
        P(EP, None, TP),
        P(EP, TP, None),
    )
    return jax.shard_map(
        body,
        mesh=fine,
        in_specs=placed,
        out_specs=(P((*EP, *TP), None), P(EP, TP)),
        check_vma=False,
    )
```

time: 173 us -> 181 us (1.046)
  waiting for transfers between devices: 5.13 us -> 42.5 us
  starting transfers between devices: 63.8 us -> 36.5 us
  blocking collectives: 68.5 us -> 80.6 us
  Pallas kernels: 23.9 us -> 13.5 us
  other arithmetic: 2.1 us -> 0.13 us
    ppermute x8 -> x7, waiting for transfers between devices: 1.55 us -> 24.1 us  [moved(): return lax.ppermute(array, EP, pairs)]
    ppermute x8 -> x7, starting transfers between devices: 40.1 us -> 22.4 us  [moved(): return lax.ppermute(array, EP, pairs)]
    all_to_all x2, waiting for transfers between devices: 3.57 us -> 18.4 us  [exchanged(): return lax.all_to_all(array, axes, split_axis=0, concat_axis=0, tiled=True)]
    all_to_all x2, blocking collectives: 68.5 us -> 80.6 us  [exchanged(): return lax.all_to_all(array, axes, split_axis=0, concat_axis=0, tiled=True)]
    all_to_all x2, starting transfers between devices: 23.6 us -> 14.1 us  [exchanged(): return lax.all_to_all(array, axes, split_axis=0, concat_axis=0, tiled=True)]
    pallas_call x4 -> x5, Pallas kernels: 19.7 us -> 12.3 us  [the longest x1 4.53 us: ffn(): pl.pallas_call(ffn_kernel, out_shape=pltpu.VMEM((N_TP, OUT_ROWS, WIDE), B...]
    unnamed x16 -> x24, local copies, waits for them, and re-layouts: 6.23 us -> 5.31 us
  transfers between devices with their start and end apart: 10 -> 9, of which waited for: 3 -> 7; matrix products, arithmetic and copies ran while one was open for 4% -> 0% of each run, Pallas kernels for 5% -> 2%
where the time goes in v2:
time: 181 us; the launch traced here: 180 us
  blocking collectives  80.6 us (45%)
  waiting for transfers between devices  42.5 us (23%)
  starting transfers between devices  36.5 us (20%)
  Pallas kernels  13.5 us (7%)
  local copies, waits for them, and re-layouts  5.31 us (3%)
    all_to_all x2, blocking collectives, exchanged(): return lax.all_to_all(array, axes, split_axis=0, concat_axis=0, tiled=True)  80.6 us
    ppermute x7, waiting for transfers between devices, moved(): return lax.ppermute(array, EP, pairs)  24.1 us
    ppermute x7, starting transfers between devices, moved(): return lax.ppermute(array, EP, pairs)  22.4 us
    all_to_all x2, waiting for transfers between devices, exchanged(): return lax.all_to_all(array, axes, split_axis=0, concat_axis=0, tiled=True)  18.4 us
    all_to_all x2, starting transfers between devices, exchanged(): return lax.all_to_all(array, axes, split_axis=0, concat_axis=0, tiled=True)  14.1 us
    unnamed x24, local copies, waits for them, and re-layouts  5.31 us
    pallas_call x1, Pallas kernels, ffn(): pl.pallas_call(ffn_kernel, out_shape=pltpu.VMEM((N_TP, OUT_ROWS, WIDE), B...  4.53 us
    pallas_call x1, Pallas kernels, attend(): pl.pallas_call(attend_kernel, out_shape=pltpu.VMEM((N_TP, TOK, WIDE), BF1...  3.81 us
  transfers between devices with their start and end apart: 9, of which 7 were waited for; matrix products, arithmetic and copies ran while one was open for 0% of the time, Pallas kernels for 2%

profile of v2, /device:TPU:1, one launch (start us, length us, event | category | flops | bytes accessed | tf_op | source)
XLA Modules:
  0.0 180.0 jit_solution(13313405921606528133)
XLA Ops:
  0.6 0.0 copy-start
  0.6 1.0 copy-done
  1.7 0.0 copy-start.5
  1.7 0.7 copy-done.5
  2.4 0.0 copy-start.6
  2.4 0.7 copy-done.6
  3.1 0.4 dispatch.1
  3.5 35.3 %all_to_all.20.in_ref = bf16[32,24,128]{2,1,0:T(8,128)(2,1)S(1)} all-to-all(bf16[32,24,128]{2,1,0:T(8,128)(2,1)S(1)} %dispatch.1), channel_id=1, replica_groups=mesh['z'=16,'core'=2,'y'=4,'x'=4] {'z','core'}, dimensions={0} | all-to-all | bytes 393216 | tf_op jit(solution)/shard_map/all_to_all | solution.py:334
  38.8 2.4 %compact.1 = bf16[16,640,128]{2,1,0:T(8,128)(2,1)} custom-call(bf16[32,24,128]{2,1,0:T(8,128)(2,1)S(1)} %all_to_all.20.in_ref), custom_call_target="tpu_custom_call" | custom-call | tf_op jit(solution)/shard_map/compact/pallas_call | solution.py:112
  41.2 0.0 copy-start.10
  41.2 0.0 copy-start.11
  41.2 0.0 copy-start.4
  41.2 0.0 copy-start.9
  41.2 6.9 %all-to-all-start.1 = ((bf16[16,640,128]{2,1,0:T(8,128)(2,1)}), bf16[16,640,128]{2,1,0:T(8,128)(2,1)S(1)}, u32[]{:S(2)}, u32[]{:S(2)}) async-start(bf16[16,640,128]{2,1,0:T(8,128)(2,1)} %compact.1), calls=%async_computation.1 | async-start | bytes 5242880 | tf_op jit(solution)/shard_map/all_to_all | solution.py:334
  48.1 0.0 copy-done.10
  48.1 0.0 copy-done.11
  48.1 1.9 %collective-permute-start.1 = (bf16[128,256]{1,0:T(8,128)(2,1)S(1)}, bf16[128,256]{1,0:T(8,128)(2,1)S(1)}, u32[]{:S(2)}, u32[]{:S(2)}) collective-permute-start(bf16[128,256]{1,0:T(8,128)(2,1)S(1)} %pad_maximum_fusion.3), channel_id=1, source_target_pairs={{48,16},{80,48},{112,80},{144,112},{176,144},{208,176},{240,208},{... | collective-permute-start | bytes 196616 | tf_op jit(solution)/shard_map/ppermute | solution.py:322
  50.1 0.5 collective-permute-start
  50.5 2.7 %collective-permute-done.1 = bf16[128,256]{1,0:T(8,128)(2,1)S(1)} collective-permute-done((bf16[128,256]{1,0:T(8,128)(2,1)S(1)}, bf16[128,256]{1,0:T(8,128)(2,1)S(1)}, u32[]{:S(2)}, u32[]{:S(2)}) %collective-permute-start.1) | collective-permute-done | bytes 65568 | tf_op jit(solution)/shard_map/ppermute | solution.py:322
  53.2 0.6 collective-permute-done
  53.9 3.1 %collective-permute-start.2 = (bf16[2,128,256]{2,1,0:T(8,128)(2,1)S(1)}, bf16[2,128,256]{2,1,0:T(8,128)(2,1)S(1)}, u32[]{:S(2)}, u32[]{:S(2)}) collective-permute-start(bf16[2,128,256]{2,1,0:T(8,128)(2,1)S(1)} %pad_maximum_fusion.2), channel_id=1, source_target_pairs={{384,0},{144,16},{416,32},{176,48},{448,64},{208,80},{480,96},{240... | collective-permute-start | bytes 393224 | tf_op jit(solution)/shard_map/ppermute | solution.py:322
  56.9 9.8 %collective-permute-done.2 = bf16[2,128,256]{2,1,0:T(8,128)(2,1)S(1)} collective-permute-done((bf16[2,128,256]{2,1,0:T(8,128)(2,1)S(1)}, bf16[2,128,256]{2,1,0:T(8,128)(2,1)S(1)}, u32[]{:S(2)}, u32[]{:S(2)}) %collective-permute-start.2) | collective-permute-done | bytes 131104 | tf_op jit(solution)/shard_map/ppermute | solution.py:322
  66.7 1.9 %collective-permute-start.3 = (bf16[4,128,256]{2,1,0:T(8,128)(2,1)S(1)}, bf16[4,128,256]{2,1,0:T(8,128)(2,1)S(1)}, u32[]{:S(2)}, u32[]{:S(2)}) collective-permute-start(bf16[4,128,256]{2,1,0:T(8,128)(2,1)S(1)} %pad_maximum_fusion.1), channel_id=1, source_target_pairs={{448,0},{80,16},{480,32},{112,48},{0,64},{144,80},{32,96},{176,112... | collective-permute-start | bytes 786440 | tf_op jit(solution)/shard_map/ppermute | solution.py:322
  68.7 6.5 %collective-permute-done.3 = bf16[4,128,256]{2,1,0:T(8,128)(2,1)S(1)} collective-permute-done((bf16[4,128,256]{2,1,0:T(8,128)(2,1)S(1)}, bf16[4,128,256]{2,1,0:T(8,128)(2,1)S(1)}, u32[]{:S(2)}, u32[]{:S(2)}) %collective-permute-start.3) | collective-permute-done | bytes 262176 | tf_op jit(solution)/shard_map/ppermute | solution.py:322
  75.1 0.1 pad_maximum_fusion.a_ref
  75.2 6.8 %collective-permute-start.4 = (bf16[8,128,256]{2,1,0:T(8,128)(2,1)S(1)}, bf16[8,128,256]{2,1,0:T(8,128)(2,1)}, u32[]{:S(2)}, u32[]{:S(2)}) collective-permute-start(bf16[8,128,256]{2,1,0:T(8,128)(2,1)S(1)} %pad_maximum_fusion.a_ref), channel_id=1, source_target_pairs={{480,0},{48,16},{0,32},{80,48},{32,64},{112,80},{64,96},{144,112},... | collective-permute-start | bytes 1572872 | tf_op jit(solution)/shard_map/ppermute | solution.py:322
  82.0 1.9 %collective-permute-start.5 = (bf16[8,128,256]{2,1,0:T(8,128)(2,1)S(1)}, bf16[8,128,256]{2,1,0:T(8,128)(2,1)}, u32[]{:S(2)}, u32[]{:S(2)}) collective-permute-start(bf16[8,128,256]{2,1,0:T(8,128)(2,1)S(1)} %pad_maximum_fusion.a_ref), channel_id=1, source_target_pairs={{16,0},{0,16},{48,32},{32,48},{80,64},{64,80},{112,96},{96,112},{1... | collective-permute-start | bytes 1572872 | tf_op jit(solution)/shard_map/ppermute | solution.py:322
  84.0 0.0 copy-start.1
  84.0 0.8 copy-done.1
  84.8 3.4 %collective-permute-done.4.b_ref = bf16[8,128,256]{2,1,0:T(8,128)(2,1)} collective-permute-done((bf16[8,128,256]{2,1,0:T(8,128)(2,1)S(1)}, bf16[8,128,256]{2,1,0:T(8,128)(2,1)}, u32[]{:S(2)}, u32[]{:S(2)}) %collective-permute-start.4) | collective-permute-done | bytes 524320 | tf_op jit(solution)/shard_map/ppermute | solution.py:322
  88.1 6.2 %collective-permute-start.6 = (bf16[8,128,256]{2,1,0:T(8,128)(2,1)}, bf16[8,128,256]{2,1,0:T(8,128)(2,1)}, u32[]{:S(2)}, u32[]{:S(2)}) collective-permute-start(bf16[8,128,256]{2,1,0:T(8,128)(2,1)} %collective-permute-done.4.b_ref), channel_id=1, source_target_pairs={{16,0},{0,16},{48,32},{32,48},{80,64},{64,80},{112,96},{96,112},{1... | collective-permute-start | bytes 1572872 | tf_op jit(solution)/shard_map/ppermute | solution.py:322
  95.0 0.0 collective-permute-done.5.c_ref
  95.0 1.2 collective-permute-done.6.d_ref
  96.2 0.0 copy-done.4
  96.2 0.0 copy-done.9
  96.2 1.0 copy-done.2
  97.3 1.0 copy-done.3
  98.3 3.8 %attend.1.proj_ref = bf16[16,128,128]{2,1,0:T(8,128)(2,1)S(1)} custom-call(s32[1]{0:T(128)} %bitcast.6.z_ref, s32[1]{0:T(128)} %bitcast.7.core_ref, f32[1]{0:T(128)S(6)} %copy.15.lam_ref, bf16[128,128]{1,0:T(8,128)(2,1)S(1)} %bitcast.16, bf16[8,128,256]{2,1,0:T(8,128)(2,1)S(1)} %copy-done.2, bf16[8,128,256]{2,1,0:T(8,128)(2,1)} %collective-permute-done.4.b_ref, ...), custom_call_target="tpu_custom_call" | custom-call | tf_op jit(solution)/shard_map/attend/pallas_call | solution.py:304
  102.1 0.0 all-to-all-done.1.x_ref
  102.1 4.5 %ffn.1 = bf16[16,768,128]{2,1,0:T(8,128)(2,1)S(1)} custom-call(bf16[16,640,128]{2,1,0:T(8,128)(2,1)S(1)} %all-to-all-done.1.x_ref, bf16[2048,256]{1,0:T(8,128)(2,1)} %bitcast.22, bf16[2048,256]{1,0:T(8,128)(2,1)} %bitcast.23, bf16[256,2048]{1,0:T(8,128)(2,1)} %bitcast.24, bf16[16,128,128]{2,1,0:T(8,128)(2,1)S(1)} %attend.1.proj_ref), custom_call_target="tpu_custom_call" | custom-call | tf_op jit(solution)/shard_map/ffn/pallas_call | solution.py:156
  106.7 45.3 %all_to_all.21.in_ref = bf16[16,768,128]{2,1,0:T(8,128)(2,1)S(1)} all-to-all(bf16[16,768,128]{2,1,0:T(8,128)(2,1)S(1)} %ffn.1), channel_id=1, replica_groups=mesh['z'=16,'core'=2,'y'=4,'x'=4] {'y','x'}, dimensions={0} | all-to-all | bytes 6291456 | tf_op jit(solution)/shard_map/all_to_all | solution.py:334
  151.9 1.2 reduce_terms.1
  153.2 7.2 %all-to-all-start.3 = ((bf16[32,24,128]{2,1,0:T(8,128)(2,1)}), bf16[32,24,128]{2,1,0:T(8,128)(2,1)S(1)}, u32[]{:S(2)}, u32[]{:S(2)}) async-start(bf16[32,24,128]{2,1,0:T(8,128)(2,1)} %get-tuple-element.7), calls=%async_computation.3 | async-start | bytes 393216 | tf_op jit(solution)/shard_map/all_to_all | solution.py:334
  160.4 0.0 copy-done.7
  160.4 0.0 copy-done.8
  160.4 0.3 weigh.1
  160.7 18.4 %all-to-all-done.3.back_ref = bf16[32,24,128]{2,1,0:T(8,128)(2,1)S(1)} async-done(((bf16[32,24,128]{2,1,0:T(8,128)(2,1)}), bf16[32,24,128]{2,1,0:T(8,128)(2,1)S(1)}, u32[]{:S(2)}, u32[]{:S(2)}) %all-to-all-start.3) | async-done | bytes 196640 | tf_op jit(solution)/shard_map/all_to_all | solution.py:334
  179.2 0.9 combine.1
  (8 shorter events, 0.1 us)
Async XLA Ops:
  0.6 1.0 copy-start
  1.7 0.7 copy-start.5
  2.4 0.7 copy-start.6
  41.2 6.9 %copy-start.10 = (bf16[128,1,128]{2,0,1:T(8,128)(2,1)S(1)}, bf16[128,1,128]{2,0,1:T(8,128)(2,1)}, u32[]{:S(2)}) copy-start(bf16[128,1,128]{2,0,1:T(8,128)(2,1)} %param.15) | copy-start | bytes 98308
  41.2 6.9 %copy-start.11 = (bf16[128,1,128]{2,0,1:T(8,128)(2,1)S(1)}, bf16[128,1,128]{2,0,1:T(8,128)(2,1)}, u32[]{:S(2)}) copy-start(bf16[128,1,128]{2,0,1:T(8,128)(2,1)} %param.14) | copy-start | bytes 98308
  41.2 55.1 %copy-start.4 = (bf16[128,1,128]{2,0,1:T(8,128)(2,1)S(1)}, bf16[128,1,128]{2,0,1:T(8,128)(2,1)}, u32[]{:S(2)}) copy-start(bf16[128,1,128]{2,0,1:T(8,128)(2,1)} %param.13) | copy-start | bytes 98308
  41.2 55.1 %copy-start.9 = (f32[128]{0:T(128)S(1)}, f32[128]{0:T(128)}, u32[]{:S(2)}) copy-start(f32[128]{0:T(128)} %param.17) | copy-start | bytes 1540
  41.2 61.0 %all-to-all-start.1 = ((bf16[16,640,128]{2,1,0:T(8,128)(2,1)}), bf16[16,640,128]{2,1,0:T(8,128)(2,1)S(1)}, u32[]{:S(2)}, u32[]{:S(2)}) async-start(bf16[16,640,128]{2,1,0:T(8,128)(2,1)} %compact.1), calls=%async_computation.1 | async-start | bytes 5242880 | tf_op jit(solution)/shard_map/all_to_all | solution.py:334
  48.1 5.1 %collective-permute-start.1 = (bf16[128,256]{1,0:T(8,128)(2,1)S(1)}, bf16[128,256]{1,0:T(8,128)(2,1)S(1)}, u32[]{:S(2)}, u32[]{:S(2)}) collective-permute-start(bf16[128,256]{1,0:T(8,128)(2,1)S(1)} %pad_maximum_fusion.3), channel_id=1, source_target_pairs={{48,16},{80,48},{112,80},{144,112},{176,144},{208,176},{240,208},{... | collective-permute-start | bytes 196616 | tf_op jit(solution)/shard_map/ppermute | solution.py:322
  50.1 3.8 %collective-permute-start = (bf16[128,256]{1,0:T(8,128)(2,1)S(1)}, bf16[128,256]{1,0:T(8,128)(2,1)S(1)}, u32[]{:S(2)}, u32[]{:S(2)}) collective-permute-start(bf16[128,256]{1,0:T(8,128)(2,1)S(1)} %pad_maximum_fusion.3), channel_id=1, source_target_pairs={{16,0},{32,16},{48,32},{64,48},{80,64},{96,80},{112,96},{128,112},... | collective-permute-start | bytes 196616 | tf_op jit(solution)/shard_map/ppermute | solution.py:322
  53.9 12.8 %collective-permute-start.2 = (bf16[2,128,256]{2,1,0:T(8,128)(2,1)S(1)}, bf16[2,128,256]{2,1,0:T(8,128)(2,1)S(1)}, u32[]{:S(2)}, u32[]{:S(2)}) collective-permute-start(bf16[2,128,256]{2,1,0:T(8,128)(2,1)S(1)} %pad_maximum_fusion.2), channel_id=1, source_target_pairs={{384,0},{144,16},{416,32},{176,48},{448,64},{208,80},{480,96},{240... | collective-permute-start | bytes 393224 | tf_op jit(solution)/shard_map/ppermute | solution.py:322
  66.7 8.4 %collective-permute-start.3 = (bf16[4,128,256]{2,1,0:T(8,128)(2,1)S(1)}, bf16[4,128,256]{2,1,0:T(8,128)(2,1)S(1)}, u32[]{:S(2)}, u32[]{:S(2)}) collective-permute-start(bf16[4,128,256]{2,1,0:T(8,128)(2,1)S(1)} %pad_maximum_fusion.1), channel_id=1, source_target_pairs={{448,0},{80,16},{480,32},{112,48},{0,64},{144,80},{32,96},{176,112... | collective-permute-start | bytes 786440 | tf_op jit(solution)/shard_map/ppermute | solution.py:322
  75.2 12.9 %collective-permute-start.4 = (bf16[8,128,256]{2,1,0:T(8,128)(2,1)S(1)}, bf16[8,128,256]{2,1,0:T(8,128)(2,1)}, u32[]{:S(2)}, u32[]{:S(2)}) collective-permute-start(bf16[8,128,256]{2,1,0:T(8,128)(2,1)S(1)} %pad_maximum_fusion.a_ref), channel_id=1, source_target_pairs={{480,0},{48,16},{0,32},{80,48},{32,64},{112,80},{64,96},{144,112},... | collective-permute-start | bytes 1572872 | tf_op jit(solution)/shard_map/ppermute | solution.py:322
  82.0 13.0 %collective-permute-start.5 = (bf16[8,128,256]{2,1,0:T(8,128)(2,1)S(1)}, bf16[8,128,256]{2,1,0:T(8,128)(2,1)}, u32[]{:S(2)}, u32[]{:S(2)}) collective-permute-start(bf16[8,128,256]{2,1,0:T(8,128)(2,1)S(1)} %pad_maximum_fusion.a_ref), channel_id=1, source_target_pairs={{16,0},{0,16},{48,32},{32,48},{80,64},{64,80},{112,96},{96,112},{1... | collective-permute-start | bytes 1572872 | tf_op jit(solution)/shard_map/ppermute | solution.py:322
  84.0 0.8 copy-start.1
  88.1 8.1 %collective-permute-start.6 = (bf16[8,128,256]{2,1,0:T(8,128)(2,1)}, bf16[8,128,256]{2,1,0:T(8,128)(2,1)}, u32[]{:S(2)}, u32[]{:S(2)}) collective-permute-start(bf16[8,128,256]{2,1,0:T(8,128)(2,1)} %collective-permute-done.4.b_ref), channel_id=1, source_target_pairs={{16,0},{0,16},{48,32},{32,48},{80,64},{64,80},{112,96},{96,112},{1... | collective-permute-start | bytes 1572872 | tf_op jit(solution)/shard_map/ppermute | solution.py:322
  96.2 1.0 copy-start.2
  97.3 1.0 copy-start.3
  151.9 8.4 %copy-start.7 = (s32[128,4]{0,1:T(4,128)S(1)}, s32[128,4]{0,1:T(4,128)}, u32[]{:S(2)}) copy-start(s32[128,4]{0,1:T(4,128)} %param.21) | copy-start | bytes 6148
  151.9 8.4 %copy-start.8 = (f32[128,4]{0,1:T(4,128)S(1)}, f32[128,4]{0,1:T(4,128)}, u32[]{:S(2)}) copy-start(f32[128,4]{0,1:T(4,128)} %param.22) | copy-start | bytes 6148
  153.2 26.0 %all-to-all-start.3 = ((bf16[32,24,128]{2,1,0:T(8,128)(2,1)}), bf16[32,24,128]{2,1,0:T(8,128)(2,1)S(1)}, u32[]{:S(2)}, u32[]{:S(2)}) async-start(bf16[32,24,128]{2,1,0:T(8,128)(2,1)} %get-tuple-element.7), calls=%async_computation.3 | async-start | bytes 393216 | tf_op jit(solution)/shard_map/all_to_all | solution.py:334

commit v3 on v2

--- a/solution.py
+++ b/solution.py
@@ -24,7 +24,7 @@
 PADDED = N_EP * PAD
 WIDE = 128
 MODEL = N_TP * WIDE
-OUT_ROWS = ROWS + TOK
+OWN_ROWS = TOK // N_TP
 
 STEPS = (0, 4, 2, 6, 1, 5, 3, 7)
 MIB = 1 << 20
@@ -90,7 +90,7 @@
         ),
         compiler_params=params(8),
         name="dispatch",
-    )(at, token_rows, token_rows, gain, ids)
+    )(at, *(pltpu.with_memory_space_constraint(a, pltpu.HBM) for a in (token_rows, token_rows, gain, ids)))
 
 
 COMPACT_STEPS = 4
@@ -123,54 +123,63 @@
 FFN_ROWS = ROWS // 2
 
 
-def ffn_kernel(x_ref, wg_hbm, wu_hbm, wd_hbm, proj_ref, out_ref, wg_ref, wu_ref, wd_ref, sems):
+def ffn_kernel(
+    x_ref, wg_hbm, wu_hbm, wd_hbm, out_hbm, wg_ref, wu_ref, wd_ref, out_ref, load_sems, store_sems
+):
     loads = [
-        pltpu.make_async_copy(src, dst, sems.at[n])
+        pltpu.make_async_copy(src, dst, load_sems.at[n])
         for n, (src, dst) in enumerate(((wg_hbm, wg_ref), (wu_hbm, wu_ref), (wd_hbm, wd_ref)))
     ]
     for load in loads:
         load.start()
-    out_ref[:, ROWS:, :] = proj_ref[...]
-    for low in range(0, ROWS, FFN_ROWS):
-        here = slice(low, low + FFN_ROWS)
+    stores = []
+    for n in range(ROWS // FFN_ROWS):
+        here = slice(n * FFN_ROWS, (n + 1) * FFN_ROWS)
         rows = jnp.concatenate([x_ref[t, here, :] for t in range(N_TP)], axis=-1)
-        if low == 0:
+        if n == 0:
             loads[0].wait()
         gate = jnp.dot(rows, wg_ref[...], preferred_element_type=F32)
-        if low == 0:
+        if n == 0:
             loads[1].wait()
         up = jnp.dot(rows, wu_ref[...], preferred_element_type=F32)
         gated = jnp.minimum(gate, CLAMP_LIMIT)
         clipped = jnp.clip(up, -CLAMP_LIMIT, CLAMP_LIMIT)
         active = ((clipped + 1.0) * gated * jax.nn.sigmoid(GATE_SLOPE * gated)).astype(BF16)
-        if low == 0:
+        if n == 0:
             loads[2].wait()
         terms = jnp.dot(active, wd_ref[...], preferred_element_type=F32).astype(BF16)
         for t in range(N_TP):
-            out_ref[t, here, :] = terms[:, t * WIDE : (t + 1) * WIDE]
-
-
-def ffn(x, wg, wu, wd, proj):
+            out_ref[n, t] = terms[:, t * WIDE : (t + 1) * WIDE]
+        stores.append(
+            pltpu.make_async_copy(
+                out_ref.at[n], out_hbm.at[:, pl.ds(n * FFN_ROWS, FFN_ROWS), :], store_sems.at[n]
+            )
+        )
+        stores[-1].start()
+    for store in stores:
+        store.wait()
+
+
+def ffn(x, wg, wu, wd):
     vmem = pl.BlockSpec(memory_space=pltpu.VMEM)
     hbm = pl.BlockSpec(memory_space=pl.ANY)
+    steps = ROWS // FFN_ROWS
     return pl.pallas_call(
         ffn_kernel,
-        out_shape=pltpu.VMEM((N_TP, OUT_ROWS, WIDE), BF16),
-        in_specs=[vmem, hbm, hbm, hbm, vmem],
-        out_specs=vmem,
+        out_shape=pltpu.HBM((N_TP, ROWS, WIDE), BF16),
+        in_specs=[vmem, hbm, hbm, hbm],
+        out_specs=hbm,
         scratch_shapes=[
             pltpu.VMEM(wg.shape, BF16),
             pltpu.VMEM(wu.shape, BF16),
             pltpu.VMEM(wd.shape, BF16),
+            pltpu.VMEM((steps, N_TP, FFN_ROWS, WIDE), BF16),
             pltpu.SemaphoreType.DMA((3,)),
+            pltpu.SemaphoreType.DMA((steps,)),
         ],
-        compiler_params=params(16),
+        compiler_params=params(20),
         name="ffn",
-    )(
-        in_vmem(x),
-        *(pltpu.with_memory_space_constraint(w, pltpu.HBM) for w in (wg, wu, wd)),
-        in_vmem(proj),
-    )
+    )(in_vmem(x), *(pltpu.with_memory_space_constraint(w, pltpu.HBM) for w in (wg, wu, wd)))
 
 
 def summed_rows(in_ref, low, count):
@@ -180,7 +189,7 @@
     return total.astype(BF16)
 
 
-def reduce_kernel(in_ref, pack_ref, mixed_ref):
+def reduce_kernel(in_ref, pack_ref):
     to = lax.broadcasted_iota(jnp.int32, (2 * PAD, 2 * CAP), 0)
     src = lax.broadcasted_iota(jnp.int32, (2 * PAD, 2 * CAP), 1)
     hit = to == jnp.where(src < CAP, src, src + (PAD - CAP))
@@ -189,23 +198,47 @@
         block = summed_rows(in_ref, CAP * g, 2 * CAP)
         spread = jnp.dot(place, block, preferred_element_type=F32).astype(BF16)
         pack_ref[g : g + 2] = spread.reshape(2, PAD, WIDE)
-    for c in range(N_TP):
-        mixed_ref[:, c * WIDE : (c + 1) * WIDE] = summed_rows(in_ref, ROWS + 8 * c, 8)
 
 
 def reduce_terms(y):
     vmem = pl.BlockSpec(memory_space=pltpu.VMEM)
     return pl.pallas_call(
         reduce_kernel,
-        out_shape=(
-            pltpu.VMEM((N_EP, PAD, WIDE), BF16),
-            jax.ShapeDtypeStruct((TOK // N_TP, MODEL), BF16),
-        ),
+        out_shape=jax.ShapeDtypeStruct((N_EP, PAD, WIDE), BF16),
         in_specs=[vmem],
-        out_specs=(vmem, vmem),
+        out_specs=vmem,
         compiler_params=params(8),
         name="reduce_terms",
     )(in_vmem(y))
+
+
+def partial_kernel(at_ref, *refs):
+    inputs, outputs = refs[:Y], refs[Y:]
+    total = inputs[0][...].astype(F32)
+    for ref in inputs[1:]:
+        total = total + ref[...].astype(F32)
+    if len(outputs) == 1:
+        outputs[0][...] = total.astype(BF16)
+        return
+    *outputs, total_ref = outputs
+    total_ref[...] = total
+    for step, ref in enumerate(outputs):
+        to = (at_ref[0] + step) % Y
+        ref[...] = total_ref[pl.ds(pl.multiple_of(to * OWN_ROWS, OWN_ROWS), OWN_ROWS), :].astype(BF16)
+
+
+def partial_sum(at, terms, last):
+    vmem = pl.BlockSpec(memory_space=pltpu.VMEM)
+    one = jax.ShapeDtypeStruct((OWN_ROWS, MODEL), BF16)
+    return pl.pallas_call(
+        partial_kernel,
+        out_shape=one if last else (one,) * Y,
+        in_specs=[pl.BlockSpec(memory_space=pltpu.SMEM)] + [vmem] * Y,
+        out_specs=vmem if last else (vmem,) * Y,
+        scratch_shapes=[] if last else [pltpu.VMEM((Y * OWN_ROWS, MODEL), F32)],
+        compiler_params=params(8),
+        name="sum_last" if last else "sum_first",
+    )(at, *terms)
 
 
 def weigh_kernel(ids_ref, weights_ref, high_ref, low_ref):
@@ -247,8 +280,20 @@
 
 
 def attend_kernel(
-    z_ref, core_ref, lam_ref, q_ref, a_ref, b_ref, c_ref, d_ref, gain_ref, w_ref, out_ref, score_ref
+    z_ref,
+    core_ref,
+    x_ref,
+    lam_ref,
+    q_ref,
+    a_ref,
+    b_ref,
+    c_ref,
+    d_ref,
+    gain_ref,
+    w_ref,
+    *out_and_scratch,
 ):
+    *out_refs, score_ref, product_ref = out_and_scratch
     q = q_ref[...]
     q = (q.astype(F32) * (64**-0.5)).astype(BF16)
     lane = lax.broadcasted_iota(jnp.int32, (TOK, WIDE), 1)
@@ -292,24 +337,30 @@
     attended = ratio[:TOK] - lam_ref[0] * ratio[TOK:]
     mean_sq = jnp.mean(attended * attended, axis=-1, keepdims=True)
     head_rows = (attended * lax.rsqrt(mean_sq + NORM_EPS) * gain_ref[...]).astype(BF16)
-    product = jnp.dot(head_rows, w_ref[...], preferred_element_type=F32).astype(BF16)
-    for c in range(N_TP):
-        piece = product[:, c * WIDE : (c + 1) * WIDE].reshape(N_TP, TOK // N_TP, WIDE)
-        out_ref[:, 8 * c : 8 * (c + 1), :] = piece
-
-
-def attend(z_at, core_at, lam, q, blocks, gain, w):
+    product_ref[...] = jnp.dot(head_rows, w_ref[...], preferred_element_type=F32)
+    for step, out_ref in enumerate(out_refs):
+        to = (x_ref[0] + step) % X
+        for y in range(Y):
+            low = pl.multiple_of((y * X + to) * OWN_ROWS, OWN_ROWS)
+            piece = product_ref[pl.ds(low, OWN_ROWS), :]
+            out_ref[y * OWN_ROWS : (y + 1) * OWN_ROWS, :] = piece.astype(BF16)
+
+
+def attend(z_at, core_at, x_at, lam, q, blocks, gain, w):
     vmem = pl.BlockSpec(memory_space=pltpu.VMEM)
     smem = pl.BlockSpec(memory_space=pltpu.SMEM)
     return pl.pallas_call(
         attend_kernel,
-        out_shape=pltpu.VMEM((N_TP, TOK, WIDE), BF16),
-        in_specs=[smem] * 3 + [vmem] * 7,
-        out_specs=vmem,
-        scratch_shapes=[pltpu.VMEM((Z, 2 * TOK, 2 * TOK), F32)],
+        out_shape=(jax.ShapeDtypeStruct((Y * OWN_ROWS, MODEL), BF16),) * X,
+        in_specs=[smem] * 4 + [vmem] * 7,
+        out_specs=(vmem,) * X,
+        scratch_shapes=[
+            pltpu.VMEM((Z, 2 * TOK, 2 * TOK), F32),
+            pltpu.VMEM((TOK, MODEL), F32),
+        ],
         compiler_params=params(16),
         name="attend",
-    )(z_at, core_at, lam, q, *blocks, gain, w)
+    )(z_at, core_at, x_at, lam, q, *blocks, gain, w)
 
 
 def moved(array, source):
@@ -328,6 +379,15 @@
 
 def across(array):
     return moved(array, lambda z, core: (z, 1 - core))
+
+
+def gathered(pieces, axis):
+    length = lax.axis_size(axis)
+    arrived = [pieces[0]]
+    for step in range(1, length):
+        pairs = [(i, (i + step) % length) for i in range(length)]
+        arrived.append(lax.ppermute(pieces[step], axis, pairs))
+    return arrived
 
 
 def exchanged(array, axes):
@@ -364,27 +424,32 @@
     z_at = lax.axis_index("z").astype(jnp.int32)
     core_at = lax.axis_index("core").astype(jnp.int32)
     tp_at = lax.axis_index(TP).astype(jnp.int32)
+    y_at = lax.axis_index("y").astype(jnp.int32).reshape(1)
+    x_at = lax.axis_index("x").astype(jnp.int32).reshape(1)
     ids = expert_ids.T
     packed = dispatch(tp_at.reshape(1), token_rows, norm_gain.reshape(1, MODEL), ids)
     arrived = exchanged(packed, EP)
     blocks = collect_keys(
         key_maps.reshape(TOK, WIDE), value_rows.reshape(TOK, WIDE), core_at
     )
-    proj = attend(
+    pieces = attend(
         z_at.reshape(1),
         core_at.reshape(1),
+        x_at,
         head_lambda,
         query_maps.reshape(TOK, WIDE),
         blocks,
         head_gain.reshape(1, WIDE),
         out_weight,
     )
+    pieces = partial_sum(y_at, gathered(pieces, "x"), last=False)
+    mixed_rows = partial_sum(y_at, gathered(pieces, "y"), last=True)
     high, low = weigh(ids, route_weights.T)
     spread = compact(arrived)
     x = exchanged(spread, TP)
-    terms = ffn(x, gate_weight[0], up_weight[0], down_weight[0], proj)
+    terms = ffn(x, gate_weight[0], up_weight[0], down_weight[0])
     y = exchanged(terms, TP)
-    back, mixed_rows = reduce_terms(y)
+    back = reduce_terms(y)
     returned = exchanged(back, EP)
     mixed_experts = combine(returned, high, low)
     return (mixed_rows, mixed_experts)

time: 181 us -> 175 us (0.967)
  waiting for transfers between devices: 42.5 us -> 20.8 us
  starting transfers between devices: 36.5 us -> 58 us
  blocking collectives: 80.6 us -> 74.8 us
  local copies, waits for them, and re-layouts: 5.31 us -> 1.08 us
  Pallas kernels: 13.5 us -> 16.2 us
    all_to_all x2, waiting for transfers between devices: 18.4 us -> 0.42 us  [exchanged(): return lax.all_to_all(array, axes, split_axis=0, concat_axis=0, tiled=True)]
    ppermute x0 -> x6, starting transfers between devices: none -> 17.3 us  [gathered(): arrived.append(lax.ppermute(pieces[step], axis, pairs))]
    ppermute x7, waiting for transfers between devices: 24.1 us -> 13.8 us  [moved(): return lax.ppermute(array, EP, pairs)]
    ppermute x0 -> x6, waiting for transfers between devices: none -> 6.53 us  [gathered(): arrived.append(lax.ppermute(pieces[step], axis, pairs))]
    all_to_all x2, blocking collectives: 80.6 us -> 74.8 us  [exchanged(): return lax.all_to_all(array, axes, split_axis=0, concat_axis=0, tiled=True)]
    unnamed x24 -> x14, local copies, waits for them, and re-layouts: 5.31 us -> 1.08 us
    ppermute x7, starting transfers between devices: 22.4 us -> 25 us  [moved(): return lax.ppermute(array, EP, pairs)]
    pallas_call x3 -> x5, Pallas kernels: 9.57 us -> 11.2 us  [the longest x1 5.64 us: ffn(): pl.pallas_call(ffn_kernel, out_shape=pltpu.HBM((N_TP, ROWS, WIDE), BF16),...]
  transfers between devices with their start and end apart: 9 -> 15, of which waited for: 7 -> 9; matrix products, arithmetic and copies ran while one was open for 0% -> 0% of each run, Pallas kernels for 2% -> 3%
where the time goes in v3:
time: 175 us; the launch traced here: 172 us
  blocking collectives  74.8 us (43%)
  starting transfers between devices  58 us (33%)
  waiting for transfers between devices  20.8 us (12%)
  Pallas kernels  16.2 us (9%)
    all_to_all x2, blocking collectives, exchanged(): return lax.all_to_all(array, axes, split_axis=0, concat_axis=0, tiled=True)  74.8 us
    ppermute x7, starting transfers between devices, moved(): return lax.ppermute(array, EP, pairs)  25 us
    ppermute x6, starting transfers between devices, gathered(): arrived.append(lax.ppermute(pieces[step], axis, pairs))  17.3 us
    all_to_all x2, starting transfers between devices, exchanged(): return lax.all_to_all(array, axes, split_axis=0, concat_axis=0, tiled=True)  15.6 us
    ppermute x7, waiting for transfers between devices, moved(): return lax.ppermute(array, EP, pairs)  13.8 us
    ppermute x6, waiting for transfers between devices, gathered(): arrived.append(lax.ppermute(pieces[step], axis, pairs))  6.53 us
    pallas_call x1, Pallas kernels, ffn(): pl.pallas_call(ffn_kernel, out_shape=pltpu.HBM((N_TP, ROWS, WIDE), BF16),...  5.64 us
    pallas_call x1, Pallas kernels, attend(): pl.pallas_call(attend_kernel, out_shape=(jax.ShapeDtypeStruct((Y * OWN_RO...  3.56 us
  transfers between devices with their start and end apart: 15, of which 9 were waited for; matrix products, arithmetic and copies ran while one was open for 0% of the time, Pallas kernels for 3%

profile of v3, /device:TPU:1, one launch (start us, length us, event | category | flops | bytes accessed | tf_op | source)
XLA Modules:
  0.0 172.5 jit_solution(6387577977083478765)
XLA Ops:
  0.6 1.5 dispatch.1
  2.2 35.3 %all_to_all.20.in_ref = bf16[32,24,128]{2,1,0:T(8,128)(2,1)S(1)} all-to-all(bf16[32,24,128]{2,1,0:T(8,128)(2,1)S(1)} %dispatch.1), channel_id=1, replica_groups=mesh['z'=16,'core'=2,'y'=4,'x'=4] {'z','core'}, dimensions={0} | all-to-all | bytes 393216 | tf_op jit(solution)/shard_map/all_to_all | solution.py:394
  37.5 2.3 %compact.1 = bf16[16,640,128]{2,1,0:T(8,128)(2,1)} custom-call(bf16[32,24,128]{2,1,0:T(8,128)(2,1)S(1)} %all_to_all.20.in_ref), custom_call_target="tpu_custom_call" | custom-call | tf_op jit(solution)/shard_map/compact/pallas_call | solution.py:112
  39.8 39.5 %all_to_all.21.x_ref = bf16[16,640,128]{2,1,0:T(8,128)(2,1)S(1)} all-to-all(bf16[16,640,128]{2,1,0:T(8,128)(2,1)} %compact.1), channel_id=1, replica_groups=mesh['z'=16,'core'=2,'y'=4,'x'=4] {'y','x'}, dimensions={0} | all-to-all | bytes 5242880 | tf_op jit(solution)/shard_map/all_to_all | solution.py:394
  79.3 5.6 %ffn.1 = bf16[16,640,128]{2,1,0:T(8,128)(2,1)} custom-call(bf16[16,640,128]{2,1,0:T(8,128)(2,1)S(1)} %all_to_all.21.x_ref, bf16[2048,256]{1,0:T(8,128)(2,1)} %bitcast.23, bf16[2048,256]{1,0:T(8,128)(2,1)} %bitcast.24, bf16[256,2048]{1,0:T(8,128)(2,1)} %bitcast.25), custom_call_target="tpu_custom_call" | custom-call | tf_op jit(solution)/shard_map/ffn/pallas_call | solution.py:167
  84.9 0.0 copy-start.5
  84.9 0.0 copy-start.6
  84.9 3.7 %all-to-all-start.2 = ((bf16[16,640,128]{2,1,0:T(8,128)(2,1)}), bf16[16,640,128]{2,1,0:T(8,128)(2,1)S(1)}, u32[]{:S(2)}, u32[]{:S(2)}) async-start(bf16[16,640,128]{2,1,0:T(8,128)(2,1)} %ffn.1), calls=%async_computation.2 | async-start | bytes 5242880 | tf_op jit(solution)/shard_map/all_to_all | solution.py:394
  88.7 1.9 %collective-permute-start.1 = (bf16[128,256]{1,0:T(8,128)(2,1)S(1)}, bf16[128,256]{1,0:T(8,128)(2,1)S(1)}, u32[]{:S(2)}, u32[]{:S(2)}) collective-permute-start(bf16[128,256]{1,0:T(8,128)(2,1)S(1)} %pad_maximum_fusion.3), channel_id=1, source_target_pairs={{48,16},{80,48},{112,80},{144,112},{176,144},{208,176},{240,208},{... | collective-permute-start | bytes 196616 | tf_op jit(solution)/shard_map/ppermute | solution.py:373
  90.7 1.2 collective-permute-start
  91.9 2.0 %collective-permute-done.1 = bf16[128,256]{1,0:T(8,128)(2,1)S(1)} collective-permute-done((bf16[128,256]{1,0:T(8,128)(2,1)S(1)}, bf16[128,256]{1,0:T(8,128)(2,1)S(1)}, u32[]{:S(2)}, u32[]{:S(2)}) %collective-permute-start.1) | collective-permute-done | bytes 65568 | tf_op jit(solution)/shard_map/ppermute | solution.py:373
  93.8 0.6 collective-permute-done
  94.5 3.1 %collective-permute-start.2 = (bf16[2,128,256]{2,1,0:T(8,128)(2,1)S(1)}, bf16[2,128,256]{2,1,0:T(8,128)(2,1)S(1)}, u32[]{:S(2)}, u32[]{:S(2)}) collective-permute-start(bf16[2,128,256]{2,1,0:T(8,128)(2,1)S(1)} %pad_maximum_fusion.2), channel_id=1, source_target_pairs={{384,0},{144,16},{416,32},{176,48},{448,64},{208,80},{480,96},{240... | collective-permute-start | bytes 393224 | tf_op jit(solution)/shard_map/ppermute | solution.py:373
  97.6 6.8 %collective-permute-done.2 = bf16[2,128,256]{2,1,0:T(8,128)(2,1)S(1)} collective-permute-done((bf16[2,128,256]{2,1,0:T(8,128)(2,1)S(1)}, bf16[2,128,256]{2,1,0:T(8,128)(2,1)S(1)}, u32[]{:S(2)}, u32[]{:S(2)}) %collective-permute-start.2) | collective-permute-done | bytes 131104 | tf_op jit(solution)/shard_map/ppermute | solution.py:373
  104.4 5.5 %collective-permute-start.3 = (bf16[4,128,256]{2,1,0:T(8,128)(2,1)S(1)}, bf16[4,128,256]{2,1,0:T(8,128)(2,1)S(1)}, u32[]{:S(2)}, u32[]{:S(2)}) collective-permute-start(bf16[4,128,256]{2,1,0:T(8,128)(2,1)S(1)} %pad_maximum_fusion.1), channel_id=1, source_target_pairs={{448,0},{80,16},{480,32},{112,48},{0,64},{144,80},{32,96},{176,112... | collective-permute-start | bytes 786440 | tf_op jit(solution)/shard_map/ppermute | solution.py:373
  110.0 3.3 %collective-permute-done.3 = bf16[4,128,256]{2,1,0:T(8,128)(2,1)S(1)} collective-permute-done((bf16[4,128,256]{2,1,0:T(8,128)(2,1)S(1)}, bf16[4,128,256]{2,1,0:T(8,128)(2,1)S(1)}, u32[]{:S(2)}, u32[]{:S(2)}) %collective-permute-start.3) | collective-permute-done | bytes 262176 | tf_op jit(solution)/shard_map/ppermute | solution.py:373
  113.3 0.1 pad_maximum_fusion.a_ref
  113.3 0.0 copy-start.2
  113.3 0.0 copy-start.3
  113.3 8.9 %collective-permute-start.4 = (bf16[8,128,256]{2,1,0:T(8,128)(2,1)S(1)}, bf16[8,128,256]{2,1,0:T(8,128)(2,1)}, u32[]{:S(2)}, u32[]{:S(2)}) collective-permute-start(bf16[8,128,256]{2,1,0:T(8,128)(2,1)S(1)} %pad_maximum_fusion.a_ref), channel_id=1, source_target_pairs={{480,0},{48,16},{0,32},{80,48},{32,64},{112,80},{64,96},{144,112},... | collective-permute-start | bytes 1572872 | tf_op jit(solution)/shard_map/ppermute | solution.py:373
  122.3 0.4 all-to-all-done.2.in_ref
  122.7 1.2 reduce_terms.1
  123.9 11.9 %all-to-all-start.3 = ((bf16[32,24,128]{2,1,0:T(8,128)(2,1)}), bf16[32,24,128]{2,1,0:T(8,128)(2,1)S(1)}, u32[]{:S(2)}, u32[]{:S(2)}) async-start(bf16[32,24,128]{2,1,0:T(8,128)(2,1)} %reduce_terms.1), calls=%async_computation.3 | async-start | bytes 393216 | tf_op jit(solution)/shard_map/all_to_all | solution.py:394
  135.8 2.1 %collective-permute-start.5 = (bf16[8,128,256]{2,1,0:T(8,128)(2,1)S(1)}, bf16[8,128,256]{2,1,0:T(8,128)(2,1)S(1)}, u32[]{:S(2)}, u32[]{:S(2)}) collective-permute-start(bf16[8,128,256]{2,1,0:T(8,128)(2,1)S(1)} %pad_maximum_fusion.a_ref), channel_id=1, source_target_pairs={{16,0},{0,16},{48,32},{32,48},{80,64},{64,80},{112,96},{96,112},{1... | collective-permute-start | bytes 1572872 | tf_op jit(solution)/shard_map/ppermute | solution.py:373
  138.0 0.0 collective-permute-done.4.b_ref
  138.0 2.2 %collective-permute-start.6 = (bf16[8,128,256]{2,1,0:T(8,128)(2,1)}, bf16[8,128,256]{2,1,0:T(8,128)(2,1)S(1)}, u32[]{:S(2)}, u32[]{:S(2)}) collective-permute-start(bf16[8,128,256]{2,1,0:T(8,128)(2,1)} %collective-permute-done.4.b_ref), channel_id=1, source_target_pairs={{16,0},{0,16},{48,32},{32,48},{80,64},{64,80},{112,96},{96,112},{1... | collective-permute-start | bytes 1572872 | tf_op jit(solution)/shard_map/ppermute | solution.py:373
  140.8 0.0 collective-permute-done.5.c_ref
  140.8 1.2 collective-permute-done.6.d_ref
  142.0 0.0 copy-done.4
  142.0 1.0 copy-done
  143.0 3.6 %attend.1 = (bf16[32,2048]{1,0:T(8,128)(2,1)S(1)}, bf16[32,2048]{1,0:T(8,128)(2,1)S(1)}, bf16[32,2048]{1,0:T(8,128)(2,1)S(1)}, bf16[32,2048]{1,0:T(8,128)(2,1)S(1)}) custom-call(s32[1]{0:T(128)} %bitcast.1.z_ref, s32[1]{0:T(128)} %bitcast.2.core_ref, s32[1]{0:T(128)} %bitcast.3.x_ref, f32[1]{0:T(128)S(6)} %copy.15.lam_ref, bf16[128,128]{1,0:T(8,128)(2,1)S(1)} %bitcast.18, ...), custom_call_target="tpu_custom_call" | custom-call | tf_op jit(solution)/shard_map/attend/pallas_call | solution.py:352
  146.6 1.9 %collective-permute-start.7 = (bf16[32,2048]{1,0:T(8,128)(2,1)S(1)}, bf16[32,2048]{1,0:T(8,128)(2,1)S(1)}, u32[]{:S(2)}, u32[]{:S(2)}) collective-permute-start(bf16[32,2048]{1,0:T(8,128)(2,1)S(1)} %get-tuple-element.13), channel_id=1, source_target_pairs={{0,1},{1,2},{2,3},{3,0},{4,5},{5,6},{6,7},{7,4},{8,9},{9,10},{10,1... | collective-permute-start | bytes 393224 | tf_op jit(solution)/shard_map/ppermute | solution.py:389
  148.5 3.6 %collective-permute-start.8 = (bf16[32,2048]{1,0:T(8,128)(2,1)S(1)}, bf16[32,2048]{1,0:T(8,128)(2,1)S(1)}, u32[]{:S(2)}, u32[]{:S(2)}) collective-permute-start(bf16[32,2048]{1,0:T(8,128)(2,1)S(1)} %get-tuple-element.14), channel_id=1, source_target_pairs={{0,2},{1,3},{2,0},{3,1},{4,6},{5,7},{6,4},{7,5},{8,10},{9,11},{10,... | collective-permute-start | bytes 393224 | tf_op jit(solution)/shard_map/ppermute | solution.py:389
  152.1 2.9 %collective-permute-start.9 = (bf16[32,2048]{1,0:T(8,128)(2,1)S(1)}, bf16[32,2048]{1,0:T(8,128)(2,1)S(1)}, u32[]{:S(2)}, u32[]{:S(2)}) collective-permute-start(bf16[32,2048]{1,0:T(8,128)(2,1)S(1)} %get-tuple-element.15), channel_id=1, source_target_pairs={{0,3},{1,0},{2,1},{3,2},{4,7},{5,4},{6,5},{7,6},{8,11},{9,8},{10,9... | collective-permute-start | bytes 393224 | tf_op jit(solution)/shard_map/ppermute | solution.py:389
  155.0 0.0 collective-permute-done.7.refs_1_
  155.0 1.7 collective-permute-done.8.refs_2_
  156.8 2.9 %collective-permute-done.9.refs_3_ = bf16[32,2048]{1,0:T(8,128)(2,1)S(1)} collective-permute-done((bf16[32,2048]{1,0:T(8,128)(2,1)S(1)}, bf16[32,2048]{1,0:T(8,128)(2,1)S(1)}, u32[]{:S(2)}, u32[]{:S(2)}) %collective-permute-start.9) | collective-permute-done | bytes 131104 | tf_op jit(solution)/shard_map/ppermute | solution.py:389
  159.6 0.1 sum_first.1
  159.7 2.1 %collective-permute-start.10 = (bf16[8,2048]{1,0:T(8,128)(2,1)S(1)}, bf16[8,2048]{1,0:T(8,128)(2,1)S(1)}, u32[]{:S(2)}, u32[]{:S(2)}) collective-permute-start(bf16[8,2048]{1,0:T(8,128)(2,1)S(1)} %get-tuple-element.17), channel_id=1, source_target_pairs={{0,4},{4,8},{8,12},{12,0},{1,5},{5,9},{9,13},{13,1},{2,6},{6,10},{... | collective-permute-start | bytes 98312 | tf_op jit(solution)/shard_map/ppermute | solution.py:389
  161.9 4.4 %collective-permute-start.11 = (bf16[8,2048]{1,0:T(8,128)(2,1)S(1)}, bf16[8,2048]{1,0:T(8,128)(2,1)S(1)}, u32[]{:S(2)}, u32[]{:S(2)}) collective-permute-start(bf16[8,2048]{1,0:T(8,128)(2,1)S(1)} %get-tuple-element.18), channel_id=1, source_target_pairs={{0,8},{4,12},{8,0},{12,4},{1,9},{5,13},{9,1},{13,5},{2,10},{6,14},... | collective-permute-start | bytes 98312 | tf_op jit(solution)/shard_map/ppermute | solution.py:389
  166.3 2.4 %collective-permute-start.12 = (bf16[8,2048]{1,0:T(8,128)(2,1)S(1)}, bf16[8,2048]{1,0:T(8,128)(2,1)S(1)}, u32[]{:S(2)}, u32[]{:S(2)}) collective-permute-start(bf16[8,2048]{1,0:T(8,128)(2,1)S(1)} %get-tuple-element.19), channel_id=1, source_target_pairs={{0,12},{4,0},{8,4},{12,8},{1,13},{5,1},{9,5},{13,9},{2,14},{6,2},{... | collective-permute-start | bytes 98312 | tf_op jit(solution)/shard_map/ppermute | solution.py:389
  168.7 0.3 weigh.1
  169.0 0.0 collective-permute-done.10.refs_1_
  169.0 0.0 collective-permute-done.11.refs_2_
  169.0 1.9 %collective-permute-done.12.refs_3_ = bf16[8,2048]{1,0:T(8,128)(2,1)S(1)} collective-permute-done((bf16[8,2048]{1,0:T(8,128)(2,1)S(1)}, bf16[8,2048]{1,0:T(8,128)(2,1)S(1)}, u32[]{:S(2)}, u32[]{:S(2)}) %collective-permute-start.12) | collective-permute-done | bytes 32800 | tf_op jit(solution)/shard_map/ppermute | solution.py:389
  171.0 0.6 sum_last.1
  171.6 0.0 all-to-all-done.3.back_ref
  171.6 0.9 combine.1
  (12 shorter events, 0.1 us)
Async XLA Ops:
  84.9 3.8 %copy-start.5 = (bf16[128,1,128]{2,0,1:T(8,128)(2,1)S(1)}, bf16[128,1,128]{2,0,1:T(8,128)(2,1)}, u32[]{:S(2)}) copy-start(bf16[128,1,128]{2,0,1:T(8,128)(2,1)} %param.15) | copy-start | bytes 98308
  84.9 3.8 %copy-start.6 = (bf16[128,1,128]{2,0,1:T(8,128)(2,1)S(1)}, bf16[128,1,128]{2,0,1:T(8,128)(2,1)}, u32[]{:S(2)}) copy-start(bf16[128,1,128]{2,0,1:T(8,128)(2,1)} %param.14) | copy-start | bytes 98308
  84.9 37.8 %all-to-all-start.2 = ((bf16[16,640,128]{2,1,0:T(8,128)(2,1)}), bf16[16,640,128]{2,1,0:T(8,128)(2,1)S(1)}, u32[]{:S(2)}, u32[]{:S(2)}) async-start(bf16[16,640,128]{2,1,0:T(8,128)(2,1)} %ffn.1), calls=%async_computation.2 | async-start | bytes 5242880 | tf_op jit(solution)/shard_map/all_to_all | solution.py:394
  88.7 5.1 %collective-permute-start.1 = (bf16[128,256]{1,0:T(8,128)(2,1)S(1)}, bf16[128,256]{1,0:T(8,128)(2,1)S(1)}, u32[]{:S(2)}, u32[]{:S(2)}) collective-permute-start(bf16[128,256]{1,0:T(8,128)(2,1)S(1)} %pad_maximum_fusion.3), channel_id=1, source_target_pairs={{48,16},{80,48},{112,80},{144,112},{176,144},{208,176},{240,208},{... | collective-permute-start | bytes 196616 | tf_op jit(solution)/shard_map/ppermute | solution.py:373
  90.7 3.8 %collective-permute-start = (bf16[128,256]{1,0:T(8,128)(2,1)S(1)}, bf16[128,256]{1,0:T(8,128)(2,1)S(1)}, u32[]{:S(2)}, u32[]{:S(2)}) collective-permute-start(bf16[128,256]{1,0:T(8,128)(2,1)S(1)} %pad_maximum_fusion.3), channel_id=1, source_target_pairs={{16,0},{32,16},{48,32},{64,48},{80,64},{96,80},{112,96},{128,112},... | collective-permute-start | bytes 196616 | tf_op jit(solution)/shard_map/ppermute | solution.py:373
  91.8 50.1 %copy-start.1 = (bf16[128,1,128]{2,0,1:T(8,128)(2,1)S(1)}, bf16[128,1,128]{2,0,1:T(8,128)(2,1)}, u32[]{:S(2)}) copy-start(bf16[128,1,128]{2,0,1:T(8,128)(2,1)} %param.13) | copy-start | bytes 98308
  91.8 50.1 %copy-start.4 = (f32[128]{0:T(128)S(1)}, f32[128]{0:T(128)}, u32[]{:S(2)}) copy-start(f32[128]{0:T(128)} %param.17) | copy-start | bytes 1540
  94.5 9.9 %collective-permute-start.2 = (bf16[2,128,256]{2,1,0:T(8,128)(2,1)S(1)}, bf16[2,128,256]{2,1,0:T(8,128)(2,1)S(1)}, u32[]{:S(2)}, u32[]{:S(2)}) collective-permute-start(bf16[2,128,256]{2,1,0:T(8,128)(2,1)S(1)} %pad_maximum_fusion.2), channel_id=1, source_target_pairs={{384,0},{144,16},{416,32},{176,48},{448,64},{208,80},{480,96},{240... | collective-permute-start | bytes 393224 | tf_op jit(solution)/shard_map/ppermute | solution.py:373
  104.4 8.8 %collective-permute-start.3 = (bf16[4,128,256]{2,1,0:T(8,128)(2,1)S(1)}, bf16[4,128,256]{2,1,0:T(8,128)(2,1)S(1)}, u32[]{:S(2)}, u32[]{:S(2)}) collective-permute-start(bf16[4,128,256]{2,1,0:T(8,128)(2,1)S(1)} %pad_maximum_fusion.1), channel_id=1, source_target_pairs={{448,0},{80,16},{480,32},{112,48},{0,64},{144,80},{32,96},{176,112... | collective-permute-start | bytes 786440 | tf_op jit(solution)/shard_map/ppermute | solution.py:373
  113.3 55.4 %copy-start.2 = (s32[128,4]{0,1:T(4,128)S(1)}, s32[128,4]{0,1:T(4,128)}, u32[]{:S(2)}) copy-start(s32[128,4]{0,1:T(4,128)} %param.21) | copy-start | bytes 6148
  113.3 55.4 %copy-start.3 = (f32[128,4]{0,1:T(4,128)S(1)}, f32[128,4]{0,1:T(4,128)}, u32[]{:S(2)}) copy-start(f32[128,4]{0,1:T(4,128)} %param.22) | copy-start | bytes 6148
  113.3 24.6 %collective-permute-start.4 = (bf16[8,128,256]{2,1,0:T(8,128)(2,1)S(1)}, bf16[8,128,256]{2,1,0:T(8,128)(2,1)}, u32[]{:S(2)}, u32[]{:S(2)}) collective-permute-start(bf16[8,128,256]{2,1,0:T(8,128)(2,1)S(1)} %pad_maximum_fusion.a_ref), channel_id=1, source_target_pairs={{480,0},{48,16},{0,32},{80,48},{32,64},{112,80},{64,96},{144,112},... | collective-permute-start | bytes 1572872 | tf_op jit(solution)/shard_map/ppermute | solution.py:373
  123.9 47.7 %all-to-all-start.3 = ((bf16[32,24,128]{2,1,0:T(8,128)(2,1)}), bf16[32,24,128]{2,1,0:T(8,128)(2,1)S(1)}, u32[]{:S(2)}, u32[]{:S(2)}) async-start(bf16[32,24,128]{2,1,0:T(8,128)(2,1)} %reduce_terms.1), calls=%async_computation.3 | async-start | bytes 393216 | tf_op jit(solution)/shard_map/all_to_all | solution.py:394
  135.8 5.0 %collective-permute-start.5 = (bf16[8,128,256]{2,1,0:T(8,128)(2,1)S(1)}, bf16[8,128,256]{2,1,0:T(8,128)(2,1)S(1)}, u32[]{:S(2)}, u32[]{:S(2)}) collective-permute-start(bf16[8,128,256]{2,1,0:T(8,128)(2,1)S(1)} %pad_maximum_fusion.a_ref), channel_id=1, source_target_pairs={{16,0},{0,16},{48,32},{32,48},{80,64},{64,80},{112,96},{96,112},{1... | collective-permute-start | bytes 1572872 | tf_op jit(solution)/shard_map/ppermute | solution.py:373
  138.0 4.0 %collective-permute-start.6 = (bf16[8,128,256]{2,1,0:T(8,128)(2,1)}, bf16[8,128,256]{2,1,0:T(8,128)(2,1)S(1)}, u32[]{:S(2)}, u32[]{:S(2)}) collective-permute-start(bf16[8,128,256]{2,1,0:T(8,128)(2,1)} %collective-permute-done.4.b_ref), channel_id=1, source_target_pairs={{16,0},{0,16},{48,32},{32,48},{80,64},{64,80},{112,96},{96,112},{1... | collective-permute-start | bytes 1572872 | tf_op jit(solution)/shard_map/ppermute | solution.py:373
  142.0 1.0 copy-start
  146.6 8.4 %collective-permute-start.7 = (bf16[32,2048]{1,0:T(8,128)(2,1)S(1)}, bf16[32,2048]{1,0:T(8,128)(2,1)S(1)}, u32[]{:S(2)}, u32[]{:S(2)}) collective-permute-start(bf16[32,2048]{1,0:T(8,128)(2,1)S(1)} %get-tuple-element.13), channel_id=1, source_target_pairs={{0,1},{1,2},{2,3},{3,0},{4,5},{5,6},{6,7},{7,4},{8,9},{9,10},{10,1... | collective-permute-start | bytes 393224 | tf_op jit(solution)/shard_map/ppermute | solution.py:389
  148.5 8.2 %collective-permute-start.8 = (bf16[32,2048]{1,0:T(8,128)(2,1)S(1)}, bf16[32,2048]{1,0:T(8,128)(2,1)S(1)}, u32[]{:S(2)}, u32[]{:S(2)}) collective-permute-start(bf16[32,2048]{1,0:T(8,128)(2,1)S(1)} %get-tuple-element.14), channel_id=1, source_target_pairs={{0,2},{1,3},{2,0},{3,1},{4,6},{5,7},{6,4},{7,5},{8,10},{9,11},{10,... | collective-permute-start | bytes 393224 | tf_op jit(solution)/shard_map/ppermute | solution.py:389
  152.1 7.5 %collective-permute-start.9 = (bf16[32,2048]{1,0:T(8,128)(2,1)S(1)}, bf16[32,2048]{1,0:T(8,128)(2,1)S(1)}, u32[]{:S(2)}, u32[]{:S(2)}) collective-permute-start(bf16[32,2048]{1,0:T(8,128)(2,1)S(1)} %get-tuple-element.15), channel_id=1, source_target_pairs={{0,3},{1,0},{2,1},{3,2},{4,7},{5,4},{6,5},{7,6},{8,11},{9,8},{10,9... | collective-permute-start | bytes 393224 | tf_op jit(solution)/shard_map/ppermute | solution.py:389
  159.7 9.3 %collective-permute-start.10 = (bf16[8,2048]{1,0:T(8,128)(2,1)S(1)}, bf16[8,2048]{1,0:T(8,128)(2,1)S(1)}, u32[]{:S(2)}, u32[]{:S(2)}) collective-permute-start(bf16[8,2048]{1,0:T(8,128)(2,1)S(1)} %get-tuple-element.17), channel_id=1, source_target_pairs={{0,4},{4,8},{8,12},{12,0},{1,5},{5,9},{9,13},{13,1},{2,6},{6,10},{... | collective-permute-start | bytes 98312 | tf_op jit(solution)/shard_map/ppermute | solution.py:389
  161.9 7.2 %collective-permute-start.11 = (bf16[8,2048]{1,0:T(8,128)(2,1)S(1)}, bf16[8,2048]{1,0:T(8,128)(2,1)S(1)}, u32[]{:S(2)}, u32[]{:S(2)}) collective-permute-start(bf16[8,2048]{1,0:T(8,128)(2,1)S(1)} %get-tuple-element.18), channel_id=1, source_target_pairs={{0,8},{4,12},{8,0},{12,4},{1,9},{5,13},{9,1},{13,5},{2,10},{6,14},... | collective-permute-start | bytes 98312 | tf_op jit(solution)/shard_map/ppermute | solution.py:389
  166.3 4.7 %collective-permute-start.12 = (bf16[8,2048]{1,0:T(8,128)(2,1)S(1)}, bf16[8,2048]{1,0:T(8,128)(2,1)S(1)}, u32[]{:S(2)}, u32[]{:S(2)}) collective-permute-start(bf16[8,2048]{1,0:T(8,128)(2,1)S(1)} %get-tuple-element.19), channel_id=1, source_target_pairs={{0,12},{4,0},{8,4},{12,8},{1,13},{5,1},{9,5},{13,9},{2,14},{6,2},{... | collective-permute-start | bytes 98312 | tf_op jit(solution)/shard_map/ppermute | solution.py:389

commit v4 on v2

--- a/solution.py
+++ b/solution.py
@@ -32,6 +32,10 @@
 
 def in_vmem(array):
     return pltpu.with_memory_space_constraint(array, pltpu.VMEM)
+
+
+def in_hbm(array):
+    return pltpu.with_memory_space_constraint(array, pltpu.HBM)
 
 
 def params(mib):
@@ -90,7 +94,7 @@
         ),
         compiler_params=params(8),
         name="dispatch",
-    )(at, token_rows, token_rows, gain, ids)
+    )(at, *(in_hbm(a) for a in (token_rows, token_rows, gain, ids)))
 
 
 COMPACT_STEPS = 4
@@ -168,7 +172,7 @@
         name="ffn",
     )(
         in_vmem(x),
-        *(pltpu.with_memory_space_constraint(w, pltpu.HBM) for w in (wg, wu, wd)),
+        *(in_hbm(w) for w in (wg, wu, wd)),
         in_vmem(proj),
     )
 
@@ -309,7 +313,7 @@
         scratch_shapes=[pltpu.VMEM((Z, 2 * TOK, 2 * TOK), F32)],
         compiler_params=params(16),
         name="attend",
-    )(z_at, core_at, lam, q, *blocks, gain, w)
+    )(z_at, core_at, lam, q, *(in_hbm(b) for b in blocks), gain, in_hbm(w))
 
 
 def moved(array, source):

time: 181 us -> 178 us (0.983)
  local copies, waits for them, and re-layouts: 5.31 us -> 0.03 us
    unnamed x24 -> x14, local copies, waits for them, and re-layouts: 5.31 us -> 0.03 us
  transfers between devices with their start and end apart: 9 -> 9, of which waited for: 7 -> 7; matrix products, arithmetic and copies ran while one was open for 0% -> 0% of each run, Pallas kernels for 2% -> 3%
where the time goes in v4:
time: 178 us; the launch traced here: 177 us
  blocking collectives  80.6 us (45%)
  waiting for transfers between devices  43.3 us (24%)
  starting transfers between devices  36.5 us (21%)
  Pallas kernels  14.9 us (8%)
    all_to_all x2, blocking collectives, exchanged(): return lax.all_to_all(array, axes, split_axis=0, concat_axis=0, tiled=True)  80.6 us
    ppermute x7, waiting for transfers between devices, moved(): return lax.ppermute(array, EP, pairs)  24.9 us
    ppermute x7, starting transfers between devices, moved(): return lax.ppermute(array, EP, pairs)  22.4 us
    all_to_all x2, waiting for transfers between devices, exchanged(): return lax.all_to_all(array, axes, split_axis=0, concat_axis=0, tiled=True)  18.4 us
    all_to_all x2, starting transfers between devices, exchanged(): return lax.all_to_all(array, axes, split_axis=0, concat_axis=0, tiled=True)  14.1 us
    pallas_call x1, Pallas kernels, ffn(): pl.pallas_call(ffn_kernel, out_shape=pltpu.VMEM((N_TP, OUT_ROWS, WIDE), B...  4.53 us
    pallas_call x1, Pallas kernels, attend(): pl.pallas_call(attend_kernel, out_shape=pltpu.VMEM((N_TP, TOK, WIDE), BF1...  4.11 us
  transfers between devices with their start and end apart: 9, of which 7 were waited for; matrix products, arithmetic and copies ran while one was open for 0% of the time, Pallas kernels for 3%

profile of v4, /device:TPU:1, one launch (start us, length us, event | category | flops | bytes accessed | tf_op | source)
XLA Modules:
  0.0 177.0 jit_solution(13458720713158083633)
XLA Ops:
  0.6 1.5 dispatch.1
  2.2 35.3 %all_to_all.20.in_ref = bf16[32,24,128]{2,1,0:T(8,128)(2,1)S(1)} all-to-all(bf16[32,24,128]{2,1,0:T(8,128)(2,1)S(1)} %dispatch.1), channel_id=1, replica_groups=mesh['z'=16,'core'=2,'y'=4,'x'=4] {'z','core'}, dimensions={0} | all-to-all | bytes 393216 | tf_op jit(solution)/shard_map/all_to_all | solution.py:338
  37.5 2.4 %compact.1 = bf16[16,640,128]{2,1,0:T(8,128)(2,1)} custom-call(bf16[32,24,128]{2,1,0:T(8,128)(2,1)S(1)} %all_to_all.20.in_ref), custom_call_target="tpu_custom_call" | custom-call | tf_op jit(solution)/shard_map/compact/pallas_call | solution.py:116
  39.8 0.0 copy-start.5
  39.9 0.0 copy-start.6
  39.9 0.0 copy-start
  39.9 0.0 copy-start.3
  39.9 6.9 %all-to-all-start.1 = ((bf16[16,640,128]{2,1,0:T(8,128)(2,1)}), bf16[16,640,128]{2,1,0:T(8,128)(2,1)S(1)}, u32[]{:S(2)}, u32[]{:S(2)}) async-start(bf16[16,640,128]{2,1,0:T(8,128)(2,1)} %compact.1), calls=%async_computation.1 | async-start | bytes 5242880 | tf_op jit(solution)/shard_map/all_to_all | solution.py:338
  46.8 0.0 copy-done.5
  46.8 0.0 copy-done.6
  46.8 1.9 %collective-permute-start.1 = (bf16[128,256]{1,0:T(8,128)(2,1)S(1)}, bf16[128,256]{1,0:T(8,128)(2,1)S(1)}, u32[]{:S(2)}, u32[]{:S(2)}) collective-permute-start(bf16[128,256]{1,0:T(8,128)(2,1)S(1)} %pad_maximum_fusion.3), channel_id=1, source_target_pairs={{48,16},{80,48},{112,80},{144,112},{176,144},{208,176},{240,208},{... | collective-permute-start | bytes 196616 | tf_op jit(solution)/shard_map/ppermute | solution.py:326
  48.7 0.5 collective-permute-start
  49.2 2.7 %collective-permute-done.1 = bf16[128,256]{1,0:T(8,128)(2,1)S(1)} collective-permute-done((bf16[128,256]{1,0:T(8,128)(2,1)S(1)}, bf16[128,256]{1,0:T(8,128)(2,1)S(1)}, u32[]{:S(2)}, u32[]{:S(2)}) %collective-permute-start.1) | collective-permute-done | bytes 65568 | tf_op jit(solution)/shard_map/ppermute | solution.py:326
  51.9 0.6 collective-permute-done
  52.5 3.1 %collective-permute-start.2 = (bf16[2,128,256]{2,1,0:T(8,128)(2,1)S(1)}, bf16[2,128,256]{2,1,0:T(8,128)(2,1)S(1)}, u32[]{:S(2)}, u32[]{:S(2)}) collective-permute-start(bf16[2,128,256]{2,1,0:T(8,128)(2,1)S(1)} %pad_maximum_fusion.2), channel_id=1, source_target_pairs={{384,0},{144,16},{416,32},{176,48},{448,64},{208,80},{480,96},{240... | collective-permute-start | bytes 393224 | tf_op jit(solution)/shard_map/ppermute | solution.py:326
  55.6 9.8 %collective-permute-done.2 = bf16[2,128,256]{2,1,0:T(8,128)(2,1)S(1)} collective-permute-done((bf16[2,128,256]{2,1,0:T(8,128)(2,1)S(1)}, bf16[2,128,256]{2,1,0:T(8,128)(2,1)S(1)}, u32[]{:S(2)}, u32[]{:S(2)}) %collective-permute-start.2) | collective-permute-done | bytes 131104 | tf_op jit(solution)/shard_map/ppermute | solution.py:326
  65.4 1.9 %collective-permute-start.3 = (bf16[4,128,256]{2,1,0:T(8,128)(2,1)S(1)}, bf16[4,128,256]{2,1,0:T(8,128)(2,1)S(1)}, u32[]{:S(2)}, u32[]{:S(2)}) collective-permute-start(bf16[4,128,256]{2,1,0:T(8,128)(2,1)S(1)} %pad_maximum_fusion.1), channel_id=1, source_target_pairs={{448,0},{80,16},{480,32},{112,48},{0,64},{144,80},{32,96},{176,112... | collective-permute-start | bytes 786440 | tf_op jit(solution)/shard_map/ppermute | solution.py:326
  67.3 6.5 %collective-permute-done.3 = bf16[4,128,256]{2,1,0:T(8,128)(2,1)S(1)} collective-permute-done((bf16[4,128,256]{2,1,0:T(8,128)(2,1)S(1)}, bf16[4,128,256]{2,1,0:T(8,128)(2,1)S(1)}, u32[]{:S(2)}, u32[]{:S(2)}) %collective-permute-start.3) | collective-permute-done | bytes 262176 | tf_op jit(solution)/shard_map/ppermute | solution.py:326
  73.8 0.1 pad_maximum_fusion.a_ref
  73.9 0.0 copy-start.4
  73.9 6.8 %collective-permute-start.4 = (bf16[8,128,256]{2,1,0:T(8,128)(2,1)S(1)}, bf16[8,128,256]{2,1,0:T(8,128)(2,1)}, u32[]{:S(2)}, u32[]{:S(2)}) collective-permute-start(bf16[8,128,256]{2,1,0:T(8,128)(2,1)S(1)} %pad_maximum_fusion.a_ref), channel_id=1, source_target_pairs={{480,0},{48,16},{0,32},{80,48},{32,64},{112,80},{64,96},{144,112},... | collective-permute-start | bytes 1572872 | tf_op jit(solution)/shard_map/ppermute | solution.py:326
  80.7 1.9 %collective-permute-start.5 = (bf16[8,128,256]{2,1,0:T(8,128)(2,1)S(1)}, bf16[8,128,256]{2,1,0:T(8,128)(2,1)}, u32[]{:S(2)}, u32[]{:S(2)}) collective-permute-start(bf16[8,128,256]{2,1,0:T(8,128)(2,1)S(1)} %pad_maximum_fusion.a_ref), channel_id=1, source_target_pairs={{16,0},{0,16},{48,32},{32,48},{80,64},{64,80},{112,96},{96,112},{1... | collective-permute-start | bytes 1572872 | tf_op jit(solution)/shard_map/ppermute | solution.py:326
  82.6 4.2 %collective-permute-done.4.b_ref = bf16[8,128,256]{2,1,0:T(8,128)(2,1)} collective-permute-done((bf16[8,128,256]{2,1,0:T(8,128)(2,1)S(1)}, bf16[8,128,256]{2,1,0:T(8,128)(2,1)}, u32[]{:S(2)}, u32[]{:S(2)}) %collective-permute-start.4) | collective-permute-done | bytes 524320 | tf_op jit(solution)/shard_map/ppermute | solution.py:326
  86.8 6.2 %collective-permute-start.6 = (bf16[8,128,256]{2,1,0:T(8,128)(2,1)}, bf16[8,128,256]{2,1,0:T(8,128)(2,1)}, u32[]{:S(2)}, u32[]{:S(2)}) collective-permute-start(bf16[8,128,256]{2,1,0:T(8,128)(2,1)} %collective-permute-done.4.b_ref), channel_id=1, source_target_pairs={{16,0},{0,16},{48,32},{32,48},{80,64},{64,80},{112,96},{96,112},{1... | collective-permute-start | bytes 1572872 | tf_op jit(solution)/shard_map/ppermute | solution.py:326
  93.7 0.0 collective-permute-done.5.c_ref
  93.7 1.2 collective-permute-done.6.d_ref
  94.9 0.0 copy-done.4
  94.9 0.0 copy-done
  94.9 0.0 copy-done.3
  94.9 4.1 %attend.1.proj_ref = bf16[16,128,128]{2,1,0:T(8,128)(2,1)S(1)} custom-call(s32[1]{0:T(128)} %bitcast.6.z_ref, s32[1]{0:T(128)} %bitcast.7.core_ref, f32[1]{0:T(128)S(6)} %copy.15.lam_ref, bf16[128,128]{1,0:T(8,128)(2,1)S(1)} %bitcast.16, bf16[8,128,256]{2,1,0:T(8,128)(2,1)} %copy-done.4, bf16[8,128,256]{2,1,0:T(8,128)(2,1)} %collective-permute-done.4.b_ref, ...), custom_call_target="tpu_custom_call" | custom-call | tf_op jit(solution)/shard_map/attend/pallas_call | solution.py:308
  99.1 0.0 all-to-all-done.1.x_ref
  99.1 4.5 %ffn.1 = bf16[16,768,128]{2,1,0:T(8,128)(2,1)S(1)} custom-call(bf16[16,640,128]{2,1,0:T(8,128)(2,1)S(1)} %all-to-all-done.1.x_ref, bf16[2048,256]{1,0:T(8,128)(2,1)} %bitcast.21, bf16[2048,256]{1,0:T(8,128)(2,1)} %bitcast.22, bf16[256,2048]{1,0:T(8,128)(2,1)} %bitcast.23, bf16[16,128,128]{2,1,0:T(8,128)(2,1)S(1)} %attend.1.proj_ref), custom_call_target="tpu_custom_call" | custom-call | tf_op jit(solution)/shard_map/ffn/pallas_call | solution.py:160
  103.6 45.3 %all_to_all.21.in_ref = bf16[16,768,128]{2,1,0:T(8,128)(2,1)S(1)} all-to-all(bf16[16,768,128]{2,1,0:T(8,128)(2,1)S(1)} %ffn.1), channel_id=1, replica_groups=mesh['z'=16,'core'=2,'y'=4,'x'=4] {'y','x'}, dimensions={0} | all-to-all | bytes 6291456 | tf_op jit(solution)/shard_map/all_to_all | solution.py:338
  148.9 0.0 copy-start.1
  148.9 0.0 copy-start.2
  148.9 1.2 reduce_terms.1
  150.1 7.2 %all-to-all-start.3 = ((bf16[32,24,128]{2,1,0:T(8,128)(2,1)}), bf16[32,24,128]{2,1,0:T(8,128)(2,1)S(1)}, u32[]{:S(2)}, u32[]{:S(2)}) async-start(bf16[32,24,128]{2,1,0:T(8,128)(2,1)} %get-tuple-element.7), calls=%async_computation.3 | async-start | bytes 393216 | tf_op jit(solution)/shard_map/all_to_all | solution.py:338
  157.3 0.0 copy-done.1
  157.3 0.0 copy-done.2
  157.3 0.3 weigh.1
  157.6 18.4 %all-to-all-done.3.back_ref = bf16[32,24,128]{2,1,0:T(8,128)(2,1)S(1)} async-done(((bf16[32,24,128]{2,1,0:T(8,128)(2,1)}), bf16[32,24,128]{2,1,0:T(8,128)(2,1)S(1)}, u32[]{:S(2)}, u32[]{:S(2)}) %all-to-all-start.3) | async-done | bytes 196640 | tf_op jit(solution)/shard_map/all_to_all | solution.py:338
  176.1 0.9 combine.1
  (4 shorter events, 0.1 us)
Async XLA Ops:
  39.8 6.9 %copy-start.5 = (bf16[128,1,128]{2,0,1:T(8,128)(2,1)S(1)}, bf16[128,1,128]{2,0,1:T(8,128)(2,1)}, u32[]{:S(2)}) copy-start(bf16[128,1,128]{2,0,1:T(8,128)(2,1)} %param.15) | copy-start | bytes 98308
  39.9 6.9 %copy-start.6 = (bf16[128,1,128]{2,0,1:T(8,128)(2,1)S(1)}, bf16[128,1,128]{2,0,1:T(8,128)(2,1)}, u32[]{:S(2)}) copy-start(bf16[128,1,128]{2,0,1:T(8,128)(2,1)} %param.14) | copy-start | bytes 98308
  39.9 55.1 %copy-start = (bf16[128,1,128]{2,0,1:T(8,128)(2,1)S(1)}, bf16[128,1,128]{2,0,1:T(8,128)(2,1)}, u32[]{:S(2)}) copy-start(bf16[128,1,128]{2,0,1:T(8,128)(2,1)} %param.13) | copy-start | bytes 98308
  39.9 55.1 %copy-start.3 = (f32[128]{0:T(128)S(1)}, f32[128]{0:T(128)}, u32[]{:S(2)}) copy-start(f32[128]{0:T(128)} %param.17) | copy-start | bytes 1540
  39.9 59.2 %all-to-all-start.1 = ((bf16[16,640,128]{2,1,0:T(8,128)(2,1)}), bf16[16,640,128]{2,1,0:T(8,128)(2,1)S(1)}, u32[]{:S(2)}, u32[]{:S(2)}) async-start(bf16[16,640,128]{2,1,0:T(8,128)(2,1)} %compact.1), calls=%async_computation.1 | async-start | bytes 5242880 | tf_op jit(solution)/shard_map/all_to_all | solution.py:338
  46.8 5.1 %collective-permute-start.1 = (bf16[128,256]{1,0:T(8,128)(2,1)S(1)}, bf16[128,256]{1,0:T(8,128)(2,1)S(1)}, u32[]{:S(2)}, u32[]{:S(2)}) collective-permute-start(bf16[128,256]{1,0:T(8,128)(2,1)S(1)} %pad_maximum_fusion.3), channel_id=1, source_target_pairs={{48,16},{80,48},{112,80},{144,112},{176,144},{208,176},{240,208},{... | collective-permute-start | bytes 196616 | tf_op jit(solution)/shard_map/ppermute | solution.py:326
  48.7 3.8 %collective-permute-start = (bf16[128,256]{1,0:T(8,128)(2,1)S(1)}, bf16[128,256]{1,0:T(8,128)(2,1)S(1)}, u32[]{:S(2)}, u32[]{:S(2)}) collective-permute-start(bf16[128,256]{1,0:T(8,128)(2,1)S(1)} %pad_maximum_fusion.3), channel_id=1, source_target_pairs={{16,0},{32,16},{48,32},{64,48},{80,64},{96,80},{112,96},{128,112},... | collective-permute-start | bytes 196616 | tf_op jit(solution)/shard_map/ppermute | solution.py:326
  52.5 12.8 %collective-permute-start.2 = (bf16[2,128,256]{2,1,0:T(8,128)(2,1)S(1)}, bf16[2,128,256]{2,1,0:T(8,128)(2,1)S(1)}, u32[]{:S(2)}, u32[]{:S(2)}) collective-permute-start(bf16[2,128,256]{2,1,0:T(8,128)(2,1)S(1)} %pad_maximum_fusion.2), channel_id=1, source_target_pairs={{384,0},{144,16},{416,32},{176,48},{448,64},{208,80},{480,96},{240... | collective-permute-start | bytes 393224 | tf_op jit(solution)/shard_map/ppermute | solution.py:326
  65.4 8.4 %collective-permute-start.3 = (bf16[4,128,256]{2,1,0:T(8,128)(2,1)S(1)}, bf16[4,128,256]{2,1,0:T(8,128)(2,1)S(1)}, u32[]{:S(2)}, u32[]{:S(2)}) collective-permute-start(bf16[4,128,256]{2,1,0:T(8,128)(2,1)S(1)} %pad_maximum_fusion.1), channel_id=1, source_target_pairs={{448,0},{80,16},{480,32},{112,48},{0,64},{144,80},{32,96},{176,112... | collective-permute-start | bytes 786440 | tf_op jit(solution)/shard_map/ppermute | solution.py:326
  73.9 21.0 %copy-start.4 = (bf16[8,128,256]{2,1,0:T(8,128)(2,1)}, bf16[8,128,256]{2,1,0:T(8,128)(2,1)S(1)}, u32[]{:S(2)}) copy-start(bf16[8,128,256]{2,1,0:T(8,128)(2,1)S(1)} %pad_maximum_fusion.a_ref) | copy-start | bytes 1572868
  73.9 12.9 %collective-permute-start.4 = (bf16[8,128,256]{2,1,0:T(8,128)(2,1)S(1)}, bf16[8,128,256]{2,1,0:T(8,128)(2,1)}, u32[]{:S(2)}, u32[]{:S(2)}) collective-permute-start(bf16[8,128,256]{2,1,0:T(8,128)(2,1)S(1)} %pad_maximum_fusion.a_ref), channel_id=1, source_target_pairs={{480,0},{48,16},{0,32},{80,48},{32,64},{112,80},{64,96},{144,112},... | collective-permute-start | bytes 1572872 | tf_op jit(solution)/shard_map/ppermute | solution.py:326
  80.7 13.0 %collective-permute-start.5 = (bf16[8,128,256]{2,1,0:T(8,128)(2,1)S(1)}, bf16[8,128,256]{2,1,0:T(8,128)(2,1)}, u32[]{:S(2)}, u32[]{:S(2)}) collective-permute-start(bf16[8,128,256]{2,1,0:T(8,128)(2,1)S(1)} %pad_maximum_fusion.a_ref), channel_id=1, source_target_pairs={{16,0},{0,16},{48,32},{32,48},{80,64},{64,80},{112,96},{96,112},{1... | collective-permute-start | bytes 1572872 | tf_op jit(solution)/shard_map/ppermute | solution.py:326
  86.8 8.1 %collective-permute-start.6 = (bf16[8,128,256]{2,1,0:T(8,128)(2,1)}, bf16[8,128,256]{2,1,0:T(8,128)(2,1)}, u32[]{:S(2)}, u32[]{:S(2)}) collective-permute-start(bf16[8,128,256]{2,1,0:T(8,128)(2,1)} %collective-permute-done.4.b_ref), channel_id=1, source_target_pairs={{16,0},{0,16},{48,32},{32,48},{80,64},{64,80},{112,96},{96,112},{1... | collective-permute-start | bytes 1572872 | tf_op jit(solution)/shard_map/ppermute | solution.py:326
  148.9 8.4 %copy-start.1 = (s32[128,4]{0,1:T(4,128)S(1)}, s32[128,4]{0,1:T(4,128)}, u32[]{:S(2)}) copy-start(s32[128,4]{0,1:T(4,128)} %param.21) | copy-start | bytes 6148
  148.9 8.4 %copy-start.2 = (f32[128,4]{0,1:T(4,128)S(1)}, f32[128,4]{0,1:T(4,128)}, u32[]{:S(2)}) copy-start(f32[128,4]{0,1:T(4,128)} %param.22) | copy-start | bytes 6148
  150.1 26.0 %all-to-all-start.3 = ((bf16[32,24,128]{2,1,0:T(8,128)(2,1)}), bf16[32,24,128]{2,1,0:T(8,128)(2,1)S(1)}, u32[]{:S(2)}, u32[]{:S(2)}) async-start(bf16[32,24,128]{2,1,0:T(8,128)(2,1)} %get-tuple-element.7), calls=%async_computation.3 | async-start | bytes 393216 | tf_op jit(solution)/shard_map/all_to_all | solution.py:338

commit v5 on v4

--- a/solution.py
+++ b/solution.py
@@ -26,7 +26,7 @@
 MODEL = N_TP * WIDE
 OUT_ROWS = ROWS + TOK
 
-STEPS = (0, 4, 2, 6, 1, 5, 3, 7)
+STEPS = (0, 8, 4, 12, 2, 10, 6, 14, 1, 9, 5, 13, 3, 11, 7, 15)
 MIB = 1 << 20
 
 
@@ -97,7 +97,7 @@
     )(at, *(in_hbm(a) for a in (token_rows, token_rows, gain, ids)))
 
 
-COMPACT_STEPS = 4
+COMPACT_STEPS = 2
 COMPACT_SRC = N_EP // COMPACT_STEPS
 
 
@@ -250,49 +250,81 @@
     )(*(in_vmem(a) for a in (back, high, low)))
 
 
-def attend_kernel(
-    z_ref, core_ref, lam_ref, q_ref, a_ref, b_ref, c_ref, d_ref, gain_ref, w_ref, out_ref, score_ref
-):
-    q = q_ref[...]
-    q = (q.astype(F32) * (64**-0.5)).astype(BF16)
+def attend_kernel(z_ref, core_ref, q_ref, swapped_ref, a_ref, b_ref, own_ref, other_ref, score_ref):
     lane = lax.broadcasted_iota(jnp.int32, (TOK, WIDE), 1)
-    zero = jnp.zeros_like(q)
-    both = jnp.concatenate(
-        [jnp.where(lane < 64, q, zero), jnp.where(lane < 64, zero, q)], axis=0
-    )
+    parts = []
+    for ref in (q_ref, swapped_ref):
+        q = (ref[...].astype(F32) * (64**-0.5)).astype(BF16)
+        zero = jnp.zeros_like(q)
+        parts += [jnp.where(lane < 64, q, zero), jnp.where(lane < 64, zero, q)]
+    queries = jnp.concatenate(parts, axis=0)
     row = lax.broadcasted_iota(jnp.int32, (2 * TOK, TOK), 0)
     row = jnp.where(row < TOK, row, row - TOK)
     ahead = lax.broadcasted_iota(jnp.int32, (2 * TOK, TOK), 1) - row
     z, core = z_ref[0], core_ref[0]
-    me = CORE * z + core
-    chips = []
-    for half, refs in ((core, (a_ref, b_ref)), (1 - core, (c_ref, d_ref))):
-        for n, step in enumerate(STEPS):
-            down = CORE * ((z - step) & (Z - 1))
-            up = CORE * ((z + 1 + step) & (Z - 1))
-            first = jnp.where(half == 0, down + 1, up)
-            second = jnp.where(half == 0, down, up + 1)
-            chips.append((refs[n // 4], 2 * (n % 4), (first, second)))
-    top = jnp.full((2 * TOK, TOK), -1e30, F32)
-    for n, (ref, low, blocks) in enumerate(chips):
-        keys = ref[low : low + 2, :, :WIDE].reshape(2 * TOK, WIDE)
+    mine, theirs = CORE * z + core, CORE * z + 1 - core
+    sign = 2 * core - 1
+    blocks = [CORE * ((z + sign * step) & (Z - 1)) + core for step in STEPS]
+    top = jnp.full((4 * TOK, TOK), -1e30, F32)
+    for n in range(0, Z, 2):
+        keys = (a_ref, b_ref)[n // 8][n % 8 : n % 8 + 2, :, :WIDE].reshape(2 * TOK, WIDE)
         scores = lax.dot_general(
-            both, keys, (((1,), (1,)), ((), ())), preferred_element_type=F32
+            queries, keys, (((1,), (1,)), ((), ())), preferred_element_type=F32
         )
         for h in range(2):
-            part = scores[:, h * TOK : (h + 1) * TOK]
-            part = jnp.where(ahead <= (me - blocks[h]) * TOK, part, -1e30)
-            score_ref[n, :, h * TOK : (h + 1) * TOK] = part
+            cols = slice(h * TOK, (h + 1) * TOK)
+            part = jnp.concatenate(
+                [
+                    jnp.where(
+                        ahead <= (who - blocks[n + h]) * TOK,
+                        scores[2 * TOK * i : 2 * TOK * (i + 1), cols],
+                        -1e30,
+                    )
+                    for i, who in enumerate((mine, theirs))
+                ],
+                axis=0,
+            )
+            score_ref[n // 2, :, cols] = part
             top = jnp.maximum(top, part)
     row_max = jnp.max(top, axis=-1, keepdims=True)
-    total = jnp.zeros((2 * TOK, 2 * TOK), F32)
-    value_sum = jnp.zeros((2 * TOK, WIDE), F32)
-    for n, (ref, low, _) in enumerate(chips):
-        terms = jnp.exp(score_ref[n] - row_max)
+    total = jnp.zeros((4 * TOK, 2 * TOK), F32)
+    value_sum = jnp.zeros((4 * TOK, WIDE), F32)
+    for n in range(0, Z, 2):
+        terms = jnp.exp(score_ref[n // 2] - row_max)
         total = total + terms
-        values = ref[low : low + 2, :, WIDE:].reshape(2 * TOK, WIDE)
+        values = (a_ref, b_ref)[n // 8][n % 8 : n % 8 + 2, :, WIDE:].reshape(2 * TOK, WIDE)
         value_sum = value_sum + jnp.dot(terms.astype(BF16), values, preferred_element_type=F32)
-    ratio = value_sum / jnp.sum(total, axis=-1, keepdims=True)
+    total = jnp.sum(total, axis=-1, keepdims=True)
+    wide = lax.broadcasted_iota(jnp.int32, (4 * TOK, WIDE), 1)
+    beside = jnp.where(wide < 64, row_max, total)
+    for i, ref in enumerate((own_ref, other_ref)):
+        rows = slice(2 * TOK * i, 2 * TOK * (i + 1))
+        ref[:, :WIDE] = value_sum[rows]
+        ref[:, WIDE:] = beside[rows]
+
+
+def attend(z_at, core_at, q, swapped, blocks):
+    vmem = pl.BlockSpec(memory_space=pltpu.VMEM)
+    smem = pl.BlockSpec(memory_space=pltpu.SMEM)
+    part = jax.ShapeDtypeStruct((2 * TOK, 2 * WIDE), F32)
+    return pl.pallas_call(
+        attend_kernel,
+        out_shape=(part, part),
+        in_specs=[smem] * 2 + [vmem] * 4,
+        out_specs=(vmem, vmem),
+        scratch_shapes=[pltpu.VMEM((Z // 2, 4 * TOK, 2 * TOK), F32)],
+        compiler_params=params(20),
+        name="attend",
+    )(z_at, core_at, q, swapped, *blocks)
+
+
+def project_kernel(lam_ref, own_ref, other_ref, gain_ref, w_ref, out_ref):
+    tops = [ref[:, WIDE : WIDE + 1] for ref in (own_ref, other_ref)]
+    totals = [ref[:, WIDE + 64 : WIDE + 65] for ref in (own_ref, other_ref)]
+    top = jnp.maximum(*tops)
+    scales = [jnp.exp(t - top) for t in tops]
+    total = totals[0] * scales[0] + totals[1] * scales[1]
+    ratio = (own_ref[:, :WIDE] * scales[0] + other_ref[:, :WIDE] * scales[1]) / total
     attended = ratio[:TOK] - lam_ref[0] * ratio[TOK:]
     mean_sq = jnp.mean(attended * attended, axis=-1, keepdims=True)
     head_rows = (attended * lax.rsqrt(mean_sq + NORM_EPS) * gain_ref[...]).astype(BF16)
@@ -302,18 +334,16 @@
         out_ref[:, 8 * c : 8 * (c + 1), :] = piece
 
 
-def attend(z_at, core_at, lam, q, blocks, gain, w):
-    vmem = pl.BlockSpec(memory_space=pltpu.VMEM)
-    smem = pl.BlockSpec(memory_space=pltpu.SMEM)
-    return pl.pallas_call(
-        attend_kernel,
+def project(lam, own, other, gain, w):
+    vmem = pl.BlockSpec(memory_space=pltpu.VMEM)
+    return pl.pallas_call(
+        project_kernel,
         out_shape=pltpu.VMEM((N_TP, TOK, WIDE), BF16),
-        in_specs=[smem] * 3 + [vmem] * 7,
+        in_specs=[pl.BlockSpec(memory_space=pltpu.SMEM)] + [vmem] * 4,
         out_specs=vmem,
-        scratch_shapes=[pltpu.VMEM((Z, 2 * TOK, 2 * TOK), F32)],
-        compiler_params=params(16),
-        name="attend",
-    )(z_at, core_at, lam, q, *(in_hbm(b) for b in blocks), gain, in_hbm(w))
+        compiler_params=params(8),
+        name="project",
+    )(lam, own, other, gain, w)
 
 
 def moved(array, source):
@@ -338,16 +368,12 @@
     return lax.all_to_all(array, axes, split_axis=0, concat_axis=0, tiled=True)
 
 
-def collect_keys(keys, values, core_at):
-    mine = jnp.concatenate([keys, values], axis=-1)
-    first = moved(mine, lambda z, core: (z + 1, 0) if core else (z, 1))
-    second = moved(mine, lambda z, core: (z + 1, 1) if core else None)
-    pair = jnp.stack([first, jnp.where(core_at == 0, mine, second)])
-    two = jnp.concatenate([pair, along(pair, 4)], axis=0)
-    four = jnp.concatenate([two, along(two, 2)], axis=0)
-    rest = along(four, 1)
-    other = across(four)
-    return four, rest, other, across(rest)
+def collect_keys(keys, values):
+    held = jnp.concatenate([keys, values], axis=-1)[None]
+    held = jnp.concatenate([held, along(held, 8)], axis=0)
+    held = jnp.concatenate([held, along(held, 4)], axis=0)
+    held = jnp.concatenate([held, along(held, 2)], axis=0)
+    return held, along(held, 1)
 
 
 def body(
@@ -371,18 +397,12 @@
     ids = expert_ids.T
     packed = dispatch(tp_at.reshape(1), token_rows, norm_gain.reshape(1, MODEL), ids)
     arrived = exchanged(packed, EP)
-    blocks = collect_keys(
-        key_maps.reshape(TOK, WIDE), value_rows.reshape(TOK, WIDE), core_at
-    )
-    proj = attend(
-        z_at.reshape(1),
-        core_at.reshape(1),
-        head_lambda,
-        query_maps.reshape(TOK, WIDE),
-        blocks,
-        head_gain.reshape(1, WIDE),
-        out_weight,
-    )
+    blocks = collect_keys(key_maps.reshape(TOK, WIDE), value_rows.reshape(TOK, WIDE))
+    queries = query_maps.reshape(TOK, WIDE)
+    swapped = across(queries)
+    own, theirs = attend(z_at.reshape(1), core_at.reshape(1), queries, swapped, blocks)
+    other = across(theirs)
+    proj = project(head_lambda, own, other, head_gain.reshape(1, WIDE), out_weight)
     high, low = weigh(ids, route_weights.T)
     spread = compact(arrived)
     x = exchanged(spread, TP)

time: 178 us -> 188 us (1.056)
  starting transfers between devices: 36.5 us -> 44 us
    ppermute x7 -> x6, starting transfers between devices: 22.4 us -> 29.1 us  [moved(): return lax.ppermute(array, EP, pairs)]
    ppermute x7 -> x6, waiting for transfers between devices: 24.9 us -> 26.6 us  [moved(): return lax.ppermute(array, EP, pairs)]
    pallas_call x1 -> x2, Pallas kernels: 4.11 us -> 4.67 us  [the longest x1 4.04 us: attend(): pl.pallas_call(attend_kernel, out_shape=(part, part), in_specs=[smem] * 2...]
  transfers between devices with their start and end apart: 9 -> 8, of which waited for: 7 -> 7; matrix products, arithmetic and copies ran while one was open for 0% -> 0% of each run, Pallas kernels for 3% -> 3%
where the time goes in v5:
time: 188 us
  blocking collectives  80.9 us (43%)
  waiting for transfers between devices  45.1 us (24%)
  starting transfers between devices  44 us (23%)
  Pallas kernels  14.9 us (8%)
    all_to_all x2, blocking collectives, exchanged(): return lax.all_to_all(array, axes, split_axis=0, concat_axis=0, tiled=True)  80.9 us
    ppermute x6, starting transfers between devices, moved(): return lax.ppermute(array, EP, pairs)  29.1 us
    ppermute x6, waiting for transfers between devices, moved(): return lax.ppermute(array, EP, pairs)  26.6 us
    all_to_all x2, waiting for transfers between devices, exchanged(): return lax.all_to_all(array, axes, split_axis=0, concat_axis=0, tiled=True)  18.4 us
    all_to_all x2, starting transfers between devices, exchanged(): return lax.all_to_all(array, axes, split_axis=0, concat_axis=0, tiled=True)  14.9 us
    pallas_call x1, Pallas kernels, ffn(): pl.pallas_call(ffn_kernel, out_shape=pltpu.VMEM((N_TP, OUT_ROWS, WIDE), B...  4.53 us
    pallas_call x1, Pallas kernels, attend(): pl.pallas_call(attend_kernel, out_shape=(part, part), in_specs=[smem] * 2...  4.04 us
  transfers between devices with their start and end apart: 8, of which 7 were waited for; matrix products, arithmetic and copies ran while one was open for 0% of the time, Pallas kernels for 3%

profile of v5, /device:TPU:1, one launch (start us, length us, event | category | flops | bytes accessed | tf_op | source)
XLA Modules:
  0.0 187.5 jit_solution(11517732398005896839)
XLA Ops:
  0.6 1.5 dispatch.1
  2.2 35.3 %all_to_all.20.in_ref = bf16[32,24,128]{2,1,0:T(8,128)(2,1)S(1)} all-to-all(bf16[32,24,128]{2,1,0:T(8,128)(2,1)S(1)} %dispatch.1), channel_id=1, replica_groups=mesh['z'=16,'core'=2,'y'=4,'x'=4] {'z','core'}, dimensions={0} | all-to-all | bytes 393216 | tf_op jit(solution)/shard_map/all_to_all | solution.py:368
  37.5 1.8 compact.1
  39.3 0.0 copy-start.5
  39.3 0.0 copy-start.6
  39.3 0.0 copy-start.1
  39.3 0.0 copy-start.4
  39.3 6.9 %all-to-all-start.1 = ((bf16[16,640,128]{2,1,0:T(8,128)(2,1)}), bf16[16,640,128]{2,1,0:T(8,128)(2,1)S(1)}, u32[]{:S(2)}, u32[]{:S(2)}) async-start(bf16[16,640,128]{2,1,0:T(8,128)(2,1)} %compact.1), calls=%async_computation.1 | async-start | bytes 5242880 | tf_op jit(solution)/shard_map/all_to_all | solution.py:368
  46.2 0.0 copy-done.5
  46.2 0.0 copy-done.6
  46.2 3.0 %collective-permute-start.1 = (bf16[1,128,256]{2,1,0:T(8,128)(2,1)S(1)}, bf16[1,128,256]{2,1,0:T(8,128)(2,1)S(1)}, u32[]{:S(2)}, u32[]{:S(2)}) collective-permute-start(bf16[1,128,256]{2,1,0:T(8,128)(2,1)S(1)} %maximum_bitcast_fusion), channel_id=1, source_target_pairs={{256,0},{272,16},{288,32},{304,48},{320,64},{336,80},{352,96},{368... | collective-permute-start | bytes 196616 | tf_op jit(solution)/shard_map/ppermute | solution.py:356
  49.3 11.6 %collective-permute-done.1 = bf16[1,128,256]{2,1,0:T(8,128)(2,1)S(1)} collective-permute-done((bf16[1,128,256]{2,1,0:T(8,128)(2,1)S(1)}, bf16[1,128,256]{2,1,0:T(8,128)(2,1)S(1)}, u32[]{:S(2)}, u32[]{:S(2)}) %collective-permute-start.1) | collective-permute-done | bytes 65568 | tf_op jit(solution)/shard_map/ppermute | solution.py:356
  60.8 6.2 %collective-permute-start.2 = (bf16[2,128,256]{2,1,0:T(8,128)(2,1)S(1)}, bf16[2,128,256]{2,1,0:T(8,128)(2,1)S(1)}, u32[]{:S(2)}, u32[]{:S(2)}) collective-permute-start(bf16[2,128,256]{2,1,0:T(8,128)(2,1)S(1)} %pad_maximum_fusion.2), channel_id=1, source_target_pairs={{384,0},{144,16},{416,32},{176,48},{448,64},{208,80},{480,96},{240... | collective-permute-start | bytes 393224 | tf_op jit(solution)/shard_map/ppermute | solution.py:356
  67.1 5.7 %collective-permute-done.2 = bf16[2,128,256]{2,1,0:T(8,128)(2,1)S(1)} collective-permute-done((bf16[2,128,256]{2,1,0:T(8,128)(2,1)S(1)}, bf16[2,128,256]{2,1,0:T(8,128)(2,1)S(1)}, u32[]{:S(2)}, u32[]{:S(2)}) %collective-permute-start.2) | collective-permute-done | bytes 131104 | tf_op jit(solution)/shard_map/ppermute | solution.py:356
  72.8 7.0 %collective-permute-start.3 = (bf16[4,128,256]{2,1,0:T(8,128)(2,1)S(1)}, bf16[4,128,256]{2,1,0:T(8,128)(2,1)S(1)}, u32[]{:S(2)}, u32[]{:S(2)}) collective-permute-start(bf16[4,128,256]{2,1,0:T(8,128)(2,1)S(1)} %pad_maximum_fusion.1), channel_id=1, source_target_pairs={{448,0},{80,16},{480,32},{112,48},{0,64},{144,80},{32,96},{176,112... | collective-permute-start | bytes 786440 | tf_op jit(solution)/shard_map/ppermute | solution.py:356
  79.8 5.7 %collective-permute-done.3 = bf16[4,128,256]{2,1,0:T(8,128)(2,1)S(1)} collective-permute-done((bf16[4,128,256]{2,1,0:T(8,128)(2,1)S(1)}, bf16[4,128,256]{2,1,0:T(8,128)(2,1)S(1)}, u32[]{:S(2)}, u32[]{:S(2)}) %collective-permute-start.3) | collective-permute-done | bytes 262176 | tf_op jit(solution)/shard_map/ppermute | solution.py:356
  85.5 0.1 pad_maximum_fusion.a_ref
  85.5 3.2 %collective-permute-start.4 = (bf16[8,128,256]{2,1,0:T(8,128)(2,1)S(1)}, bf16[8,128,256]{2,1,0:T(8,128)(2,1)}, u32[]{:S(2)}, u32[]{:S(2)}) collective-permute-start(bf16[8,128,256]{2,1,0:T(8,128)(2,1)S(1)} %pad_maximum_fusion.a_ref), channel_id=1, source_target_pairs={{480,0},{48,16},{0,32},{80,48},{32,64},{112,80},{64,96},{144,112},... | collective-permute-start | bytes 1572872 | tf_op jit(solution)/shard_map/ppermute | solution.py:356
  88.7 0.0 copy-done.1
  88.7 3.9 %collective-permute-start = (bf16[128,128]{1,0:T(8,128)(2,1)S(1)}, bf16[128,128]{1,0:T(8,128)(2,1)S(1)}, u32[]{:S(2)}, u32[]{:S(2)}) collective-permute-start(bf16[128,128]{1,0:T(8,128)(2,1)S(1)} %bitcast.15), channel_id=1, source_target_pairs={{16,0},{0,16},{48,32},{32,48},{80,64},{64,80},{112,96},{96,112},{1... | collective-permute-start | bytes 98312 | tf_op jit(solution)/shard_map/ppermute | solution.py:356
  92.6 0.8 collective-permute-done.swapped_ref
  93.5 2.4 %collective-permute-done.4.b_ref = bf16[8,128,256]{2,1,0:T(8,128)(2,1)} collective-permute-done((bf16[8,128,256]{2,1,0:T(8,128)(2,1)S(1)}, bf16[8,128,256]{2,1,0:T(8,128)(2,1)}, u32[]{:S(2)}, u32[]{:S(2)}) %collective-permute-start.4) | collective-permute-done | bytes 524320 | tf_op jit(solution)/shard_map/ppermute | solution.py:356
  95.8 4.0 %attend.1 = (f32[256,256]{1,0:T(8,128)S(1)}, f32[256,256]{1,0:T(8,128)S(1)}) custom-call(s32[1]{0:T(128)} %bitcast.6.z_ref, s32[1]{0:T(128)} %bitcast.7.core_ref, bf16[128,128]{1,0:T(8,128)(2,1)S(1)} %bitcast.16, bf16[128,128]{1,0:T(8,128)(2,1)S(1)} %collective-permute-done.swapped_ref, bf16[8,128,256]{2,1,0:T(8,128)(2,1)S(1)} %pad_maximum_fusion.a_ref, ...), custom_call_target="tpu_custom_call" | custom-call | tf_op jit(solution)/shard_map/attend/pallas_call | solution.py:310
  99.9 5.8 %collective-permute-start.5 = (f32[256,256]{1,0:T(8,128)S(1)}, f32[256,256]{1,0:T(8,128)S(1)}, u32[]{:S(2)}, u32[]{:S(2)}) collective-permute-start(f32[256,256]{1,0:T(8,128)S(1)} %get-tuple-element.9), channel_id=1, source_target_pairs={{16,0},{0,16},{48,32},{32,48},{80,64},{64,80},{112,96},{96,112},{1... | collective-permute-start | bytes 786440 | tf_op jit(solution)/shard_map/ppermute | solution.py:356
  106.3 0.5 collective-permute-done.5.other_ref
  106.8 0.0 copy-done.4
  106.8 0.0 copy-start
  106.8 1.0 copy-done
  107.8 0.6 project.1.proj_ref
  108.5 0.0 all-to-all-done.1.x_ref
  108.5 4.5 %ffn.1 = bf16[16,768,128]{2,1,0:T(8,128)(2,1)S(1)} custom-call(bf16[16,640,128]{2,1,0:T(8,128)(2,1)S(1)} %all-to-all-done.1.x_ref, bf16[2048,256]{1,0:T(8,128)(2,1)} %bitcast.21, bf16[2048,256]{1,0:T(8,128)(2,1)} %bitcast.22, bf16[256,2048]{1,0:T(8,128)(2,1)} %bitcast.23, bf16[16,128,128]{2,1,0:T(8,128)(2,1)S(1)} %project.1.proj_ref), custom_call_target="tpu_custom_call" | custom-call | tf_op jit(solution)/shard_map/ffn/pallas_call | solution.py:160
  113.0 45.6 %all_to_all.21.in_ref = bf16[16,768,128]{2,1,0:T(8,128)(2,1)S(1)} all-to-all(bf16[16,768,128]{2,1,0:T(8,128)(2,1)S(1)} %ffn.1), channel_id=1, replica_groups=mesh['z'=16,'core'=2,'y'=4,'x'=4] {'y','x'}, dimensions={0} | all-to-all | bytes 6291456 | tf_op jit(solution)/shard_map/all_to_all | solution.py:368
  158.6 0.0 copy-start.2
  158.6 0.0 copy-start.3
  158.6 1.2 reduce_terms.1
  159.8 8.0 %all-to-all-start.3 = ((bf16[32,24,128]{2,1,0:T(8,128)(2,1)}), bf16[32,24,128]{2,1,0:T(8,128)(2,1)S(1)}, u32[]{:S(2)}, u32[]{:S(2)}) async-start(bf16[32,24,128]{2,1,0:T(8,128)(2,1)} %get-tuple-element.11), calls=%async_computation.3 | async-start | bytes 393216 | tf_op jit(solution)/shard_map/all_to_all | solution.py:368
  167.9 0.0 copy-done.2
  167.9 0.0 copy-done.3
  167.9 0.3 weigh.1
  168.2 18.4 %all-to-all-done.3.back_ref = bf16[32,24,128]{2,1,0:T(8,128)(2,1)S(1)} async-done(((bf16[32,24,128]{2,1,0:T(8,128)(2,1)}), bf16[32,24,128]{2,1,0:T(8,128)(2,1)S(1)}, u32[]{:S(2)}, u32[]{:S(2)}) %all-to-all-start.3) | async-done | bytes 196640 | tf_op jit(solution)/shard_map/all_to_all | solution.py:368
  186.7 0.9 combine.1
  (3 shorter events, 0.1 us)
Async XLA Ops:
  39.3 6.9 %copy-start.5 = (bf16[128,1,128]{2,0,1:T(8,128)(2,1)S(1)}, bf16[128,1,128]{2,0,1:T(8,128)(2,1)}, u32[]{:S(2)}) copy-start(bf16[128,1,128]{2,0,1:T(8,128)(2,1)} %param.15) | copy-start | bytes 98308
  39.3 6.9 %copy-start.6 = (bf16[128,1,128]{2,0,1:T(8,128)(2,1)S(1)}, bf16[128,1,128]{2,0,1:T(8,128)(2,1)}, u32[]{:S(2)}) copy-start(bf16[128,1,128]{2,0,1:T(8,128)(2,1)} %param.14) | copy-start | bytes 98308
  39.3 49.5 %copy-start.1 = (bf16[128,1,128]{2,0,1:T(8,128)(2,1)S(1)}, bf16[128,1,128]{2,0,1:T(8,128)(2,1)}, u32[]{:S(2)}) copy-start(bf16[128,1,128]{2,0,1:T(8,128)(2,1)} %param.13) | copy-start | bytes 98308
  39.3 67.5 %copy-start.4 = (f32[128]{0:T(128)S(1)}, f32[128]{0:T(128)}, u32[]{:S(2)}) copy-start(f32[128]{0:T(128)} %param.17) | copy-start | bytes 1540
  39.3 69.2 %all-to-all-start.1 = ((bf16[16,640,128]{2,1,0:T(8,128)(2,1)}), bf16[16,640,128]{2,1,0:T(8,128)(2,1)S(1)}, u32[]{:S(2)}, u32[]{:S(2)}) async-start(bf16[16,640,128]{2,1,0:T(8,128)(2,1)} %compact.1), calls=%async_computation.1 | async-start | bytes 5242880 | tf_op jit(solution)/shard_map/all_to_all | solution.py:368
  46.2 14.6 %collective-permute-start.1 = (bf16[1,128,256]{2,1,0:T(8,128)(2,1)S(1)}, bf16[1,128,256]{2,1,0:T(8,128)(2,1)S(1)}, u32[]{:S(2)}, u32[]{:S(2)}) collective-permute-start(bf16[1,128,256]{2,1,0:T(8,128)(2,1)S(1)} %maximum_bitcast_fusion), channel_id=1, source_target_pairs={{256,0},{272,16},{288,32},{304,48},{320,64},{336,80},{352,96},{368... | collective-permute-start | bytes 196616 | tf_op jit(solution)/shard_map/ppermute | solution.py:356
  60.8 12.0 %collective-permute-start.2 = (bf16[2,128,256]{2,1,0:T(8,128)(2,1)S(1)}, bf16[2,128,256]{2,1,0:T(8,128)(2,1)S(1)}, u32[]{:S(2)}, u32[]{:S(2)}) collective-permute-start(bf16[2,128,256]{2,1,0:T(8,128)(2,1)S(1)} %pad_maximum_fusion.2), channel_id=1, source_target_pairs={{384,0},{144,16},{416,32},{176,48},{448,64},{208,80},{480,96},{240... | collective-permute-start | bytes 393224 | tf_op jit(solution)/shard_map/ppermute | solution.py:356
  72.8 12.6 %collective-permute-start.3 = (bf16[4,128,256]{2,1,0:T(8,128)(2,1)S(1)}, bf16[4,128,256]{2,1,0:T(8,128)(2,1)S(1)}, u32[]{:S(2)}, u32[]{:S(2)}) collective-permute-start(bf16[4,128,256]{2,1,0:T(8,128)(2,1)S(1)} %pad_maximum_fusion.1), channel_id=1, source_target_pairs={{448,0},{80,16},{480,32},{112,48},{0,64},{144,80},{32,96},{176,112... | collective-permute-start | bytes 786440 | tf_op jit(solution)/shard_map/ppermute | solution.py:356
  85.5 10.3 %collective-permute-start.4 = (bf16[8,128,256]{2,1,0:T(8,128)(2,1)S(1)}, bf16[8,128,256]{2,1,0:T(8,128)(2,1)}, u32[]{:S(2)}, u32[]{:S(2)}) collective-permute-start(bf16[8,128,256]{2,1,0:T(8,128)(2,1)S(1)} %pad_maximum_fusion.a_ref), channel_id=1, source_target_pairs={{480,0},{48,16},{0,32},{80,48},{32,64},{112,80},{64,96},{144,112},... | collective-permute-start | bytes 1572872 | tf_op jit(solution)/shard_map/ppermute | solution.py:356
  88.7 4.7 %collective-permute-start = (bf16[128,128]{1,0:T(8,128)(2,1)S(1)}, bf16[128,128]{1,0:T(8,128)(2,1)S(1)}, u32[]{:S(2)}, u32[]{:S(2)}) collective-permute-start(bf16[128,128]{1,0:T(8,128)(2,1)S(1)} %bitcast.15), channel_id=1, source_target_pairs={{16,0},{0,16},{48,32},{32,48},{80,64},{64,80},{112,96},{96,112},{1... | collective-permute-start | bytes 98312 | tf_op jit(solution)/shard_map/ppermute | solution.py:356
  99.9 6.9 %collective-permute-start.5 = (f32[256,256]{1,0:T(8,128)S(1)}, f32[256,256]{1,0:T(8,128)S(1)}, u32[]{:S(2)}, u32[]{:S(2)}) collective-permute-start(f32[256,256]{1,0:T(8,128)S(1)} %get-tuple-element.9), channel_id=1, source_target_pairs={{16,0},{0,16},{48,32},{32,48},{80,64},{64,80},{112,96},{96,112},{1... | collective-permute-start | bytes 786440 | tf_op jit(solution)/shard_map/ppermute | solution.py:356
  106.8 1.0 copy-start
  158.6 9.3 %copy-start.2 = (s32[128,4]{0,1:T(4,128)S(1)}, s32[128,4]{0,1:T(4,128)}, u32[]{:S(2)}) copy-start(s32[128,4]{0,1:T(4,128)} %param.21) | copy-start | bytes 6148
  158.6 9.3 %copy-start.3 = (f32[128,4]{0,1:T(4,128)S(1)}, f32[128,4]{0,1:T(4,128)}, u32[]{:S(2)}) copy-start(f32[128,4]{0,1:T(4,128)} %param.22) | copy-start | bytes 6148
  159.8 26.8 %all-to-all-start.3 = ((bf16[32,24,128]{2,1,0:T(8,128)(2,1)}), bf16[32,24,128]{2,1,0:T(8,128)(2,1)S(1)}, u32[]{:S(2)}, u32[]{:S(2)}) async-start(bf16[32,24,128]{2,1,0:T(8,128)(2,1)} %get-tuple-element.11), calls=%async_computation.3 | async-start | bytes 393216 | tf_op jit(solution)/shard_map/all_to_all | solution.py:368

commit v6 on v5

--- a/solution.py
+++ b/solution.py
@@ -19,14 +19,13 @@
 N_TP = Y * X
 TOK = 128
 CAP = 20
-PAD = 24
 ROWS = N_EP * CAP
-PADDED = N_EP * PAD
+QUARTER = 4
 WIDE = 128
 MODEL = N_TP * WIDE
 OUT_ROWS = ROWS + TOK
 
-STEPS = (0, 8, 4, 12, 2, 10, 6, 14, 1, 9, 5, 13, 3, 11, 7, 15)
+STEPS = (0, 4, 2, 6, 1, 5, 3, 7)
 MIB = 1 << 20
 
 
@@ -59,13 +58,19 @@
         jnp.where(earlier, 1.0, 0.0).astype(BF16),
         preferred_element_type=F32,
     )
-    slot = jnp.where(named > 0.5, rank.astype(jnp.int32), -1)
-    place = lax.broadcasted_iota(jnp.int32, (PAD, TOK), 0)
-    pieces = []
-    for e in range(N_EP):
-        here = slot[e : e + 1, :] == place
-        pieces.append(jnp.where(here, 1.0 if values is None else weight[e : e + 1, :], 0.0))
-    return jnp.concatenate(pieces, axis=0)
+    slot = jnp.where(named > 0.5, rank, -1.0)
+    row = lax.broadcasted_iota(jnp.int32, (ROWS, N_EP), 0)
+    first = lax.broadcasted_iota(jnp.int32, (ROWS, N_EP), 1) * CAP
+    owner = jnp.where((row >= first) & (row < first + CAP), 1.0, 0.0).astype(BF16)
+    parts = [slot, expert.astype(F32)]
+    if values is not None:
+        for _ in range(3):
+            parts.append(weight.astype(BF16).astype(F32))
+            weight = weight - parts[-1]
+    spread = [jnp.dot(owner, p.astype(BF16), preferred_element_type=F32) for p in parts]
+    place = lax.broadcasted_iota(jnp.int32, (ROWS, TOK), 0).astype(F32) - CAP * spread[1]
+    value = 1.0 if values is None else spread[2] + spread[3] + spread[4]
+    return jnp.where(spread[0] == place, value, 0.0)
 
 
 def dispatch_kernel(at_ref, rows_ref, part_ref, gain_ref, ids_ref, out_ref):
@@ -74,13 +79,13 @@
     part = part_ref[...].astype(F32) * lax.rsqrt(mean_sq + NORM_EPS) * gain_ref[...]
     chosen = routing(ids_ref[...]).astype(BF16)
     packed = jnp.dot(chosen, part.astype(BF16), preferred_element_type=F32)
-    out_ref[...] = packed.astype(BF16).reshape(N_EP, PAD, WIDE)
+    out_ref[...] = packed.astype(BF16)
 
 
 def dispatch(at, token_rows, gain, ids):
     return pl.pallas_call(
         dispatch_kernel,
-        out_shape=jax.ShapeDtypeStruct((N_EP, PAD, WIDE), BF16),
+        out_shape=jax.ShapeDtypeStruct((ROWS, WIDE), BF16),
         grid_spec=pltpu.PrefetchScalarGridSpec(
             num_scalar_prefetch=1,
             grid=(1,),
@@ -90,38 +95,11 @@
                 pl.BlockSpec((1, WIDE), lambda i, at: (0, at[0])),
                 pl.BlockSpec((4, TOK), lambda i, at: (0, 0)),
             ],
-            out_specs=pl.BlockSpec((N_EP, PAD, WIDE), lambda i, at: (0, 0, 0)),
+            out_specs=pl.BlockSpec((ROWS, WIDE), lambda i, at: (0, 0)),
         ),
         compiler_params=params(8),
         name="dispatch",
     )(at, *(in_hbm(a) for a in (token_rows, token_rows, gain, ids)))
-
-
-COMPACT_STEPS = 2
-COMPACT_SRC = N_EP // COMPACT_STEPS
-
-
-def compact_kernel(in_ref, out_ref):
-    to = lax.broadcasted_iota(jnp.int32, (2 * CAP, 2 * PAD), 0)
-    src = lax.broadcasted_iota(jnp.int32, (2 * CAP, 2 * PAD), 1)
-    pick = jnp.where(src == jnp.where(to < CAP, to, to + (PAD - CAP)), 1.0, 0.0).astype(BF16)
-    for g in range(0, COMPACT_SRC, 2):
-        block = in_ref[g : g + 2].reshape(2 * PAD, WIDE)
-        kept = jnp.dot(pick, block, preferred_element_type=F32).astype(BF16)
-        for t in range(N_TP):
-            out_ref[t, CAP * g : CAP * (g + 2), :] = kept
-
-
-def compact(arrived):
-    return pl.pallas_call(
-        compact_kernel,
-        out_shape=pltpu.HBM((N_TP, ROWS, WIDE), BF16),
-        grid=(COMPACT_STEPS,),
-        in_specs=[pl.BlockSpec((COMPACT_SRC, PAD, WIDE), lambda i: (i, 0, 0))],
-        out_specs=pl.BlockSpec((N_TP, COMPACT_SRC * CAP, WIDE), lambda i: (0, i, 0)),
-        compiler_params=params(8),
-        name="compact",
-    )(arrived)
 
 
 FFN_ROWS = ROWS // 2
@@ -177,6 +155,9 @@
     )
 
 
+SUM_ROWS = 32
+
+
 def summed_rows(in_ref, low, count):
     total = in_ref[0, low : low + count, :].astype(F32)
     for t in range(1, N_TP):
@@ -185,14 +166,8 @@
 
 
 def reduce_kernel(in_ref, pack_ref, mixed_ref):
-    to = lax.broadcasted_iota(jnp.int32, (2 * PAD, 2 * CAP), 0)
-    src = lax.broadcasted_iota(jnp.int32, (2 * PAD, 2 * CAP), 1)
-    hit = to == jnp.where(src < CAP, src, src + (PAD - CAP))
-    place = jnp.where(hit, 1.0, 0.0).astype(BF16)
-    for g in range(0, N_EP, 2):
-        block = summed_rows(in_ref, CAP * g, 2 * CAP)
-        spread = jnp.dot(place, block, preferred_element_type=F32).astype(BF16)
-        pack_ref[g : g + 2] = spread.reshape(2, PAD, WIDE)
+    for low in range(0, ROWS, SUM_ROWS):
+        pack_ref[low : low + SUM_ROWS, :] = summed_rows(in_ref, low, SUM_ROWS)
     for c in range(N_TP):
         mixed_ref[:, c * WIDE : (c + 1) * WIDE] = summed_rows(in_ref, ROWS + 8 * c, 8)
 
@@ -202,7 +177,7 @@
     return pl.pallas_call(
         reduce_kernel,
         out_shape=(
-            pltpu.VMEM((N_EP, PAD, WIDE), BF16),
+            jax.ShapeDtypeStruct((ROWS, WIDE), BF16),
             jax.ShapeDtypeStruct((TOK // N_TP, MODEL), BF16),
         ),
         in_specs=[vmem],
@@ -223,7 +198,7 @@
     vmem = pl.BlockSpec(memory_space=pltpu.VMEM)
     return pl.pallas_call(
         weigh_kernel,
-        out_shape=(pltpu.VMEM((TOK, PADDED), BF16),) * 2,
+        out_shape=(pltpu.VMEM((TOK, ROWS), BF16),) * 2,
         in_specs=[vmem] * 2,
         out_specs=(vmem, vmem),
         compiler_params=params(8),
@@ -232,7 +207,7 @@
 
 
 def combine_kernel(back_ref, high_ref, low_ref, out_ref):
-    back = back_ref[...].reshape(PADDED, WIDE)
+    back = back_ref[...]
     mixed = jnp.dot(high_ref[...], back, preferred_element_type=F32)
     mixed = mixed + jnp.dot(low_ref[...], back, preferred_element_type=F32)
     out_ref[...] = mixed.astype(BF16)
@@ -263,8 +238,11 @@
     ahead = lax.broadcasted_iota(jnp.int32, (2 * TOK, TOK), 1) - row
     z, core = z_ref[0], core_ref[0]
     mine, theirs = CORE * z + core, CORE * z + 1 - core
-    sign = 2 * core - 1
-    blocks = [CORE * ((z + sign * step) & (Z - 1)) + core for step in STEPS]
+    blocks = []
+    for step in STEPS:
+        down = CORE * ((z - step) & (Z - 1))
+        up = CORE * ((z + 1 + step) & (Z - 1))
+        blocks += [jnp.where(core == 0, down + 1, up), jnp.where(core == 0, down, up + 1)]
     top = jnp.full((4 * TOK, TOK), -1e30, F32)
     for n in range(0, Z, 2):
         keys = (a_ref, b_ref)[n // 8][n % 8 : n % 8 + 2, :, :WIDE].reshape(2 * TOK, WIDE)
@@ -343,7 +321,7 @@
         out_specs=vmem,
         compiler_params=params(8),
         name="project",
-    )(lam, own, other, gain, w)
+    )(lam, own, other, gain, in_hbm(w))
 
 
 def moved(array, source):
@@ -368,9 +346,15 @@
     return lax.all_to_all(array, axes, split_axis=0, concat_axis=0, tiled=True)
 
 
-def collect_keys(keys, values):
-    held = jnp.concatenate([keys, values], axis=-1)[None]
-    held = jnp.concatenate([held, along(held, 8)], axis=0)
+def exchanged_rows(rows):
+    return exchanged(rows.reshape(ROWS // QUARTER, QUARTER, WIDE), EP).reshape(ROWS, WIDE)
+
+
+def collect_keys(keys, values, core_at):
+    mine = jnp.concatenate([keys, values], axis=-1)
+    first = moved(mine, lambda z, core: (z + 1, 0) if core else (z, 1))
+    second = moved(mine, lambda z, core: (z + 1, 1) if core else None)
+    held = jnp.stack([first, jnp.where(core_at == 0, mine, second)])
     held = jnp.concatenate([held, along(held, 4)], axis=0)
     held = jnp.concatenate([held, along(held, 2)], axis=0)
     return held, along(held, 1)
@@ -396,20 +380,20 @@
     tp_at = lax.axis_index(TP).astype(jnp.int32)
     ids = expert_ids.T
     packed = dispatch(tp_at.reshape(1), token_rows, norm_gain.reshape(1, MODEL), ids)
-    arrived = exchanged(packed, EP)
-    blocks = collect_keys(key_maps.reshape(TOK, WIDE), value_rows.reshape(TOK, WIDE))
+    arrived = exchanged_rows(packed)
+    blocks = collect_keys(key_maps.reshape(TOK, WIDE), value_rows.reshape(TOK, WIDE), core_at)
     queries = query_maps.reshape(TOK, WIDE)
     swapped = across(queries)
     own, theirs = attend(z_at.reshape(1), core_at.reshape(1), queries, swapped, blocks)
     other = across(theirs)
     proj = project(head_lambda, own, other, head_gain.reshape(1, WIDE), out_weight)
     high, low = weigh(ids, route_weights.T)
-    spread = compact(arrived)
+    spread = jnp.broadcast_to(arrived[None], (N_TP, ROWS, WIDE))
     x = exchanged(spread, TP)
     terms = ffn(x, gate_weight[0], up_weight[0], down_weight[0], proj)
     y = exchanged(terms, TP)
     back, mixed_rows = reduce_terms(y)
-    returned = exchanged(back, EP)
+    returned = exchanged_rows(back)
     mixed_experts = combine(returned, high, low)
     return (mixed_rows, mixed_experts)
 

time: 188 us -> 174 us (0.926)
  starting transfers between devices: 44 us -> 37.2 us
  waiting for transfers between devices: 45.1 us -> 39.6 us
  blocking collectives: 80.9 us -> 78.9 us
    ppermute x6 -> x7, starting transfers between devices: 29.1 us -> 24.2 us  [moved(): return lax.ppermute(array, EP, pairs)]
    ppermute x6 -> x7, waiting for transfers between devices: 26.6 us -> 23.1 us  [moved(): return lax.ppermute(array, EP, pairs)]
    broadcast_in_dim x0 -> x1, local copies, waits for them, and re-layouts: none -> 2 us  [body(): spread = jnp.broadcast_to(arrived[None], (N_TP, ROWS, WIDE))]
    all_to_all x2, blocking collectives: 80.9 us -> 78.9 us  [exchanged(): return lax.all_to_all(array, axes, split_axis=0, concat_axis=0, tiled=True)]
    all_to_all x2, waiting for transfers between devices: 18.4 us -> 16.5 us  [exchanged(): return lax.all_to_all(array, axes, split_axis=0, concat_axis=0, tiled=True)]
    all_to_all x2, starting transfers between devices: 14.9 us -> 13 us  [exchanged(): return lax.all_to_all(array, axes, split_axis=0, concat_axis=0, tiled=True)]
    pallas_call x4 -> x3, Pallas kernels: 4.83 us -> 3.24 us  [the longest x1 1.62 us: dispatch(): pl.pallas_call(dispatch_kernel, out_shape=jax.ShapeDtypeStruct((ROWS, WID...]
  transfers between devices with their start and end apart: 8 -> 9, of which waited for: 7 -> 8; matrix products, arithmetic and copies ran while one was open for 0% -> 0% of each run, Pallas kernels for 3% -> 4%
where the time goes in v6:
time: 174 us
  blocking collectives  78.9 us (45%)
  waiting for transfers between devices  39.6 us (23%)
  starting transfers between devices  37.2 us (21%)
  Pallas kernels  14.3 us (8%)
  local copies, waits for them, and re-layouts  2.03 us (1%)
    all_to_all x2, blocking collectives, exchanged(): return lax.all_to_all(array, axes, split_axis=0, concat_axis=0, tiled=True)  78.9 us
    ppermute x7, starting transfers between devices, moved(): return lax.ppermute(array, EP, pairs)  24.2 us
    ppermute x7, waiting for transfers between devices, moved(): return lax.ppermute(array, EP, pairs)  23.1 us
    all_to_all x2, waiting for transfers between devices, exchanged(): return lax.all_to_all(array, axes, split_axis=0, concat_axis=0, tiled=True)  16.5 us
    all_to_all x2, starting transfers between devices, exchanged(): return lax.all_to_all(array, axes, split_axis=0, concat_axis=0, tiled=True)  13 us
    pallas_call x1, Pallas kernels, ffn(): pl.pallas_call(ffn_kernel, out_shape=pltpu.VMEM((N_TP, OUT_ROWS, WIDE), B...  4.53 us
    pallas_call x1, Pallas kernels, attend(): pl.pallas_call(attend_kernel, out_shape=(part, part), in_specs=[smem] * 2...  4.04 us
  transfers between devices with their start and end apart: 9, of which 8 were waited for; matrix products, arithmetic and copies ran while one was open for 0% of the time, Pallas kernels for 4%

profile of v6, /device:TPU:1, one launch (start us, length us, event | category | flops | bytes accessed | tf_op | source)
XLA Modules:
  0.0 173.7 jit_solution(9561738515685231680)
XLA Ops:
  0.6 1.6 dispatch.1
  2.3 33.7 %all_to_all.20 = bf16[160,4,128]{2,1,0:T(4,128)(2,1)S(1)} all-to-all(bf16[160,4,128]{2,1,0:T(4,128)(2,1)S(1)} %bitcast.20), channel_id=1, replica_groups=mesh['z'=16,'core'=2,'y'=4,'x'=4] {'z','core'}, dimensions={0} | all-to-all | bytes 327680 | tf_op jit(solution)/shard_map/all_to_all | solution.py:346
  35.9 2.0 %broadcast_in_dim.8 = bf16[16,640,128]{2,1,0:T(8,128)(2,1)} broadcast(bf16[640,128]{1,0:T(8,128)(2,1)S(1)} %bitcast.31), dimensions={1,2} | broadcast | bytes 2785280 | tf_op jit(solution)/shard_map/broadcast_in_dim | solution.py:391
  37.9 0.0 copy-start.4
  37.9 0.0 copy-start.5
  37.9 0.0 copy-start
  37.9 0.0 copy-start.3
  38.0 6.9 %all-to-all-start.1 = ((bf16[16,640,128]{2,1,0:T(8,128)(2,1)}), bf16[16,640,128]{2,1,0:T(8,128)(2,1)S(1)}, u32[]{:S(2)}, u32[]{:S(2)}) async-start(bf16[16,640,128]{2,1,0:T(8,128)(2,1)} %broadcast_in_dim.8), calls=%async_computation.1 | async-start | bytes 5242880 | tf_op jit(solution)/shard_map/all_to_all | solution.py:346
  44.9 0.0 copy-done.4
  44.9 0.0 copy-done.5
  44.9 1.9 %collective-permute-start.2 = (bf16[128,256]{1,0:T(8,128)(2,1)S(1)}, bf16[128,256]{1,0:T(8,128)(2,1)S(1)}, u32[]{:S(2)}, u32[]{:S(2)}) collective-permute-start(bf16[128,256]{1,0:T(8,128)(2,1)S(1)} %pad_maximum_fusion.3), channel_id=1, source_target_pairs={{48,16},{80,48},{112,80},{144,112},{176,144},{208,176},{240,208},{... | collective-permute-start | bytes 196616 | tf_op jit(solution)/shard_map/ppermute | solution.py:334
  46.8 0.7 collective-permute-start.1
  47.6 2.4 %collective-permute-done.2 = bf16[128,256]{1,0:T(8,128)(2,1)S(1)} collective-permute-done((bf16[128,256]{1,0:T(8,128)(2,1)S(1)}, bf16[128,256]{1,0:T(8,128)(2,1)S(1)}, u32[]{:S(2)}, u32[]{:S(2)}) %collective-permute-start.2) | collective-permute-done | bytes 65568 | tf_op jit(solution)/shard_map/ppermute | solution.py:334
  50.0 0.6 collective-permute-done.1
  50.6 3.4 %collective-permute-start.3 = (bf16[2,128,256]{2,1,0:T(8,128)(2,1)S(1)}, bf16[2,128,256]{2,1,0:T(8,128)(2,1)S(1)}, u32[]{:S(2)}, u32[]{:S(2)}) collective-permute-start(bf16[2,128,256]{2,1,0:T(8,128)(2,1)S(1)} %pad_maximum_fusion.2), channel_id=1, source_target_pairs={{384,0},{144,16},{416,32},{176,48},{448,64},{208,80},{480,96},{240... | collective-permute-start | bytes 393224 | tf_op jit(solution)/shard_map/ppermute | solution.py:334
  54.0 9.4 %collective-permute-done.3 = bf16[2,128,256]{2,1,0:T(8,128)(2,1)S(1)} collective-permute-done((bf16[2,128,256]{2,1,0:T(8,128)(2,1)S(1)}, bf16[2,128,256]{2,1,0:T(8,128)(2,1)S(1)}, u32[]{:S(2)}, u32[]{:S(2)}) %collective-permute-start.3) | collective-permute-done | bytes 131104 | tf_op jit(solution)/shard_map/ppermute | solution.py:334
  63.5 1.9 %collective-permute-start.4 = (bf16[4,128,256]{2,1,0:T(8,128)(2,1)S(1)}, bf16[4,128,256]{2,1,0:T(8,128)(2,1)S(1)}, u32[]{:S(2)}, u32[]{:S(2)}) collective-permute-start(bf16[4,128,256]{2,1,0:T(8,128)(2,1)S(1)} %pad_maximum_fusion.1), channel_id=1, source_target_pairs={{448,0},{80,16},{480,32},{112,48},{0,64},{144,80},{32,96},{176,112... | collective-permute-start | bytes 786440 | tf_op jit(solution)/shard_map/ppermute | solution.py:334
  65.4 6.6 %collective-permute-done.4 = bf16[4,128,256]{2,1,0:T(8,128)(2,1)S(1)} collective-permute-done((bf16[4,128,256]{2,1,0:T(8,128)(2,1)S(1)}, bf16[4,128,256]{2,1,0:T(8,128)(2,1)S(1)}, u32[]{:S(2)}, u32[]{:S(2)}) %collective-permute-start.4) | collective-permute-done | bytes 262176 | tf_op jit(solution)/shard_map/ppermute | solution.py:334
  72.0 0.1 pad_maximum_fusion.a_ref
  72.1 6.8 %collective-permute-start.5 = (bf16[8,128,256]{2,1,0:T(8,128)(2,1)S(1)}, bf16[8,128,256]{2,1,0:T(8,128)(2,1)}, u32[]{:S(2)}, u32[]{:S(2)}) collective-permute-start(bf16[8,128,256]{2,1,0:T(8,128)(2,1)S(1)} %pad_maximum_fusion.a_ref), channel_id=1, source_target_pairs={{480,0},{48,16},{0,32},{80,48},{32,64},{112,80},{64,96},{144,112},... | collective-permute-start | bytes 1572872 | tf_op jit(solution)/shard_map/ppermute | solution.py:334
  78.9 0.0 copy-done
  78.9 2.5 %collective-permute-start = (bf16[128,128]{1,0:T(8,128)(2,1)S(1)}, bf16[128,128]{1,0:T(8,128)(2,1)S(1)}, u32[]{:S(2)}, u32[]{:S(2)}) collective-permute-start(bf16[128,128]{1,0:T(8,128)(2,1)S(1)} %bitcast.22), channel_id=1, source_target_pairs={{16,0},{0,16},{48,32},{32,48},{80,64},{64,80},{112,96},{96,112},{1... | collective-permute-start | bytes 98312 | tf_op jit(solution)/shard_map/ppermute | solution.py:334
  81.4 0.8 collective-permute-done.swapped_ref
  82.3 2.7 %collective-permute-done.5.b_ref = bf16[8,128,256]{2,1,0:T(8,128)(2,1)} collective-permute-done((bf16[8,128,256]{2,1,0:T(8,128)(2,1)S(1)}, bf16[8,128,256]{2,1,0:T(8,128)(2,1)}, u32[]{:S(2)}, u32[]{:S(2)}) %collective-permute-start.5) | collective-permute-done | bytes 524320 | tf_op jit(solution)/shard_map/ppermute | solution.py:334
  85.0 4.0 %attend.1 = (f32[256,256]{1,0:T(8,128)S(1)}, f32[256,256]{1,0:T(8,128)S(1)}) custom-call(s32[1]{0:T(128)} %bitcast.8.z_ref, s32[1]{0:T(128)} %bitcast.9.core_ref, bf16[128,128]{1,0:T(8,128)(2,1)S(1)} %bitcast.23, bf16[128,128]{1,0:T(8,128)(2,1)S(1)} %collective-permute-done.swapped_ref, bf16[8,128,256]{2,1,0:T(8,128)(2,1)S(1)} %pad_maximum_fusion.a_ref, ...), custom_call_target="tpu_custom_call" | custom-call | tf_op jit(solution)/shard_map/attend/pallas_call | solution.py:288
  89.1 6.9 %collective-permute-start.6 = (f32[256,256]{1,0:T(8,128)S(1)}, f32[256,256]{1,0:T(8,128)S(1)}, u32[]{:S(2)}, u32[]{:S(2)}) collective-permute-start(f32[256,256]{1,0:T(8,128)S(1)} %get-tuple-element.9), channel_id=1, source_target_pairs={{16,0},{0,16},{48,32},{32,48},{80,64},{64,80},{112,96},{96,112},{1... | collective-permute-start | bytes 786440 | tf_op jit(solution)/shard_map/ppermute | solution.py:334
  96.6 0.5 collective-permute-done.6.other_ref
  97.1 0.0 copy-done.3
  97.1 1.7 project.1.proj_ref
  98.7 0.0 all-to-all-done.1.x_ref
  98.8 4.5 %ffn.1 = bf16[16,768,128]{2,1,0:T(8,128)(2,1)S(1)} custom-call(bf16[16,640,128]{2,1,0:T(8,128)(2,1)S(1)} %all-to-all-done.1.x_ref, bf16[2048,256]{1,0:T(8,128)(2,1)} %bitcast.28, bf16[2048,256]{1,0:T(8,128)(2,1)} %bitcast.29, bf16[256,2048]{1,0:T(8,128)(2,1)} %bitcast.30, bf16[16,128,128]{2,1,0:T(8,128)(2,1)S(1)} %project.1.proj_ref), custom_call_target="tpu_custom_call" | custom-call | tf_op jit(solution)/shard_map/ffn/pallas_call | solution.py:138
  103.3 45.3 %all_to_all.21.in_ref = bf16[16,768,128]{2,1,0:T(8,128)(2,1)S(1)} all-to-all(bf16[16,768,128]{2,1,0:T(8,128)(2,1)S(1)} %ffn.1), channel_id=1, replica_groups=mesh['z'=16,'core'=2,'y'=4,'x'=4] {'y','x'}, dimensions={0} | all-to-all | bytes 6291456 | tf_op jit(solution)/shard_map/all_to_all | solution.py:346
  148.6 0.0 copy-start.1
  148.6 0.0 copy-start.2
  148.6 1.0 reduce_terms.1
  149.6 6.1 %all-to-all-start.3 = ((bf16[160,4,128]{2,1,0:T(4,128)(2,1)}), bf16[160,4,128]{2,1,0:T(4,128)(2,1)S(1)}, u32[]{:S(2)}, u32[]{:S(2)}) async-start(bf16[160,4,128]{2,1,0:T(4,128)(2,1)} %bitcast.16), calls=%async_computation.3 | async-start | bytes 327680 | tf_op jit(solution)/shard_map/all_to_all | solution.py:346
  155.7 0.0 copy-done.1
  155.7 0.0 copy-done.2
  155.7 0.6 weigh.1
  156.3 16.5 %all-to-all-done.3 = bf16[160,4,128]{2,1,0:T(4,128)(2,1)S(1)} async-done(((bf16[160,4,128]{2,1,0:T(4,128)(2,1)}), bf16[160,4,128]{2,1,0:T(4,128)(2,1)S(1)}, u32[]{:S(2)}, u32[]{:S(2)}) %all-to-all-start.3) | async-done | bytes 163872 | tf_op jit(solution)/shard_map/all_to_all | solution.py:346
  172.8 0.9 combine.1
  (4 shorter events, 0.1 us)
Async XLA Ops:
  37.9 6.9 %copy-start.4 = (bf16[128,1,128]{2,0,1:T(8,128)(2,1)S(1)}, bf16[128,1,128]{2,0,1:T(8,128)(2,1)}, u32[]{:S(2)}) copy-start(bf16[128,1,128]{2,0,1:T(8,128)(2,1)} %param.15) | copy-start | bytes 98308
  37.9 6.9 %copy-start.5 = (bf16[128,1,128]{2,0,1:T(8,128)(2,1)S(1)}, bf16[128,1,128]{2,0,1:T(8,128)(2,1)}, u32[]{:S(2)}) copy-start(bf16[128,1,128]{2,0,1:T(8,128)(2,1)} %param.14) | copy-start | bytes 98308
  37.9 41.0 %copy-start = (bf16[128,1,128]{2,0,1:T(8,128)(2,1)S(1)}, bf16[128,1,128]{2,0,1:T(8,128)(2,1)}, u32[]{:S(2)}) copy-start(bf16[128,1,128]{2,0,1:T(8,128)(2,1)} %param.13) | copy-start | bytes 98308
  37.9 59.1 %copy-start.3 = (f32[128]{0:T(128)S(1)}, f32[128]{0:T(128)}, u32[]{:S(2)}) copy-start(f32[128]{0:T(128)} %param.17) | copy-start | bytes 1540
  38.0 60.8 %all-to-all-start.1 = ((bf16[16,640,128]{2,1,0:T(8,128)(2,1)}), bf16[16,640,128]{2,1,0:T(8,128)(2,1)S(1)}, u32[]{:S(2)}, u32[]{:S(2)}) async-start(bf16[16,640,128]{2,1,0:T(8,128)(2,1)} %broadcast_in_dim.8), calls=%async_computation.1 | async-start | bytes 5242880 | tf_op jit(solution)/shard_map/all_to_all | solution.py:346
  44.9 5.1 %collective-permute-start.2 = (bf16[128,256]{1,0:T(8,128)(2,1)S(1)}, bf16[128,256]{1,0:T(8,128)(2,1)S(1)}, u32[]{:S(2)}, u32[]{:S(2)}) collective-permute-start(bf16[128,256]{1,0:T(8,128)(2,1)S(1)} %pad_maximum_fusion.3), channel_id=1, source_target_pairs={{48,16},{80,48},{112,80},{144,112},{176,144},{208,176},{240,208},{... | collective-permute-start | bytes 196616 | tf_op jit(solution)/shard_map/ppermute | solution.py:334
  46.8 3.8 %collective-permute-start.1 = (bf16[128,256]{1,0:T(8,128)(2,1)S(1)}, bf16[128,256]{1,0:T(8,128)(2,1)S(1)}, u32[]{:S(2)}, u32[]{:S(2)}) collective-permute-start(bf16[128,256]{1,0:T(8,128)(2,1)S(1)} %pad_maximum_fusion.3), channel_id=1, source_target_pairs={{16,0},{32,16},{48,32},{64,48},{80,64},{96,80},{112,96},{128,112},... | collective-permute-start | bytes 196616 | tf_op jit(solution)/shard_map/ppermute | solution.py:334
  50.6 12.9 %collective-permute-start.3 = (bf16[2,128,256]{2,1,0:T(8,128)(2,1)S(1)}, bf16[2,128,256]{2,1,0:T(8,128)(2,1)S(1)}, u32[]{:S(2)}, u32[]{:S(2)}) collective-permute-start(bf16[2,128,256]{2,1,0:T(8,128)(2,1)S(1)} %pad_maximum_fusion.2), channel_id=1, source_target_pairs={{384,0},{144,16},{416,32},{176,48},{448,64},{208,80},{480,96},{240... | collective-permute-start | bytes 393224 | tf_op jit(solution)/shard_map/ppermute | solution.py:334
  63.5 8.5 %collective-permute-start.4 = (bf16[4,128,256]{2,1,0:T(8,128)(2,1)S(1)}, bf16[4,128,256]{2,1,0:T(8,128)(2,1)S(1)}, u32[]{:S(2)}, u32[]{:S(2)}) collective-permute-start(bf16[4,128,256]{2,1,0:T(8,128)(2,1)S(1)} %pad_maximum_fusion.1), channel_id=1, source_target_pairs={{448,0},{80,16},{480,32},{112,48},{0,64},{144,80},{32,96},{176,112... | collective-permute-start | bytes 786440 | tf_op jit(solution)/shard_map/ppermute | solution.py:334
  72.1 12.9 %collective-permute-start.5 = (bf16[8,128,256]{2,1,0:T(8,128)(2,1)S(1)}, bf16[8,128,256]{2,1,0:T(8,128)(2,1)}, u32[]{:S(2)}, u32[]{:S(2)}) collective-permute-start(bf16[8,128,256]{2,1,0:T(8,128)(2,1)S(1)} %pad_maximum_fusion.a_ref), channel_id=1, source_target_pairs={{480,0},{48,16},{0,32},{80,48},{32,64},{112,80},{64,96},{144,112},... | collective-permute-start | bytes 1572872 | tf_op jit(solution)/shard_map/ppermute | solution.py:334
  78.9 3.4 %collective-permute-start = (bf16[128,128]{1,0:T(8,128)(2,1)S(1)}, bf16[128,128]{1,0:T(8,128)(2,1)S(1)}, u32[]{:S(2)}, u32[]{:S(2)}) collective-permute-start(bf16[128,128]{1,0:T(8,128)(2,1)S(1)} %bitcast.22), channel_id=1, source_target_pairs={{16,0},{0,16},{48,32},{32,48},{80,64},{64,80},{112,96},{96,112},{1... | collective-permute-start | bytes 98312 | tf_op jit(solution)/shard_map/ppermute | solution.py:334
  89.1 8.0 %collective-permute-start.6 = (f32[256,256]{1,0:T(8,128)S(1)}, f32[256,256]{1,0:T(8,128)S(1)}, u32[]{:S(2)}, u32[]{:S(2)}) collective-permute-start(f32[256,256]{1,0:T(8,128)S(1)} %get-tuple-element.9), channel_id=1, source_target_pairs={{16,0},{0,16},{48,32},{32,48},{80,64},{64,80},{112,96},{96,112},{1... | collective-permute-start | bytes 786440 | tf_op jit(solution)/shard_map/ppermute | solution.py:334
  148.6 7.2 %copy-start.1 = (s32[128,4]{0,1:T(4,128)S(1)}, s32[128,4]{0,1:T(4,128)}, u32[]{:S(2)}) copy-start(s32[128,4]{0,1:T(4,128)} %param.21) | copy-start | bytes 6148
  148.6 7.2 %copy-start.2 = (f32[128,4]{0,1:T(4,128)S(1)}, f32[128,4]{0,1:T(4,128)}, u32[]{:S(2)}) copy-start(f32[128,4]{0,1:T(4,128)} %param.22) | copy-start | bytes 6148
  149.6 23.3 %all-to-all-start.3 = ((bf16[160,4,128]{2,1,0:T(4,128)(2,1)}), bf16[160,4,128]{2,1,0:T(4,128)(2,1)S(1)}, u32[]{:S(2)}, u32[]{:S(2)}) async-start(bf16[160,4,128]{2,1,0:T(4,128)(2,1)} %bitcast.16), calls=%async_computation.3 | async-start | bytes 327680 | tf_op jit(solution)/shard_map/all_to_all | solution.py:346

commit v7 on v6

--- a/solution.py
+++ b/solution.py
@@ -1,3 +1,5 @@
+import functools
+
 import jax
 import jax.numpy as jnp
 from jax import lax
@@ -102,6 +104,28 @@
     )(at, *(in_hbm(a) for a in (token_rows, token_rows, gain, ids)))
 
 
+def spread_kernel(in_ref, out_hbm, sems):
+    copies = [
+        pltpu.make_async_copy(in_ref, out_hbm.at[t], sems.at[t]) for t in range(N_TP)
+    ]
+    for copy in copies:
+        copy.start()
+    for copy in copies:
+        copy.wait()
+
+
+def spread_rows(rows):
+    return pl.pallas_call(
+        spread_kernel,
+        out_shape=pltpu.HBM((N_TP, ROWS, WIDE), BF16),
+        in_specs=[pl.BlockSpec(memory_space=pltpu.VMEM)],
+        out_specs=pl.BlockSpec(memory_space=pl.ANY),
+        scratch_shapes=[pltpu.SemaphoreType.DMA((N_TP,))],
+        compiler_params=params(4),
+        name="spread_rows",
+    )(in_vmem(rows))
+
+
 FFN_ROWS = ROWS // 2
 
 
@@ -225,7 +249,8 @@
     )(*(in_vmem(a) for a in (back, high, low)))
 
 
-def attend_kernel(z_ref, core_ref, q_ref, swapped_ref, a_ref, b_ref, own_ref, other_ref, score_ref):
+def attend_kernel(late, z_ref, core_ref, q_ref, swapped_ref, keys_ref, *refs):
+    found_ref, *out_refs, score_ref = refs if late else (None, *refs)
     lane = lax.broadcasted_iota(jnp.int32, (TOK, WIDE), 1)
     parts = []
     for ref in (q_ref, swapped_ref):
@@ -239,13 +264,13 @@
     z, core = z_ref[0], core_ref[0]
     mine, theirs = CORE * z + core, CORE * z + 1 - core
     blocks = []
-    for step in STEPS:
+    for step in STEPS[4:] if late else STEPS[:4]:
         down = CORE * ((z - step) & (Z - 1))
         up = CORE * ((z + 1 + step) & (Z - 1))
         blocks += [jnp.where(core == 0, down + 1, up), jnp.where(core == 0, down, up + 1)]
     top = jnp.full((4 * TOK, TOK), -1e30, F32)
-    for n in range(0, Z, 2):
-        keys = (a_ref, b_ref)[n // 8][n % 8 : n % 8 + 2, :, :WIDE].reshape(2 * TOK, WIDE)
+    for n in range(0, len(blocks), 2):
+        keys = keys_ref[n : n + 2, :, :WIDE].reshape(2 * TOK, WIDE)
         scores = lax.dot_general(
             queries, keys, (((1,), (1,)), ((), ())), preferred_element_type=F32
         )
@@ -265,35 +290,42 @@
             score_ref[n // 2, :, cols] = part
             top = jnp.maximum(top, part)
     row_max = jnp.max(top, axis=-1, keepdims=True)
+    if late:
+        row_max = jnp.maximum(row_max, found_ref[:, WIDE : WIDE + 1])
     total = jnp.zeros((4 * TOK, 2 * TOK), F32)
     value_sum = jnp.zeros((4 * TOK, WIDE), F32)
-    for n in range(0, Z, 2):
+    for n in range(0, len(blocks), 2):
         terms = jnp.exp(score_ref[n // 2] - row_max)
         total = total + terms
-        values = (a_ref, b_ref)[n // 8][n % 8 : n % 8 + 2, :, WIDE:].reshape(2 * TOK, WIDE)
+        values = keys_ref[n : n + 2, :, WIDE:].reshape(2 * TOK, WIDE)
         value_sum = value_sum + jnp.dot(terms.astype(BF16), values, preferred_element_type=F32)
     total = jnp.sum(total, axis=-1, keepdims=True)
+    if late:
+        scale = jnp.exp(found_ref[:, WIDE : WIDE + 1] - row_max)
+        total = total + found_ref[:, WIDE + 64 : WIDE + 65] * scale
+        value_sum = value_sum + found_ref[:, :WIDE] * scale
     wide = lax.broadcasted_iota(jnp.int32, (4 * TOK, WIDE), 1)
     beside = jnp.where(wide < 64, row_max, total)
-    for i, ref in enumerate((own_ref, other_ref)):
-        rows = slice(2 * TOK * i, 2 * TOK * (i + 1))
-        ref[:, :WIDE] = value_sum[rows]
-        ref[:, WIDE:] = beside[rows]
-
-
-def attend(z_at, core_at, q, swapped, blocks):
+    count = 4 * TOK // len(out_refs)
+    for i, ref in enumerate(out_refs):
+        ref[:, :WIDE] = value_sum[i * count : (i + 1) * count]
+        ref[:, WIDE:] = beside[i * count : (i + 1) * count]
+
+
+def attend(z_at, core_at, q, swapped, keys, found=None):
     vmem = pl.BlockSpec(memory_space=pltpu.VMEM)
     smem = pl.BlockSpec(memory_space=pltpu.SMEM)
-    part = jax.ShapeDtypeStruct((2 * TOK, 2 * WIDE), F32)
-    return pl.pallas_call(
-        attend_kernel,
-        out_shape=(part, part),
-        in_specs=[smem] * 2 + [vmem] * 4,
-        out_specs=(vmem, vmem),
-        scratch_shapes=[pltpu.VMEM((Z // 2, 4 * TOK, 2 * TOK), F32)],
-        compiler_params=params(20),
-        name="attend",
-    )(z_at, core_at, q, swapped, *blocks)
+    late = found is not None
+    out = ((2 * TOK, 2 * WIDE),) * 2 if late else ((4 * TOK, 2 * WIDE),)
+    return pl.pallas_call(
+        functools.partial(attend_kernel, late),
+        out_shape=tuple(jax.ShapeDtypeStruct(shape, F32) for shape in out),
+        in_specs=[smem] * 2 + [vmem] * (4 if late else 3),
+        out_specs=(vmem,) * len(out),
+        scratch_shapes=[pltpu.VMEM((Z // 4, 4 * TOK, 2 * TOK), F32)],
+        compiler_params=params(14),
+        name="attend_late" if late else "attend_early",
+    )(z_at, core_at, q, swapped, keys, *(found or ()))
 
 
 def project_kernel(lam_ref, own_ref, other_ref, gain_ref, w_ref, out_ref):
@@ -384,11 +416,13 @@
     blocks = collect_keys(key_maps.reshape(TOK, WIDE), value_rows.reshape(TOK, WIDE), core_at)
     queries = query_maps.reshape(TOK, WIDE)
     swapped = across(queries)
-    own, theirs = attend(z_at.reshape(1), core_at.reshape(1), queries, swapped, blocks)
+    at = z_at.reshape(1), core_at.reshape(1), queries, swapped
+    found = attend(*at, blocks[0])
+    own, theirs = attend(*at, blocks[1], found)
     other = across(theirs)
     proj = project(head_lambda, own, other, head_gain.reshape(1, WIDE), out_weight)
     high, low = weigh(ids, route_weights.T)
-    spread = jnp.broadcast_to(arrived[None], (N_TP, ROWS, WIDE))
+    spread = spread_rows(arrived)
     x = exchanged(spread, TP)
     terms = ffn(x, gate_weight[0], up_weight[0], down_weight[0], proj)
     y = exchanged(terms, TP)

time: 174 us -> 173 us (level)
  Pallas kernels: 14.3 us -> 16.4 us
  local copies, waits for them, and re-layouts: 2.03 us -> 0.03 us
    pallas_call x1 -> x3, Pallas kernels: 4.04 us -> 6.13 us  [the longest x2 4.49 us: attend(): pl.pallas_call(functools.partial(attend_kernel, late), out_shape=tuple((j...]
    broadcast_in_dim x1 -> x0, local copies, waits for them, and re-layouts: 2 us -> none  [body(): spread = jnp.broadcast_to(arrived[None], (N_TP, ROWS, WIDE))]
where the time goes in v7:
time: 173 us; the launch traced here: 172 us
  blocking collectives  79 us (46%)
  waiting for transfers between devices  38.1 us (22%)
  starting transfers between devices  37.2 us (22%)
  Pallas kernels  16.4 us (9%)
    all_to_all x2, blocking collectives, exchanged(): return lax.all_to_all(array, axes, split_axis=0, concat_axis=0, tiled=True)  79 us
    ppermute x7, starting transfers between devices, moved(): return lax.ppermute(array, EP, pairs)  24.2 us
    ppermute x7, waiting for transfers between devices, moved(): return lax.ppermute(array, EP, pairs)  21.6 us
    all_to_all x2, waiting for transfers between devices, exchanged(): return lax.all_to_all(array, axes, split_axis=0, concat_axis=0, tiled=True)  16.5 us
    all_to_all x2, starting transfers between devices, exchanged(): return lax.all_to_all(array, axes, split_axis=0, concat_axis=0, tiled=True)  13 us
    pallas_call x1, Pallas kernels, ffn(): pl.pallas_call(ffn_kernel, out_shape=pltpu.VMEM((N_TP, OUT_ROWS, WIDE), B...  4.52 us
    pallas_call x2, Pallas kernels, attend(): pl.pallas_call(functools.partial(attend_kernel, late), out_shape=tuple((j...  4.49 us
  transfers between devices with their start and end apart: 9, of which 8 were waited for; matrix products, arithmetic and copies ran while one was open for 0% of the time, Pallas kernels for 4%

profile of v7, /device:TPU:1, one launch (start us, length us, event | category | flops | bytes accessed | tf_op | source)
XLA Modules:
  0.0 172.3 jit_solution(15107605660088131166)
XLA Ops:
  0.6 1.6 dispatch.1
  2.3 33.7 %all_to_all.20 = bf16[160,4,128]{2,1,0:T(4,128)(2,1)S(1)} all-to-all(bf16[160,4,128]{2,1,0:T(4,128)(2,1)S(1)} %bitcast.20), channel_id=1, replica_groups=mesh['z'=16,'core'=2,'y'=4,'x'=4] {'z','core'}, dimensions={0} | all-to-all | bytes 327680 | tf_op jit(solution)/shard_map/all_to_all | solution.py:378
  35.9 1.6 spread_rows.1
  37.6 0.0 copy-start.4
  37.6 0.0 copy-start.5
  37.6 0.0 copy-start
  37.6 6.9 %all-to-all-start.1 = ((bf16[16,640,128]{2,1,0:T(8,128)(2,1)}), bf16[16,640,128]{2,1,0:T(8,128)(2,1)S(1)}, u32[]{:S(2)}, u32[]{:S(2)}) async-start(bf16[16,640,128]{2,1,0:T(8,128)(2,1)} %spread_rows.1), calls=%async_computation.1 | async-start | bytes 5242880 | tf_op jit(solution)/shard_map/all_to_all | solution.py:378
  44.5 0.0 copy-start.3
  44.5 0.0 copy-done.4
  44.5 0.0 copy-done.5
  44.6 1.9 %collective-permute-start.2 = (bf16[128,256]{1,0:T(8,128)(2,1)S(1)}, bf16[128,256]{1,0:T(8,128)(2,1)S(1)}, u32[]{:S(2)}, u32[]{:S(2)}) collective-permute-start(bf16[128,256]{1,0:T(8,128)(2,1)S(1)} %pad_maximum_fusion.3), channel_id=1, source_target_pairs={{48,16},{80,48},{112,80},{144,112},{176,144},{208,176},{240,208},{... | collective-permute-start | bytes 196616 | tf_op jit(solution)/shard_map/ppermute | solution.py:366
  46.5 0.7 collective-permute-start.1
  47.2 2.4 %collective-permute-done.2 = bf16[128,256]{1,0:T(8,128)(2,1)S(1)} collective-permute-done((bf16[128,256]{1,0:T(8,128)(2,1)S(1)}, bf16[128,256]{1,0:T(8,128)(2,1)S(1)}, u32[]{:S(2)}, u32[]{:S(2)}) %collective-permute-start.2) | collective-permute-done | bytes 65568 | tf_op jit(solution)/shard_map/ppermute | solution.py:366
  49.7 0.6 collective-permute-done.1
  50.3 3.4 %collective-permute-start.3 = (bf16[2,128,256]{2,1,0:T(8,128)(2,1)S(1)}, bf16[2,128,256]{2,1,0:T(8,128)(2,1)S(1)}, u32[]{:S(2)}, u32[]{:S(2)}) collective-permute-start(bf16[2,128,256]{2,1,0:T(8,128)(2,1)S(1)} %pad_maximum_fusion.2), channel_id=1, source_target_pairs={{384,0},{144,16},{416,32},{176,48},{448,64},{208,80},{480,96},{240... | collective-permute-start | bytes 393224 | tf_op jit(solution)/shard_map/ppermute | solution.py:366
  53.7 9.4 %collective-permute-done.3 = bf16[2,128,256]{2,1,0:T(8,128)(2,1)S(1)} collective-permute-done((bf16[2,128,256]{2,1,0:T(8,128)(2,1)S(1)}, bf16[2,128,256]{2,1,0:T(8,128)(2,1)S(1)}, u32[]{:S(2)}, u32[]{:S(2)}) %collective-permute-start.3) | collective-permute-done | bytes 131104 | tf_op jit(solution)/shard_map/ppermute | solution.py:366
  63.2 1.9 %collective-permute-start.4 = (bf16[4,128,256]{2,1,0:T(8,128)(2,1)S(1)}, bf16[4,128,256]{2,1,0:T(8,128)(2,1)S(1)}, u32[]{:S(2)}, u32[]{:S(2)}) collective-permute-start(bf16[4,128,256]{2,1,0:T(8,128)(2,1)S(1)} %pad_maximum_fusion.1), channel_id=1, source_target_pairs={{448,0},{80,16},{480,32},{112,48},{0,64},{144,80},{32,96},{176,112... | collective-permute-start | bytes 786440 | tf_op jit(solution)/shard_map/ppermute | solution.py:366
  65.1 6.6 %collective-permute-done.4 = bf16[4,128,256]{2,1,0:T(8,128)(2,1)S(1)} collective-permute-done((bf16[4,128,256]{2,1,0:T(8,128)(2,1)S(1)}, bf16[4,128,256]{2,1,0:T(8,128)(2,1)S(1)}, u32[]{:S(2)}, u32[]{:S(2)}) %collective-permute-start.4) | collective-permute-done | bytes 262176 | tf_op jit(solution)/shard_map/ppermute | solution.py:366
  71.7 0.1 pad_maximum_fusion.keys_ref
  71.8 6.8 %collective-permute-start.5 = (bf16[8,128,256]{2,1,0:T(8,128)(2,1)S(1)}, bf16[8,128,256]{2,1,0:T(8,128)(2,1)}, u32[]{:S(2)}, u32[]{:S(2)}) collective-permute-start(bf16[8,128,256]{2,1,0:T(8,128)(2,1)S(1)} %pad_maximum_fusion.keys_ref), channel_id=1, source_target_pairs={{480,0},{48,16},{0,32},{80,48},{32,64},{112,80},{64,96},{144,112},... | collective-permute-start | bytes 1572872 | tf_op jit(solution)/shard_map/ppermute | solution.py:366
  78.6 0.0 copy-done
  78.6 2.5 %collective-permute-start = (bf16[128,128]{1,0:T(8,128)(2,1)S(1)}, bf16[128,128]{1,0:T(8,128)(2,1)S(1)}, u32[]{:S(2)}, u32[]{:S(2)}) collective-permute-start(bf16[128,128]{1,0:T(8,128)(2,1)S(1)} %bitcast.23), channel_id=1, source_target_pairs={{16,0},{0,16},{48,32},{32,48},{80,64},{64,80},{112,96},{96,112},{1... | collective-permute-start | bytes 98312 | tf_op jit(solution)/shard_map/ppermute | solution.py:366
  81.1 0.8 collective-permute-done.swapped_ref
  81.9 1.5 attend_early.1.refs_0_
  83.5 1.2 collective-permute-done.5.keys_ref
  84.7 3.0 %attend_late.1 = (f32[256,256]{1,0:T(8,128)S(1)}, f32[256,256]{1,0:T(8,128)S(1)}) custom-call(s32[1]{0:T(128)} %bitcast.8.z_ref, s32[1]{0:T(128)} %bitcast.9.core_ref, bf16[128,128]{1,0:T(8,128)(2,1)S(1)} %bitcast.25, bf16[128,128]{1,0:T(8,128)(2,1)S(1)} %collective-permute-done.swapped_ref, bf16[8,128,256]{2,1,0:T(8,128)(2,1)} %collective-permute-done.5.keys_ref, ...), custom_call_target="tpu_custom_call" | custom-call | tf_op jit(solution)/shard_map/attend_late/pallas_call | solution.py:320
  87.6 6.9 %collective-permute-start.6 = (f32[256,256]{1,0:T(8,128)S(1)}, f32[256,256]{1,0:T(8,128)S(1)}, u32[]{:S(2)}, u32[]{:S(2)}) collective-permute-start(f32[256,256]{1,0:T(8,128)S(1)} %get-tuple-element.9), channel_id=1, source_target_pairs={{16,0},{0,16},{48,32},{32,48},{80,64},{64,80},{112,96},{96,112},{1... | collective-permute-start | bytes 786440 | tf_op jit(solution)/shard_map/ppermute | solution.py:366
  95.2 0.5 collective-permute-done.6.other_ref
  95.7 0.0 copy-done.3
  95.7 1.7 project.1.proj_ref
  97.3 0.0 all-to-all-done.1.x_ref
  97.3 4.5 %ffn.1 = bf16[16,768,128]{2,1,0:T(8,128)(2,1)S(1)} custom-call(bf16[16,640,128]{2,1,0:T(8,128)(2,1)S(1)} %all-to-all-done.1.x_ref, bf16[2048,256]{1,0:T(8,128)(2,1)} %bitcast.30, bf16[2048,256]{1,0:T(8,128)(2,1)} %bitcast.31, bf16[256,2048]{1,0:T(8,128)(2,1)} %bitcast.32, bf16[16,128,128]{2,1,0:T(8,128)(2,1)S(1)} %project.1.proj_ref), custom_call_target="tpu_custom_call" | custom-call | tf_op jit(solution)/shard_map/ffn/pallas_call | solution.py:162
  101.9 45.3 %all_to_all.21.in_ref = bf16[16,768,128]{2,1,0:T(8,128)(2,1)S(1)} all-to-all(bf16[16,768,128]{2,1,0:T(8,128)(2,1)S(1)} %ffn.1), channel_id=1, replica_groups=mesh['z'=16,'core'=2,'y'=4,'x'=4] {'y','x'}, dimensions={0} | all-to-all | bytes 6291456 | tf_op jit(solution)/shard_map/all_to_all | solution.py:378
  147.2 0.0 copy-start.1
  147.2 0.0 copy-start.2
  147.2 1.0 reduce_terms.1
  148.2 6.1 %all-to-all-start.3 = ((bf16[160,4,128]{2,1,0:T(4,128)(2,1)}), bf16[160,4,128]{2,1,0:T(4,128)(2,1)S(1)}, u32[]{:S(2)}, u32[]{:S(2)}) async-start(bf16[160,4,128]{2,1,0:T(4,128)(2,1)} %bitcast.16), calls=%async_computation.3 | async-start | bytes 327680 | tf_op jit(solution)/shard_map/all_to_all | solution.py:378
  154.3 0.0 copy-done.1
  154.3 0.0 copy-done.2
  154.3 0.6 weigh.1
  154.9 16.5 %all-to-all-done.3 = bf16[160,4,128]{2,1,0:T(4,128)(2,1)S(1)} async-done(((bf16[160,4,128]{2,1,0:T(4,128)(2,1)}), bf16[160,4,128]{2,1,0:T(4,128)(2,1)S(1)}, u32[]{:S(2)}, u32[]{:S(2)}) %all-to-all-start.3) | async-done | bytes 163872 | tf_op jit(solution)/shard_map/all_to_all | solution.py:378
  171.4 0.9 combine.1
  (4 shorter events, 0.1 us)
Async XLA Ops:
  37.6 7.0 %copy-start.4 = (bf16[128,1,128]{2,0,1:T(8,128)(2,1)S(1)}, bf16[128,1,128]{2,0,1:T(8,128)(2,1)}, u32[]{:S(2)}) copy-start(bf16[128,1,128]{2,0,1:T(8,128)(2,1)} %param.15) | copy-start | bytes 98308
  37.6 7.0 %copy-start.5 = (bf16[128,1,128]{2,0,1:T(8,128)(2,1)S(1)}, bf16[128,1,128]{2,0,1:T(8,128)(2,1)}, u32[]{:S(2)}) copy-start(bf16[128,1,128]{2,0,1:T(8,128)(2,1)} %param.14) | copy-start | bytes 98308
  37.6 41.0 %copy-start = (bf16[128,1,128]{2,0,1:T(8,128)(2,1)S(1)}, bf16[128,1,128]{2,0,1:T(8,128)(2,1)}, u32[]{:S(2)}) copy-start(bf16[128,1,128]{2,0,1:T(8,128)(2,1)} %param.13) | copy-start | bytes 98308
  37.6 59.7 %all-to-all-start.1 = ((bf16[16,640,128]{2,1,0:T(8,128)(2,1)}), bf16[16,640,128]{2,1,0:T(8,128)(2,1)S(1)}, u32[]{:S(2)}, u32[]{:S(2)}) async-start(bf16[16,640,128]{2,1,0:T(8,128)(2,1)} %spread_rows.1), calls=%async_computation.1 | async-start | bytes 5242880 | tf_op jit(solution)/shard_map/all_to_all | solution.py:378
  44.5 51.1 %copy-start.3 = (f32[128]{0:T(128)S(1)}, f32[128]{0:T(128)}, u32[]{:S(2)}) copy-start(f32[128]{0:T(128)} %param.17) | copy-start | bytes 1540
  44.6 5.1 %collective-permute-start.2 = (bf16[128,256]{1,0:T(8,128)(2,1)S(1)}, bf16[128,256]{1,0:T(8,128)(2,1)S(1)}, u32[]{:S(2)}, u32[]{:S(2)}) collective-permute-start(bf16[128,256]{1,0:T(8,128)(2,1)S(1)} %pad_maximum_fusion.3), channel_id=1, source_target_pairs={{48,16},{80,48},{112,80},{144,112},{176,144},{208,176},{240,208},{... | collective-permute-start | bytes 196616 | tf_op jit(solution)/shard_map/ppermute | solution.py:366
  46.5 3.8 %collective-permute-start.1 = (bf16[128,256]{1,0:T(8,128)(2,1)S(1)}, bf16[128,256]{1,0:T(8,128)(2,1)S(1)}, u32[]{:S(2)}, u32[]{:S(2)}) collective-permute-start(bf16[128,256]{1,0:T(8,128)(2,1)S(1)} %pad_maximum_fusion.3), channel_id=1, source_target_pairs={{16,0},{32,16},{48,32},{64,48},{80,64},{96,80},{112,96},{128,112},... | collective-permute-start | bytes 196616 | tf_op jit(solution)/shard_map/ppermute | solution.py:366
  50.3 12.9 %collective-permute-start.3 = (bf16[2,128,256]{2,1,0:T(8,128)(2,1)S(1)}, bf16[2,128,256]{2,1,0:T(8,128)(2,1)S(1)}, u32[]{:S(2)}, u32[]{:S(2)}) collective-permute-start(bf16[2,128,256]{2,1,0:T(8,128)(2,1)S(1)} %pad_maximum_fusion.2), channel_id=1, source_target_pairs={{384,0},{144,16},{416,32},{176,48},{448,64},{208,80},{480,96},{240... | collective-permute-start | bytes 393224 | tf_op jit(solution)/shard_map/ppermute | solution.py:366
  63.2 8.5 %collective-permute-start.4 = (bf16[4,128,256]{2,1,0:T(8,128)(2,1)S(1)}, bf16[4,128,256]{2,1,0:T(8,128)(2,1)S(1)}, u32[]{:S(2)}, u32[]{:S(2)}) collective-permute-start(bf16[4,128,256]{2,1,0:T(8,128)(2,1)S(1)} %pad_maximum_fusion.1), channel_id=1, source_target_pairs={{448,0},{80,16},{480,32},{112,48},{0,64},{144,80},{32,96},{176,112... | collective-permute-start | bytes 786440 | tf_op jit(solution)/shard_map/ppermute | solution.py:366
  71.8 12.9 %collective-permute-start.5 = (bf16[8,128,256]{2,1,0:T(8,128)(2,1)S(1)}, bf16[8,128,256]{2,1,0:T(8,128)(2,1)}, u32[]{:S(2)}, u32[]{:S(2)}) collective-permute-start(bf16[8,128,256]{2,1,0:T(8,128)(2,1)S(1)} %pad_maximum_fusion.keys_ref), channel_id=1, source_target_pairs={{480,0},{48,16},{0,32},{80,48},{32,64},{112,80},{64,96},{144,112},... | collective-permute-start | bytes 1572872 | tf_op jit(solution)/shard_map/ppermute | solution.py:366
  78.6 3.4 %collective-permute-start = (bf16[128,128]{1,0:T(8,128)(2,1)S(1)}, bf16[128,128]{1,0:T(8,128)(2,1)S(1)}, u32[]{:S(2)}, u32[]{:S(2)}) collective-permute-start(bf16[128,128]{1,0:T(8,128)(2,1)S(1)} %bitcast.23), channel_id=1, source_target_pairs={{16,0},{0,16},{48,32},{32,48},{80,64},{64,80},{112,96},{96,112},{1... | collective-permute-start | bytes 98312 | tf_op jit(solution)/shard_map/ppermute | solution.py:366
  87.6 8.0 %collective-permute-start.6 = (f32[256,256]{1,0:T(8,128)S(1)}, f32[256,256]{1,0:T(8,128)S(1)}, u32[]{:S(2)}, u32[]{:S(2)}) collective-permute-start(f32[256,256]{1,0:T(8,128)S(1)} %get-tuple-element.9), channel_id=1, source_target_pairs={{16,0},{0,16},{48,32},{32,48},{80,64},{64,80},{112,96},{96,112},{1... | collective-permute-start | bytes 786440 | tf_op jit(solution)/shard_map/ppermute | solution.py:366
  147.2 7.1 %copy-start.1 = (s32[128,4]{0,1:T(4,128)S(1)}, s32[128,4]{0,1:T(4,128)}, u32[]{:S(2)}) copy-start(s32[128,4]{0,1:T(4,128)} %param.21) | copy-start | bytes 6148
  147.2 7.2 %copy-start.2 = (f32[128,4]{0,1:T(4,128)S(1)}, f32[128,4]{0,1:T(4,128)}, u32[]{:S(2)}) copy-start(f32[128,4]{0,1:T(4,128)} %param.22) | copy-start | bytes 6148
  148.2 23.2 %all-to-all-start.3 = ((bf16[160,4,128]{2,1,0:T(4,128)(2,1)}), bf16[160,4,128]{2,1,0:T(4,128)(2,1)S(1)}, u32[]{:S(2)}, u32[]{:S(2)}) async-start(bf16[160,4,128]{2,1,0:T(4,128)(2,1)} %bitcast.16), calls=%async_computation.3 | async-start | bytes 327680 | tf_op jit(solution)/shard_map/all_to_all | solution.py:378

commit v8 on v7

--- a/solution.py
+++ b/solution.py
@@ -356,22 +356,41 @@
     )(lam, own, other, gain, in_hbm(w))
 
 
-def moved(array, source):
-    pairs = []
-    for z in range(Z):
-        for core in range(CORE):
-            sender = source(z, core)
-            if sender is not None:
-                pairs.append((sender[0] % Z * CORE + sender[1], z * CORE + core))
-    return lax.ppermute(array, EP, pairs)
-
-
-def along(array, by):
-    return moved(array, lambda z, core: (z + by if core else z - by, core))
+def key_routes():
+    devices = [(z, core) for z in range(Z) for core in range(CORE)]
+    held = {(z, core): {(z + core) % Z} for z, core in devices}
+    stages = []
+    for by in (4, 2, 1):
+        sender = {(z, c): ((z + by if c else z - by) % Z, c) for z, c in devices}
+        stages.append((sender, held))
+        if by > 1:
+            held = {d: held[d] | held[sender[d]] for d in devices}
+    need = {d: {chip for chip in held[d] if chip <= d[0]} for d in devices}
+    routes = []
+    for n, (sender, before) in reversed(list(enumerate(stages))):
+        last = n == len(stages) - 1
+        earlier = {d: need[d] & before[d] for d in devices}
+        pairs = []
+        for d in devices:
+            used = before[sender[d]] & ({*range(d[0] + 1)} if last else need[d])
+            if used:
+                pairs.append((sender[d], d))
+                earlier[sender[d]] = earlier[sender[d]] | used
+        routes.insert(0, pairs)
+        need = earlier
+    first = [((z, 1), (z, 0)) for z in range(Z) if need[z, 0]]
+    first += [(((z + 1) % Z, 0), (z, 1)) for z in range(Z) if need[z, 1]]
+    second = [(((z + 1) % Z, 1), (z, 1)) for z in range(Z) if need[z, 1]]
+    return [first, second, *routes]
+
+
+def moved(array, pairs):
+    flat = [(a[0] * CORE + a[1], b[0] * CORE + b[1]) for a, b in pairs]
+    return lax.ppermute(array, EP, flat)
 
 
 def across(array):
-    return moved(array, lambda z, core: (z, 1 - core))
+    return moved(array, [((z, 1 - core), (z, core)) for z in range(Z) for core in range(CORE)])
 
 
 def exchanged(array, axes):
@@ -383,13 +402,14 @@
 
 
 def collect_keys(keys, values, core_at):
+    routes = key_routes()
     mine = jnp.concatenate([keys, values], axis=-1)
-    first = moved(mine, lambda z, core: (z + 1, 0) if core else (z, 1))
-    second = moved(mine, lambda z, core: (z + 1, 1) if core else None)
+    first = moved(mine, routes[0])
+    second = moved(mine, routes[1])
     held = jnp.stack([first, jnp.where(core_at == 0, mine, second)])
-    held = jnp.concatenate([held, along(held, 4)], axis=0)
-    held = jnp.concatenate([held, along(held, 2)], axis=0)
-    return held, along(held, 1)
+    held = jnp.concatenate([held, moved(held, routes[2])], axis=0)
+    held = jnp.concatenate([held, moved(held, routes[3])], axis=0)
+    return held, moved(held, routes[4])
 
 
 def body(

time: 173 us -> 173 us (level)
  starting transfers between devices: 37.2 us -> 35.1 us
    ppermute x7, starting transfers between devices: 24.2 us -> 19.8 us  [moved(): return lax.ppermute(array, EP, flat)]
    all_to_all x2, starting transfers between devices: 13 us -> 15.3 us  [exchanged(): return lax.all_to_all(array, axes, split_axis=0, concat_axis=0, tiled=True)]
where the time goes in v8:
time: 173 us; the launch traced here: 172 us
  blocking collectives  79.3 us (46%)
  waiting for transfers between devices  39.4 us (23%)
  starting transfers between devices  35.1 us (20%)
  Pallas kernels  16.4 us (9%)
    all_to_all x2, blocking collectives, exchanged(): return lax.all_to_all(array, axes, split_axis=0, concat_axis=0, tiled=True)  79.3 us
    ppermute x7, waiting for transfers between devices, moved(): return lax.ppermute(array, EP, flat)  22.9 us
    ppermute x7, starting transfers between devices, moved(): return lax.ppermute(array, EP, flat)  19.8 us
    all_to_all x2, waiting for transfers between devices, exchanged(): return lax.all_to_all(array, axes, split_axis=0, concat_axis=0, tiled=True)  16.5 us
    all_to_all x2, starting transfers between devices, exchanged(): return lax.all_to_all(array, axes, split_axis=0, concat_axis=0, tiled=True)  15.3 us
    pallas_call x1, Pallas kernels, ffn(): pl.pallas_call(ffn_kernel, out_shape=pltpu.VMEM((N_TP, OUT_ROWS, WIDE), B...  4.53 us
    pallas_call x2, Pallas kernels, attend(): pl.pallas_call(functools.partial(attend_kernel, late), out_shape=tuple((j...  4.49 us
  transfers between devices with their start and end apart: 9, of which 8 were waited for; matrix products, arithmetic and copies ran while one was open for 0% of the time, Pallas kernels for 4%

profile of v8, /device:TPU:1, one launch (start us, length us, event | category | flops | bytes accessed | tf_op | source)
XLA Modules:
  0.0 172.0 jit_solution(1090997279247364357)
XLA Ops:
  0.6 1.6 dispatch.1
  2.3 33.7 %all_to_all.20 = bf16[160,4,128]{2,1,0:T(4,128)(2,1)S(1)} all-to-all(bf16[160,4,128]{2,1,0:T(4,128)(2,1)S(1)} %bitcast.20), channel_id=1, replica_groups=mesh['z'=16,'core'=2,'y'=4,'x'=4] {'z','core'}, dimensions={0} | all-to-all | bytes 327680 | tf_op jit(solution)/shard_map/all_to_all | solution.py:397
  35.9 1.6 spread_rows.1
  37.6 0.0 copy-start.4
  37.6 0.0 copy-start.5
  37.6 0.0 copy-start
  37.6 6.9 %all-to-all-start.1 = ((bf16[16,640,128]{2,1,0:T(8,128)(2,1)}), bf16[16,640,128]{2,1,0:T(8,128)(2,1)S(1)}, u32[]{:S(2)}, u32[]{:S(2)}) async-start(bf16[16,640,128]{2,1,0:T(8,128)(2,1)} %spread_rows.1), calls=%async_computation.1 | async-start | bytes 5242880 | tf_op jit(solution)/shard_map/all_to_all | solution.py:397
  44.5 0.0 copy-start.3
  44.5 0.0 copy-done.4
  44.5 0.0 copy-done.5
  44.6 1.9 %collective-permute-start.2 = (bf16[128,256]{1,0:T(8,128)(2,1)S(1)}, bf16[128,256]{1,0:T(8,128)(2,1)S(1)}, u32[]{:S(2)}, u32[]{:S(2)}) collective-permute-start(bf16[128,256]{1,0:T(8,128)(2,1)S(1)} %pad_maximum_fusion.3), channel_id=1, source_target_pairs={{48,16},{80,48},{112,80},{144,112},{176,144},{208,176},{240,208},{... | collective-permute-start | bytes 196616 | tf_op jit(solution)/shard_map/ppermute | solution.py:389
  46.5 2.6 %collective-permute-start.1 = (bf16[128,256]{1,0:T(8,128)(2,1)S(1)}, bf16[128,256]{1,0:T(8,128)(2,1)S(1)}, u32[]{:S(2)}, u32[]{:S(2)}) collective-permute-start(bf16[128,256]{1,0:T(8,128)(2,1)S(1)} %pad_maximum_fusion.3), channel_id=1, source_target_pairs={{16,0},{48,32},{80,64},{112,96},{144,128},{176,160},{208,192},{240... | collective-permute-start | bytes 196616 | tf_op jit(solution)/shard_map/ppermute | solution.py:389
  49.1 0.4 collective-permute-done.2
  49.6 2.8 %collective-permute-done.1 = bf16[128,256]{1,0:T(8,128)(2,1)S(1)} collective-permute-done((bf16[128,256]{1,0:T(8,128)(2,1)S(1)}, bf16[128,256]{1,0:T(8,128)(2,1)S(1)}, u32[]{:S(2)}, u32[]{:S(2)}) %collective-permute-start.1) | collective-permute-done | bytes 65568 | tf_op jit(solution)/shard_map/ppermute | solution.py:389
  52.4 1.9 %collective-permute-start.3 = (bf16[2,128,256]{2,1,0:T(8,128)(2,1)S(1)}, bf16[2,128,256]{2,1,0:T(8,128)(2,1)S(1)}, u32[]{:S(2)}, u32[]{:S(2)}) collective-permute-start(bf16[2,128,256]{2,1,0:T(8,128)(2,1)S(1)} %pad_maximum_fusion.2), channel_id=1, source_target_pairs={{144,16},{176,48},{208,80},{0,128},{32,160},{64,192},{96,224},{128... | collective-permute-start | bytes 393224 | tf_op jit(solution)/shard_map/ppermute | solution.py:389
  54.3 10.6 %collective-permute-done.3 = bf16[2,128,256]{2,1,0:T(8,128)(2,1)S(1)} collective-permute-done((bf16[2,128,256]{2,1,0:T(8,128)(2,1)S(1)}, bf16[2,128,256]{2,1,0:T(8,128)(2,1)S(1)}, u32[]{:S(2)}, u32[]{:S(2)}) %collective-permute-start.3) | collective-permute-done | bytes 131104 | tf_op jit(solution)/shard_map/ppermute | solution.py:389
  65.0 1.9 %collective-permute-start.4 = (bf16[4,128,256]{2,1,0:T(8,128)(2,1)S(1)}, bf16[4,128,256]{2,1,0:T(8,128)(2,1)S(1)}, u32[]{:S(2)}, u32[]{:S(2)}) collective-permute-start(bf16[4,128,256]{2,1,0:T(8,128)(2,1)S(1)} %pad_maximum_fusion.1), channel_id=1, source_target_pairs={{80,16},{0,64},{32,96},{64,128},{96,160},{128,192},{160,224},{192,... | collective-permute-start | bytes 786440 | tf_op jit(solution)/shard_map/ppermute | solution.py:389
  66.9 6.4 %collective-permute-done.4 = bf16[4,128,256]{2,1,0:T(8,128)(2,1)S(1)} collective-permute-done((bf16[4,128,256]{2,1,0:T(8,128)(2,1)S(1)}, bf16[4,128,256]{2,1,0:T(8,128)(2,1)S(1)}, u32[]{:S(2)}, u32[]{:S(2)}) %collective-permute-start.4) | collective-permute-done | bytes 262176 | tf_op jit(solution)/shard_map/ppermute | solution.py:389
  73.3 0.1 pad_maximum_fusion.keys_ref
  73.3 7.6 %collective-permute-start.5 = (bf16[8,128,256]{2,1,0:T(8,128)(2,1)S(1)}, bf16[8,128,256]{2,1,0:T(8,128)(2,1)}, u32[]{:S(2)}, u32[]{:S(2)}) collective-permute-start(bf16[8,128,256]{2,1,0:T(8,128)(2,1)S(1)} %pad_maximum_fusion.keys_ref), channel_id=1, source_target_pairs={{0,32},{32,64},{64,96},{96,128},{128,160},{160,192},{192,224},{224... | collective-permute-start | bytes 1572872 | tf_op jit(solution)/shard_map/ppermute | solution.py:389
  80.9 0.0 copy-done
  81.0 1.9 %collective-permute-start = (bf16[128,128]{1,0:T(8,128)(2,1)S(1)}, bf16[128,128]{1,0:T(8,128)(2,1)S(1)}, u32[]{:S(2)}, u32[]{:S(2)}) collective-permute-start(bf16[128,128]{1,0:T(8,128)(2,1)S(1)} %bitcast.23), channel_id=1, source_target_pairs={{16,0},{0,16},{48,32},{32,48},{80,64},{64,80},{112,96},{96,112},{1... | collective-permute-start | bytes 98312 | tf_op jit(solution)/shard_map/ppermute | solution.py:389
  82.9 1.2 collective-permute-done.swapped_ref
  84.0 1.5 attend_early.1.refs_0_
  85.6 0.7 collective-permute-done.5.keys_ref
  86.3 3.0 %attend_late.1 = (f32[256,256]{1,0:T(8,128)S(1)}, f32[256,256]{1,0:T(8,128)S(1)}) custom-call(s32[1]{0:T(128)} %bitcast.8.z_ref, s32[1]{0:T(128)} %bitcast.9.core_ref, bf16[128,128]{1,0:T(8,128)(2,1)S(1)} %bitcast.25, bf16[128,128]{1,0:T(8,128)(2,1)S(1)} %collective-permute-done.swapped_ref, bf16[8,128,256]{2,1,0:T(8,128)(2,1)} %collective-permute-done.5.keys_ref, ...), custom_call_target="tpu_custom_call" | custom-call | tf_op jit(solution)/shard_map/attend_late/pallas_call | solution.py:320
  89.2 1.9 %collective-permute-start.6 = (f32[256,256]{1,0:T(8,128)S(1)}, f32[256,256]{1,0:T(8,128)S(1)}, u32[]{:S(2)}, u32[]{:S(2)}) collective-permute-start(f32[256,256]{1,0:T(8,128)S(1)} %get-tuple-element.9), channel_id=1, source_target_pairs={{16,0},{0,16},{48,32},{32,48},{80,64},{64,80},{112,96},{96,112},{1... | collective-permute-start | bytes 786440 | tf_op jit(solution)/shard_map/ppermute | solution.py:389
  91.8 0.9 collective-permute-done.6.other_ref
  92.7 0.0 copy-done.3
  92.7 1.7 project.1.proj_ref
  94.3 0.0 all-to-all-done.1.x_ref
  94.3 4.5 %ffn.1 = bf16[16,768,128]{2,1,0:T(8,128)(2,1)S(1)} custom-call(bf16[16,640,128]{2,1,0:T(8,128)(2,1)S(1)} %all-to-all-done.1.x_ref, bf16[2048,256]{1,0:T(8,128)(2,1)} %bitcast.30, bf16[2048,256]{1,0:T(8,128)(2,1)} %bitcast.31, bf16[256,2048]{1,0:T(8,128)(2,1)} %bitcast.32, bf16[16,128,128]{2,1,0:T(8,128)(2,1)S(1)} %project.1.proj_ref), custom_call_target="tpu_custom_call" | custom-call | tf_op jit(solution)/shard_map/ffn/pallas_call | solution.py:162
  98.9 45.7 %all_to_all.21.in_ref = bf16[16,768,128]{2,1,0:T(8,128)(2,1)S(1)} all-to-all(bf16[16,768,128]{2,1,0:T(8,128)(2,1)S(1)} %ffn.1), channel_id=1, replica_groups=mesh['z'=16,'core'=2,'y'=4,'x'=4] {'y','x'}, dimensions={0} | all-to-all | bytes 6291456 | tf_op jit(solution)/shard_map/all_to_all | solution.py:397
  144.6 0.0 copy-start.1
  144.6 0.0 copy-start.2
  144.6 1.0 reduce_terms.1
  145.6 8.4 %all-to-all-start.3 = ((bf16[160,4,128]{2,1,0:T(4,128)(2,1)}), bf16[160,4,128]{2,1,0:T(4,128)(2,1)S(1)}, u32[]{:S(2)}, u32[]{:S(2)}) async-start(bf16[160,4,128]{2,1,0:T(4,128)(2,1)} %bitcast.16), calls=%async_computation.3 | async-start | bytes 327680 | tf_op jit(solution)/shard_map/all_to_all | solution.py:397
  154.0 0.0 copy-done.1
  154.0 0.0 copy-done.2
  154.0 0.6 weigh.1
  154.6 16.5 %all-to-all-done.3 = bf16[160,4,128]{2,1,0:T(4,128)(2,1)S(1)} async-done(((bf16[160,4,128]{2,1,0:T(4,128)(2,1)}), bf16[160,4,128]{2,1,0:T(4,128)(2,1)S(1)}, u32[]{:S(2)}, u32[]{:S(2)}) %all-to-all-start.3) | async-done | bytes 163872 | tf_op jit(solution)/shard_map/all_to_all | solution.py:397
  171.1 0.9 combine.1
  (4 shorter events, 0.1 us)
Async XLA Ops:
  37.6 7.0 %copy-start.4 = (bf16[128,1,128]{2,0,1:T(8,128)(2,1)S(1)}, bf16[128,1,128]{2,0,1:T(8,128)(2,1)}, u32[]{:S(2)}) copy-start(bf16[128,1,128]{2,0,1:T(8,128)(2,1)} %param.15) | copy-start | bytes 98308
  37.6 7.0 %copy-start.5 = (bf16[128,1,128]{2,0,1:T(8,128)(2,1)S(1)}, bf16[128,1,128]{2,0,1:T(8,128)(2,1)}, u32[]{:S(2)}) copy-start(bf16[128,1,128]{2,0,1:T(8,128)(2,1)} %param.14) | copy-start | bytes 98308
  37.6 43.3 %copy-start = (bf16[128,1,128]{2,0,1:T(8,128)(2,1)S(1)}, bf16[128,1,128]{2,0,1:T(8,128)(2,1)}, u32[]{:S(2)}) copy-start(bf16[128,1,128]{2,0,1:T(8,128)(2,1)} %param.13) | copy-start | bytes 98308
  37.6 56.7 %all-to-all-start.1 = ((bf16[16,640,128]{2,1,0:T(8,128)(2,1)}), bf16[16,640,128]{2,1,0:T(8,128)(2,1)S(1)}, u32[]{:S(2)}, u32[]{:S(2)}) async-start(bf16[16,640,128]{2,1,0:T(8,128)(2,1)} %spread_rows.1), calls=%async_computation.1 | async-start | bytes 5242880 | tf_op jit(solution)/shard_map/all_to_all | solution.py:397
  44.5 48.1 %copy-start.3 = (f32[128]{0:T(128)S(1)}, f32[128]{0:T(128)}, u32[]{:S(2)}) copy-start(f32[128]{0:T(128)} %param.17) | copy-start | bytes 1540
  44.6 5.0 %collective-permute-start.2 = (bf16[128,256]{1,0:T(8,128)(2,1)S(1)}, bf16[128,256]{1,0:T(8,128)(2,1)S(1)}, u32[]{:S(2)}, u32[]{:S(2)}) collective-permute-start(bf16[128,256]{1,0:T(8,128)(2,1)S(1)} %pad_maximum_fusion.3), channel_id=1, source_target_pairs={{48,16},{80,48},{112,80},{144,112},{176,144},{208,176},{240,208},{... | collective-permute-start | bytes 196616 | tf_op jit(solution)/shard_map/ppermute | solution.py:389
  46.5 5.9 %collective-permute-start.1 = (bf16[128,256]{1,0:T(8,128)(2,1)S(1)}, bf16[128,256]{1,0:T(8,128)(2,1)S(1)}, u32[]{:S(2)}, u32[]{:S(2)}) collective-permute-start(bf16[128,256]{1,0:T(8,128)(2,1)S(1)} %pad_maximum_fusion.3), channel_id=1, source_target_pairs={{16,0},{48,32},{80,64},{112,96},{144,128},{176,160},{208,192},{240... | collective-permute-start | bytes 196616 | tf_op jit(solution)/shard_map/ppermute | solution.py:389
  52.4 12.5 %collective-permute-start.3 = (bf16[2,128,256]{2,1,0:T(8,128)(2,1)S(1)}, bf16[2,128,256]{2,1,0:T(8,128)(2,1)S(1)}, u32[]{:S(2)}, u32[]{:S(2)}) collective-permute-start(bf16[2,128,256]{2,1,0:T(8,128)(2,1)S(1)} %pad_maximum_fusion.2), channel_id=1, source_target_pairs={{144,16},{176,48},{208,80},{0,128},{32,160},{64,192},{96,224},{128... | collective-permute-start | bytes 393224 | tf_op jit(solution)/shard_map/ppermute | solution.py:389
  65.0 8.3 %collective-permute-start.4 = (bf16[4,128,256]{2,1,0:T(8,128)(2,1)S(1)}, bf16[4,128,256]{2,1,0:T(8,128)(2,1)S(1)}, u32[]{:S(2)}, u32[]{:S(2)}) collective-permute-start(bf16[4,128,256]{2,1,0:T(8,128)(2,1)S(1)} %pad_maximum_fusion.1), channel_id=1, source_target_pairs={{80,16},{0,64},{32,96},{64,128},{96,160},{128,192},{160,224},{192,... | collective-permute-start | bytes 786440 | tf_op jit(solution)/shard_map/ppermute | solution.py:389
  73.3 12.9 %collective-permute-start.5 = (bf16[8,128,256]{2,1,0:T(8,128)(2,1)S(1)}, bf16[8,128,256]{2,1,0:T(8,128)(2,1)}, u32[]{:S(2)}, u32[]{:S(2)}) collective-permute-start(bf16[8,128,256]{2,1,0:T(8,128)(2,1)S(1)} %pad_maximum_fusion.keys_ref), channel_id=1, source_target_pairs={{0,32},{32,64},{64,96},{96,128},{128,160},{160,192},{192,224},{224... | collective-permute-start | bytes 1572872 | tf_op jit(solution)/shard_map/ppermute | solution.py:389
  81.0 3.1 %collective-permute-start = (bf16[128,128]{1,0:T(8,128)(2,1)S(1)}, bf16[128,128]{1,0:T(8,128)(2,1)S(1)}, u32[]{:S(2)}, u32[]{:S(2)}) collective-permute-start(bf16[128,128]{1,0:T(8,128)(2,1)S(1)} %bitcast.23), channel_id=1, source_target_pairs={{16,0},{0,16},{48,32},{32,48},{80,64},{64,80},{112,96},{96,112},{1... | collective-permute-start | bytes 98312 | tf_op jit(solution)/shard_map/ppermute | solution.py:389
  89.2 3.4 %collective-permute-start.6 = (f32[256,256]{1,0:T(8,128)S(1)}, f32[256,256]{1,0:T(8,128)S(1)}, u32[]{:S(2)}, u32[]{:S(2)}) collective-permute-start(f32[256,256]{1,0:T(8,128)S(1)} %get-tuple-element.9), channel_id=1, source_target_pairs={{16,0},{0,16},{48,32},{32,48},{80,64},{64,80},{112,96},{96,112},{1... | collective-permute-start | bytes 786440 | tf_op jit(solution)/shard_map/ppermute | solution.py:389
  144.6 9.5 %copy-start.1 = (s32[128,4]{0,1:T(4,128)S(1)}, s32[128,4]{0,1:T(4,128)}, u32[]{:S(2)}) copy-start(s32[128,4]{0,1:T(4,128)} %param.21) | copy-start | bytes 6148
  144.6 9.5 %copy-start.2 = (f32[128,4]{0,1:T(4,128)S(1)}, f32[128,4]{0,1:T(4,128)}, u32[]{:S(2)}) copy-start(f32[128,4]{0,1:T(4,128)} %param.22) | copy-start | bytes 6148
  145.6 25.6 %all-to-all-start.3 = ((bf16[160,4,128]{2,1,0:T(4,128)(2,1)}), bf16[160,4,128]{2,1,0:T(4,128)(2,1)S(1)}, u32[]{:S(2)}, u32[]{:S(2)}) async-start(bf16[160,4,128]{2,1,0:T(4,128)(2,1)} %bitcast.16), calls=%async_computation.3 | async-start | bytes 327680 | tf_op jit(solution)/shard_map/all_to_all | solution.py:397

commit v9 on v8

--- a/solution.py
+++ b/solution.py
@@ -75,33 +75,41 @@
     return jnp.where(spread[0] == place, value, 0.0)
 
 
-def dispatch_kernel(at_ref, rows_ref, part_ref, gain_ref, ids_ref, out_ref):
+def dispatch_kernel(at_ref, ids_ref, rows_hbm, gain_hbm, out_ref, rows_ref, part_ref, gain_ref, sems):
+    low = pl.multiple_of(at_ref[0] * WIDE, WIDE)
+    copies = [
+        pltpu.make_async_copy(rows_hbm, rows_ref, sems.at[0]),
+        pltpu.make_async_copy(rows_hbm.at[:, pl.ds(low, WIDE)], part_ref, sems.at[1]),
+        pltpu.make_async_copy(gain_hbm.at[:, pl.ds(low, WIDE)], gain_ref, sems.at[2]),
+    ]
+    for copy in copies:
+        copy.start()
+    chosen = routing(ids_ref[...]).astype(BF16)
+    for copy in copies:
+        copy.wait()
     rows = rows_ref[...].astype(F32)
     mean_sq = jnp.mean(rows * rows, axis=-1, keepdims=True)
     part = part_ref[...].astype(F32) * lax.rsqrt(mean_sq + NORM_EPS) * gain_ref[...]
-    chosen = routing(ids_ref[...]).astype(BF16)
-    packed = jnp.dot(chosen, part.astype(BF16), preferred_element_type=F32)
-    out_ref[...] = packed.astype(BF16)
+    out_ref[...] = jnp.dot(chosen, part.astype(BF16), preferred_element_type=F32).astype(BF16)
 
 
 def dispatch(at, token_rows, gain, ids):
+    vmem = pl.BlockSpec(memory_space=pltpu.VMEM)
+    hbm = pl.BlockSpec(memory_space=pl.ANY)
     return pl.pallas_call(
         dispatch_kernel,
         out_shape=jax.ShapeDtypeStruct((ROWS, WIDE), BF16),
-        grid_spec=pltpu.PrefetchScalarGridSpec(
-            num_scalar_prefetch=1,
-            grid=(1,),
-            in_specs=[
-                pl.BlockSpec((TOK, MODEL), lambda i, at: (0, 0)),
-                pl.BlockSpec((TOK, WIDE), lambda i, at: (0, at[0])),
-                pl.BlockSpec((1, WIDE), lambda i, at: (0, at[0])),
-                pl.BlockSpec((4, TOK), lambda i, at: (0, 0)),
-            ],
-            out_specs=pl.BlockSpec((ROWS, WIDE), lambda i, at: (0, 0)),
-        ),
+        in_specs=[pl.BlockSpec(memory_space=pltpu.SMEM), vmem, hbm, hbm],
+        out_specs=vmem,
+        scratch_shapes=[
+            pltpu.VMEM((TOK, MODEL), BF16),
+            pltpu.VMEM((TOK, WIDE), BF16),
+            pltpu.VMEM((1, WIDE), F32),
+            pltpu.SemaphoreType.DMA((3,)),
+        ],
         compiler_params=params(8),
         name="dispatch",
-    )(at, *(in_hbm(a) for a in (token_rows, token_rows, gain, ids)))
+    )(at, *(in_hbm(a) for a in (ids, token_rows, gain)))
 
 
 def spread_kernel(in_ref, out_hbm, sems):
@@ -126,34 +134,54 @@
     )(in_vmem(rows))
 
 
-FFN_ROWS = ROWS // 2
-
-
-def ffn_kernel(x_ref, wg_hbm, wu_hbm, wd_hbm, proj_ref, out_ref, wg_ref, wu_ref, wd_ref, sems):
+def spread_kernel(in_ref, out_hbm, sems):
+    copies = [
+        pltpu.make_async_copy(in_ref, out_hbm.at[t], sems.at[t]) for t in range(N_TP)
+    ]
+    for copy in copies:
+        copy.start()
+    for copy in copies:
+        copy.wait()
+
+
+def spread_rows(rows):
+    return pl.pallas_call(
+        spread_kernel,
+        out_shape=pltpu.HBM((N_TP, ROWS, WIDE), BF16),
+        in_specs=[pl.BlockSpec(memory_space=pltpu.VMEM)],
+        out_specs=pl.BlockSpec(memory_space=pl.ANY),
+        scratch_shapes=[pltpu.SemaphoreType.DMA((N_TP,))],
+        compiler_params=params(4),
+        name="spread_rows",
+    )(in_vmem(rows))
+
+
+DOWN_COLS = 4 * WIDE
+
+
+def ffn_kernel(x_ref, wg_hbm, wu_hbm, wd_hbm, proj_ref, out_ref, pair_ref, wd_ref, sems):
+    units = wg_hbm.shape[1]
     loads = [
-        pltpu.make_async_copy(src, dst, sems.at[n])
-        for n, (src, dst) in enumerate(((wg_hbm, wg_ref), (wu_hbm, wu_ref), (wd_hbm, wd_ref)))
+        pltpu.make_async_copy(wg_hbm, pair_ref.at[:, pl.ds(0, units)], sems.at[0]),
+        pltpu.make_async_copy(wu_hbm, pair_ref.at[:, pl.ds(units, units)], sems.at[1]),
+        pltpu.make_async_copy(wd_hbm, wd_ref, sems.at[2]),
     ]
     for load in loads:
         load.start()
     out_ref[:, ROWS:, :] = proj_ref[...]
-    for low in range(0, ROWS, FFN_ROWS):
-        here = slice(low, low + FFN_ROWS)
-        rows = jnp.concatenate([x_ref[t, here, :] for t in range(N_TP)], axis=-1)
-        if low == 0:
-            loads[0].wait()
-        gate = jnp.dot(rows, wg_ref[...], preferred_element_type=F32)
-        if low == 0:
-            loads[1].wait()
-        up = jnp.dot(rows, wu_ref[...], preferred_element_type=F32)
-        gated = jnp.minimum(gate, CLAMP_LIMIT)
-        clipped = jnp.clip(up, -CLAMP_LIMIT, CLAMP_LIMIT)
-        active = ((clipped + 1.0) * gated * jax.nn.sigmoid(GATE_SLOPE * gated)).astype(BF16)
-        if low == 0:
-            loads[2].wait()
-        terms = jnp.dot(active, wd_ref[...], preferred_element_type=F32).astype(BF16)
-        for t in range(N_TP):
-            out_ref[t, here, :] = terms[:, t * WIDE : (t + 1) * WIDE]
+    rows = jnp.concatenate([x_ref[t] for t in range(N_TP)], axis=-1)
+    loads[0].wait()
+    loads[1].wait()
+    both = jnp.dot(rows, pair_ref[...], preferred_element_type=F32)
+    gated = jnp.minimum(both[:, :units], CLAMP_LIMIT)
+    clipped = jnp.clip(both[:, units:], -CLAMP_LIMIT, CLAMP_LIMIT)
+    active = ((clipped + 1.0) * gated * jax.nn.sigmoid(GATE_SLOPE * gated)).astype(BF16)
+    loads[2].wait()
+    for low in range(0, MODEL, DOWN_COLS):
+        terms = jnp.dot(active, wd_ref[:, low : low + DOWN_COLS], preferred_element_type=F32)
+        for t in range(DOWN_COLS // WIDE):
+            part = terms[:, t * WIDE : (t + 1) * WIDE].astype(BF16)
+            out_ref[low // WIDE + t, :ROWS, :] = part
 
 
 def ffn(x, wg, wu, wd, proj):
@@ -165,18 +193,13 @@
         in_specs=[vmem, hbm, hbm, hbm, vmem],
         out_specs=vmem,
         scratch_shapes=[
-            pltpu.VMEM(wg.shape, BF16),
-            pltpu.VMEM(wu.shape, BF16),
+            pltpu.VMEM((MODEL, 2 * wg.shape[1]), BF16),
             pltpu.VMEM(wd.shape, BF16),
             pltpu.SemaphoreType.DMA((3,)),
         ],
         compiler_params=params(16),
         name="ffn",
-    )(
-        in_vmem(x),
-        *(in_hbm(w) for w in (wg, wu, wd)),
-        in_vmem(proj),
-    )
+    )(in_vmem(x), *(in_hbm(w) for w in (wg, wu, wd)), in_vmem(proj))
 
 
 SUM_ROWS = 32

time: 173 us -> 173 us (level)
  no operation moved by 1% of the time
where the time goes in v9:
time: 173 us; the launch traced here: 172 us
  blocking collectives  79.4 us (46%)
  waiting for transfers between devices  39.4 us (23%)
  starting transfers between devices  35.1 us (20%)
  Pallas kernels  16.4 us (9%)
    all_to_all x2, blocking collectives, exchanged(): return lax.all_to_all(array, axes, split_axis=0, concat_axis=0, tiled=True)  79.4 us
    ppermute x7, waiting for transfers between devices, moved(): return lax.ppermute(array, EP, flat)  22.9 us
    ppermute x7, starting transfers between devices, moved(): return lax.ppermute(array, EP, flat)  19.8 us
    all_to_all x2, waiting for transfers between devices, exchanged(): return lax.all_to_all(array, axes, split_axis=0, concat_axis=0, tiled=True)  16.5 us
    all_to_all x2, starting transfers between devices, exchanged(): return lax.all_to_all(array, axes, split_axis=0, concat_axis=0, tiled=True)  15.3 us
    pallas_call x2, Pallas kernels, attend(): pl.pallas_call(functools.partial(attend_kernel, late), out_shape=tuple((j...  4.49 us
    pallas_call x1, Pallas kernels, ffn(): pl.pallas_call(ffn_kernel, out_shape=pltpu.VMEM((N_TP, OUT_ROWS, WIDE), B...  3.96 us
  transfers between devices with their start and end apart: 9, of which 8 were waited for; matrix products, arithmetic and copies ran while one was open for 0% of the time, Pallas kernels for 4%

profile of v9, /device:TPU:1, one launch (start us, length us, event | category | flops | bytes accessed | tf_op | source)
XLA Modules:
  0.0 171.9 jit_solution(6602289684687997337)
XLA Ops:
  0.6 2.1 %dispatch.1 = bf16[640,128]{1,0:T(8,128)(2,1)S(1)} custom-call(s32[1]{0:T(128)} %bitcast.at_ref, s32[4,128]{1,0:T(4,128)} %bitcast.26, bf16[128,2048]{1,0:T(8,128)(2,1)} %rows_hbm.1, f32[1,2048]{1,0:T(1,128)} %bitcast.40), custom_call_target="tpu_custom_call" | custom-call | tf_op jit(solution)/shard_map/dispatch/pallas_call | solution.py:99
  2.8 33.7 %all_to_all.20 = bf16[160,4,128]{2,1,0:T(4,128)(2,1)S(1)} all-to-all(bf16[160,4,128]{2,1,0:T(4,128)(2,1)S(1)} %bitcast.21), channel_id=1, replica_groups=mesh['z'=16,'core'=2,'y'=4,'x'=4] {'z','core'}, dimensions={0} | all-to-all | bytes 327680 | tf_op jit(solution)/shard_map/all_to_all | solution.py:420
  36.5 1.6 spread_rows.1
  38.1 0.0 copy-start.4
  38.1 0.0 copy-start.5
  38.1 0.0 copy-start
  38.1 6.9 %all-to-all-start.1 = ((bf16[16,640,128]{2,1,0:T(8,128)(2,1)}), bf16[16,640,128]{2,1,0:T(8,128)(2,1)S(1)}, u32[]{:S(2)}, u32[]{:S(2)}) async-start(bf16[16,640,128]{2,1,0:T(8,128)(2,1)} %spread_rows.1), calls=%async_computation.1 | async-start | bytes 5242880 | tf_op jit(solution)/shard_map/all_to_all | solution.py:420
  45.0 0.0 copy-start.3
  45.1 0.0 copy-done.4
  45.1 0.0 copy-done.5
  45.1 1.9 %collective-permute-start.2 = (bf16[128,256]{1,0:T(8,128)(2,1)S(1)}, bf16[128,256]{1,0:T(8,128)(2,1)S(1)}, u32[]{:S(2)}, u32[]{:S(2)}) collective-permute-start(bf16[128,256]{1,0:T(8,128)(2,1)S(1)} %pad_maximum_fusion.3), channel_id=1, source_target_pairs={{48,16},{80,48},{112,80},{144,112},{176,144},{208,176},{240,208},{... | collective-permute-start | bytes 196616 | tf_op jit(solution)/shard_map/ppermute | solution.py:412
  47.0 2.6 %collective-permute-start.1 = (bf16[128,256]{1,0:T(8,128)(2,1)S(1)}, bf16[128,256]{1,0:T(8,128)(2,1)S(1)}, u32[]{:S(2)}, u32[]{:S(2)}) collective-permute-start(bf16[128,256]{1,0:T(8,128)(2,1)S(1)} %pad_maximum_fusion.3), channel_id=1, source_target_pairs={{16,0},{48,32},{80,64},{112,96},{144,128},{176,160},{208,192},{240... | collective-permute-start | bytes 196616 | tf_op jit(solution)/shard_map/ppermute | solution.py:412
  49.7 0.4 collective-permute-done.2
  50.1 2.8 %collective-permute-done.1 = bf16[128,256]{1,0:T(8,128)(2,1)S(1)} collective-permute-done((bf16[128,256]{1,0:T(8,128)(2,1)S(1)}, bf16[128,256]{1,0:T(8,128)(2,1)S(1)}, u32[]{:S(2)}, u32[]{:S(2)}) %collective-permute-start.1) | collective-permute-done | bytes 65568 | tf_op jit(solution)/shard_map/ppermute | solution.py:412
  52.9 1.9 %collective-permute-start.3 = (bf16[2,128,256]{2,1,0:T(8,128)(2,1)S(1)}, bf16[2,128,256]{2,1,0:T(8,128)(2,1)S(1)}, u32[]{:S(2)}, u32[]{:S(2)}) collective-permute-start(bf16[2,128,256]{2,1,0:T(8,128)(2,1)S(1)} %pad_maximum_fusion.2), channel_id=1, source_target_pairs={{144,16},{176,48},{208,80},{0,128},{32,160},{64,192},{96,224},{128... | collective-permute-start | bytes 393224 | tf_op jit(solution)/shard_map/ppermute | solution.py:412
  54.9 10.6 %collective-permute-done.3 = bf16[2,128,256]{2,1,0:T(8,128)(2,1)S(1)} collective-permute-done((bf16[2,128,256]{2,1,0:T(8,128)(2,1)S(1)}, bf16[2,128,256]{2,1,0:T(8,128)(2,1)S(1)}, u32[]{:S(2)}, u32[]{:S(2)}) %collective-permute-start.3) | collective-permute-done | bytes 131104 | tf_op jit(solution)/shard_map/ppermute | solution.py:412
  65.5 1.9 %collective-permute-start.4 = (bf16[4,128,256]{2,1,0:T(8,128)(2,1)S(1)}, bf16[4,128,256]{2,1,0:T(8,128)(2,1)S(1)}, u32[]{:S(2)}, u32[]{:S(2)}) collective-permute-start(bf16[4,128,256]{2,1,0:T(8,128)(2,1)S(1)} %pad_maximum_fusion.1), channel_id=1, source_target_pairs={{80,16},{0,64},{32,96},{64,128},{96,160},{128,192},{160,224},{192,... | collective-permute-start | bytes 786440 | tf_op jit(solution)/shard_map/ppermute | solution.py:412
  67.4 6.4 %collective-permute-done.4 = bf16[4,128,256]{2,1,0:T(8,128)(2,1)S(1)} collective-permute-done((bf16[4,128,256]{2,1,0:T(8,128)(2,1)S(1)}, bf16[4,128,256]{2,1,0:T(8,128)(2,1)S(1)}, u32[]{:S(2)}, u32[]{:S(2)}) %collective-permute-start.4) | collective-permute-done | bytes 262176 | tf_op jit(solution)/shard_map/ppermute | solution.py:412
  73.8 0.1 pad_maximum_fusion.keys_ref
  73.9 7.6 %collective-permute-start.5 = (bf16[8,128,256]{2,1,0:T(8,128)(2,1)S(1)}, bf16[8,128,256]{2,1,0:T(8,128)(2,1)}, u32[]{:S(2)}, u32[]{:S(2)}) collective-permute-start(bf16[8,128,256]{2,1,0:T(8,128)(2,1)S(1)} %pad_maximum_fusion.keys_ref), channel_id=1, source_target_pairs={{0,32},{32,64},{64,96},{96,128},{128,160},{160,192},{192,224},{224... | collective-permute-start | bytes 1572872 | tf_op jit(solution)/shard_map/ppermute | solution.py:412
  81.5 0.0 copy-done
  81.5 1.9 %collective-permute-start = (bf16[128,128]{1,0:T(8,128)(2,1)S(1)}, bf16[128,128]{1,0:T(8,128)(2,1)S(1)}, u32[]{:S(2)}, u32[]{:S(2)}) collective-permute-start(bf16[128,128]{1,0:T(8,128)(2,1)S(1)} %bitcast.23), channel_id=1, source_target_pairs={{16,0},{0,16},{48,32},{32,48},{80,64},{64,80},{112,96},{96,112},{1... | collective-permute-start | bytes 98312 | tf_op jit(solution)/shard_map/ppermute | solution.py:412
  83.4 1.2 collective-permute-done.swapped_ref
  84.6 1.5 attend_early.1.refs_0_
  86.1 0.7 collective-permute-done.5.keys_ref
  86.8 3.0 %attend_late.1 = (f32[256,256]{1,0:T(8,128)S(1)}, f32[256,256]{1,0:T(8,128)S(1)}) custom-call(s32[1]{0:T(128)} %bitcast.8.z_ref, s32[1]{0:T(128)} %bitcast.9.core_ref, bf16[128,128]{1,0:T(8,128)(2,1)S(1)} %bitcast.25, bf16[128,128]{1,0:T(8,128)(2,1)S(1)} %collective-permute-done.swapped_ref, bf16[8,128,256]{2,1,0:T(8,128)(2,1)} %collective-permute-done.5.keys_ref, ...), custom_call_target="tpu_custom_call" | custom-call | tf_op jit(solution)/shard_map/attend_late/pallas_call | solution.py:343
  89.8 1.9 %collective-permute-start.6 = (f32[256,256]{1,0:T(8,128)S(1)}, f32[256,256]{1,0:T(8,128)S(1)}, u32[]{:S(2)}, u32[]{:S(2)}) collective-permute-start(f32[256,256]{1,0:T(8,128)S(1)} %get-tuple-element.9), channel_id=1, source_target_pairs={{16,0},{0,16},{48,32},{32,48},{80,64},{64,80},{112,96},{96,112},{1... | collective-permute-start | bytes 786440 | tf_op jit(solution)/shard_map/ppermute | solution.py:412
  92.3 0.9 collective-permute-done.6.other_ref
  93.2 0.0 copy-done.3
  93.2 1.7 project.1.proj_ref
  94.9 0.0 all-to-all-done.1.x_ref
  94.9 4.0 %ffn.1 = bf16[16,768,128]{2,1,0:T(8,128)(2,1)S(1)} custom-call(bf16[16,640,128]{2,1,0:T(8,128)(2,1)S(1)} %all-to-all-done.1.x_ref, bf16[2048,256]{1,0:T(8,128)(2,1)} %bitcast.30, bf16[2048,256]{1,0:T(8,128)(2,1)} %bitcast.31, bf16[256,2048]{1,0:T(8,128)(2,1)} %bitcast.32, bf16[16,128,128]{2,1,0:T(8,128)(2,1)S(1)} %project.1.proj_ref), custom_call_target="tpu_custom_call" | custom-call | tf_op jit(solution)/shard_map/ffn/pallas_call | solution.py:190
  98.8 45.7 %all_to_all.21.in_ref = bf16[16,768,128]{2,1,0:T(8,128)(2,1)S(1)} all-to-all(bf16[16,768,128]{2,1,0:T(8,128)(2,1)S(1)} %ffn.1), channel_id=1, replica_groups=mesh['z'=16,'core'=2,'y'=4,'x'=4] {'y','x'}, dimensions={0} | all-to-all | bytes 6291456 | tf_op jit(solution)/shard_map/all_to_all | solution.py:420
  144.5 0.0 copy-start.1
  144.5 0.0 copy-start.2
  144.5 1.0 reduce_terms.1
  145.5 8.4 %all-to-all-start.3 = ((bf16[160,4,128]{2,1,0:T(4,128)(2,1)}), bf16[160,4,128]{2,1,0:T(4,128)(2,1)S(1)}, u32[]{:S(2)}, u32[]{:S(2)}) async-start(bf16[160,4,128]{2,1,0:T(4,128)(2,1)} %bitcast.16), calls=%async_computation.3 | async-start | bytes 327680 | tf_op jit(solution)/shard_map/all_to_all | solution.py:420
  154.0 0.0 copy-done.1
  154.0 0.0 copy-done.2
  154.0 0.6 weigh.1
  154.6 16.5 %all-to-all-done.3 = bf16[160,4,128]{2,1,0:T(4,128)(2,1)S(1)} async-done(((bf16[160,4,128]{2,1,0:T(4,128)(2,1)}), bf16[160,4,128]{2,1,0:T(4,128)(2,1)S(1)}, u32[]{:S(2)}, u32[]{:S(2)}) %all-to-all-start.3) | async-done | bytes 163872 | tf_op jit(solution)/shard_map/all_to_all | solution.py:420
  171.1 0.9 combine.1
  (4 shorter events, 0.1 us)
Async XLA Ops:
  38.1 7.0 %copy-start.4 = (bf16[128,1,128]{2,0,1:T(8,128)(2,1)S(1)}, bf16[128,1,128]{2,0,1:T(8,128)(2,1)}, u32[]{:S(2)}) copy-start(bf16[128,1,128]{2,0,1:T(8,128)(2,1)} %param.15) | copy-start | bytes 98308
  38.1 7.0 %copy-start.5 = (bf16[128,1,128]{2,0,1:T(8,128)(2,1)S(1)}, bf16[128,1,128]{2,0,1:T(8,128)(2,1)}, u32[]{:S(2)}) copy-start(bf16[128,1,128]{2,0,1:T(8,128)(2,1)} %param.14) | copy-start | bytes 98308
  38.1 43.3 %copy-start = (bf16[128,1,128]{2,0,1:T(8,128)(2,1)S(1)}, bf16[128,1,128]{2,0,1:T(8,128)(2,1)}, u32[]{:S(2)}) copy-start(bf16[128,1,128]{2,0,1:T(8,128)(2,1)} %param.13) | copy-start | bytes 98308
  38.1 56.7 %all-to-all-start.1 = ((bf16[16,640,128]{2,1,0:T(8,128)(2,1)}), bf16[16,640,128]{2,1,0:T(8,128)(2,1)S(1)}, u32[]{:S(2)}, u32[]{:S(2)}) async-start(bf16[16,640,128]{2,1,0:T(8,128)(2,1)} %spread_rows.1), calls=%async_computation.1 | async-start | bytes 5242880 | tf_op jit(solution)/shard_map/all_to_all | solution.py:420
  45.0 48.1 %copy-start.3 = (f32[128]{0:T(128)S(1)}, f32[128]{0:T(128)}, u32[]{:S(2)}) copy-start(f32[128]{0:T(128)} %param.17) | copy-start | bytes 1540
  45.1 5.0 %collective-permute-start.2 = (bf16[128,256]{1,0:T(8,128)(2,1)S(1)}, bf16[128,256]{1,0:T(8,128)(2,1)S(1)}, u32[]{:S(2)}, u32[]{:S(2)}) collective-permute-start(bf16[128,256]{1,0:T(8,128)(2,1)S(1)} %pad_maximum_fusion.3), channel_id=1, source_target_pairs={{48,16},{80,48},{112,80},{144,112},{176,144},{208,176},{240,208},{... | collective-permute-start | bytes 196616 | tf_op jit(solution)/shard_map/ppermute | solution.py:412
  47.0 5.9 %collective-permute-start.1 = (bf16[128,256]{1,0:T(8,128)(2,1)S(1)}, bf16[128,256]{1,0:T(8,128)(2,1)S(1)}, u32[]{:S(2)}, u32[]{:S(2)}) collective-permute-start(bf16[128,256]{1,0:T(8,128)(2,1)S(1)} %pad_maximum_fusion.3), channel_id=1, source_target_pairs={{16,0},{48,32},{80,64},{112,96},{144,128},{176,160},{208,192},{240... | collective-permute-start | bytes 196616 | tf_op jit(solution)/shard_map/ppermute | solution.py:412
  52.9 12.5 %collective-permute-start.3 = (bf16[2,128,256]{2,1,0:T(8,128)(2,1)S(1)}, bf16[2,128,256]{2,1,0:T(8,128)(2,1)S(1)}, u32[]{:S(2)}, u32[]{:S(2)}) collective-permute-start(bf16[2,128,256]{2,1,0:T(8,128)(2,1)S(1)} %pad_maximum_fusion.2), channel_id=1, source_target_pairs={{144,16},{176,48},{208,80},{0,128},{32,160},{64,192},{96,224},{128... | collective-permute-start | bytes 393224 | tf_op jit(solution)/shard_map/ppermute | solution.py:412
  65.5 8.3 %collective-permute-start.4 = (bf16[4,128,256]{2,1,0:T(8,128)(2,1)S(1)}, bf16[4,128,256]{2,1,0:T(8,128)(2,1)S(1)}, u32[]{:S(2)}, u32[]{:S(2)}) collective-permute-start(bf16[4,128,256]{2,1,0:T(8,128)(2,1)S(1)} %pad_maximum_fusion.1), channel_id=1, source_target_pairs={{80,16},{0,64},{32,96},{64,128},{96,160},{128,192},{160,224},{192,... | collective-permute-start | bytes 786440 | tf_op jit(solution)/shard_map/ppermute | solution.py:412
  73.9 12.9 %collective-permute-start.5 = (bf16[8,128,256]{2,1,0:T(8,128)(2,1)S(1)}, bf16[8,128,256]{2,1,0:T(8,128)(2,1)}, u32[]{:S(2)}, u32[]{:S(2)}) collective-permute-start(bf16[8,128,256]{2,1,0:T(8,128)(2,1)S(1)} %pad_maximum_fusion.keys_ref), channel_id=1, source_target_pairs={{0,32},{32,64},{64,96},{96,128},{128,160},{160,192},{192,224},{224... | collective-permute-start | bytes 1572872 | tf_op jit(solution)/shard_map/ppermute | solution.py:412
  81.5 3.1 %collective-permute-start = (bf16[128,128]{1,0:T(8,128)(2,1)S(1)}, bf16[128,128]{1,0:T(8,128)(2,1)S(1)}, u32[]{:S(2)}, u32[]{:S(2)}) collective-permute-start(bf16[128,128]{1,0:T(8,128)(2,1)S(1)} %bitcast.23), channel_id=1, source_target_pairs={{16,0},{0,16},{48,32},{32,48},{80,64},{64,80},{112,96},{96,112},{1... | collective-permute-start | bytes 98312 | tf_op jit(solution)/shard_map/ppermute | solution.py:412
  89.8 3.4 %collective-permute-start.6 = (f32[256,256]{1,0:T(8,128)S(1)}, f32[256,256]{1,0:T(8,128)S(1)}, u32[]{:S(2)}, u32[]{:S(2)}) collective-permute-start(f32[256,256]{1,0:T(8,128)S(1)} %get-tuple-element.9), channel_id=1, source_target_pairs={{16,0},{0,16},{48,32},{32,48},{80,64},{64,80},{112,96},{96,112},{1... | collective-permute-start | bytes 786440 | tf_op jit(solution)/shard_map/ppermute | solution.py:412
  144.5 9.4 %copy-start.1 = (s32[128,4]{0,1:T(4,128)S(1)}, s32[128,4]{0,1:T(4,128)}, u32[]{:S(2)}) copy-start(s32[128,4]{0,1:T(4,128)} %param.21) | copy-start | bytes 6148
  144.5 9.4 %copy-start.2 = (f32[128,4]{0,1:T(4,128)S(1)}, f32[128,4]{0,1:T(4,128)}, u32[]{:S(2)}) copy-start(f32[128,4]{0,1:T(4,128)} %param.22) | copy-start | bytes 6148
  145.5 25.5 %all-to-all-start.3 = ((bf16[160,4,128]{2,1,0:T(4,128)(2,1)}), bf16[160,4,128]{2,1,0:T(4,128)(2,1)S(1)}, u32[]{:S(2)}, u32[]{:S(2)}) async-start(bf16[160,4,128]{2,1,0:T(4,128)(2,1)} %bitcast.16), calls=%async_computation.3 | async-start | bytes 327680 | tf_op jit(solution)/shard_map/all_to_all | solution.py:420

commit v10 on v9

--- a/solution.py
+++ b/solution.py
@@ -16,6 +16,7 @@
 
 Z, CORE, Y, X = 16, 2, 4, 4
 EP = ("z", "core")
+EP_SENT = ("core", "z")
 TP = ("y", "x")
 N_EP = Z * CORE
 N_TP = Y * X
@@ -44,7 +45,8 @@
 
 
 def routing(ids, values=None):
-    expert = lax.broadcasted_iota(jnp.int32, (N_EP, TOK), 0)
+    block = lax.broadcasted_iota(jnp.int32, (N_EP, TOK), 0)
+    expert = CORE * (block % Z) + block // Z
     named = jnp.zeros((N_EP, TOK), F32)
     weight = jnp.zeros((N_EP, TOK), F32)
     for k in range(ids.shape[0]):
@@ -64,7 +66,7 @@
     row = lax.broadcasted_iota(jnp.int32, (ROWS, N_EP), 0)
     first = lax.broadcasted_iota(jnp.int32, (ROWS, N_EP), 1) * CAP
     owner = jnp.where((row >= first) & (row < first + CAP), 1.0, 0.0).astype(BF16)
-    parts = [slot, expert.astype(F32)]
+    parts = [slot, block.astype(F32)]
     if values is not None:
         for _ in range(3):
             parts.append(weight.astype(BF16).astype(F32))
@@ -75,41 +77,33 @@
     return jnp.where(spread[0] == place, value, 0.0)
 
 
-def dispatch_kernel(at_ref, ids_ref, rows_hbm, gain_hbm, out_ref, rows_ref, part_ref, gain_ref, sems):
-    low = pl.multiple_of(at_ref[0] * WIDE, WIDE)
-    copies = [
-        pltpu.make_async_copy(rows_hbm, rows_ref, sems.at[0]),
-        pltpu.make_async_copy(rows_hbm.at[:, pl.ds(low, WIDE)], part_ref, sems.at[1]),
-        pltpu.make_async_copy(gain_hbm.at[:, pl.ds(low, WIDE)], gain_ref, sems.at[2]),
-    ]
-    for copy in copies:
-        copy.start()
-    chosen = routing(ids_ref[...]).astype(BF16)
-    for copy in copies:
-        copy.wait()
+def dispatch_kernel(at_ref, rows_ref, part_ref, gain_ref, ids_ref, out_ref):
     rows = rows_ref[...].astype(F32)
     mean_sq = jnp.mean(rows * rows, axis=-1, keepdims=True)
     part = part_ref[...].astype(F32) * lax.rsqrt(mean_sq + NORM_EPS) * gain_ref[...]
-    out_ref[...] = jnp.dot(chosen, part.astype(BF16), preferred_element_type=F32).astype(BF16)
+    chosen = routing(ids_ref[...]).astype(BF16)
+    packed = jnp.dot(chosen, part.astype(BF16), preferred_element_type=F32)
+    out_ref[...] = packed.astype(BF16)
 
 
 def dispatch(at, token_rows, gain, ids):
-    vmem = pl.BlockSpec(memory_space=pltpu.VMEM)
-    hbm = pl.BlockSpec(memory_space=pl.ANY)
     return pl.pallas_call(
         dispatch_kernel,
         out_shape=jax.ShapeDtypeStruct((ROWS, WIDE), BF16),
-        in_specs=[pl.BlockSpec(memory_space=pltpu.SMEM), vmem, hbm, hbm],
-        out_specs=vmem,
-        scratch_shapes=[
-            pltpu.VMEM((TOK, MODEL), BF16),
-            pltpu.VMEM((TOK, WIDE), BF16),
-            pltpu.VMEM((1, WIDE), F32),
-            pltpu.SemaphoreType.DMA((3,)),
-        ],
+        grid_spec=pltpu.PrefetchScalarGridSpec(
+            num_scalar_prefetch=1,
+            grid=(1,),
+            in_specs=[
+                pl.BlockSpec((TOK, MODEL), lambda i, at: (0, 0)),
+                pl.BlockSpec((TOK, WIDE), lambda i, at: (0, at[0])),
+                pl.BlockSpec((1, WIDE), lambda i, at: (0, at[0])),
+                pl.BlockSpec((4, TOK), lambda i, at: (0, 0)),
+            ],
+            out_specs=pl.BlockSpec((ROWS, WIDE), lambda i, at: (0, 0)),
+        ),
         compiler_params=params(8),
         name="dispatch",
-    )(at, *(in_hbm(a) for a in (ids, token_rows, gain)))
+    )(at, *(in_hbm(a) for a in (token_rows, token_rows, gain, ids)))
 
 
 def spread_kernel(in_ref, out_hbm, sems):
@@ -421,7 +415,7 @@
 
 
 def exchanged_rows(rows):
-    return exchanged(rows.reshape(ROWS // QUARTER, QUARTER, WIDE), EP).reshape(ROWS, WIDE)
+    return exchanged(rows.reshape(ROWS // QUARTER, QUARTER, WIDE), EP_SENT).reshape(ROWS, WIDE)
 
 
 def collect_keys(keys, values, core_at):

time: 173 us -> 172 us (level)
    ppermute x7, starting transfers between devices: 19.8 us -> 13.6 us  [moved(): return lax.ppermute(array, EP, flat)]
    all_to_all x2, starting transfers between devices: 15.3 us -> 20.1 us  [exchanged(): return lax.all_to_all(array, axes, split_axis=0, concat_axis=0, tiled=True)]
where the time goes in v10:
time: 172 us
  blocking collectives  79.9 us (46%)
  waiting for transfers between devices  40.5 us (24%)
  starting transfers between devices  33.7 us (20%)
  Pallas kernels  15.9 us (9%)
    all_to_all x2, blocking collectives, exchanged(): return lax.all_to_all(array, axes, split_axis=0, concat_axis=0, tiled=True)  79.9 us
    ppermute x7, waiting for transfers between devices, moved(): return lax.ppermute(array, EP, flat)  23.5 us
    all_to_all x2, starting transfers between devices, exchanged(): return lax.all_to_all(array, axes, split_axis=0, concat_axis=0, tiled=True)  20.1 us
    all_to_all x2, waiting for transfers between devices, exchanged(): return lax.all_to_all(array, axes, split_axis=0, concat_axis=0, tiled=True)  17 us
    ppermute x7, starting transfers between devices, moved(): return lax.ppermute(array, EP, flat)  13.6 us
    pallas_call x2, Pallas kernels, attend(): pl.pallas_call(functools.partial(attend_kernel, late), out_shape=tuple((j...  4.49 us
    pallas_call x1, Pallas kernels, ffn(): pl.pallas_call(ffn_kernel, out_shape=pltpu.VMEM((N_TP, OUT_ROWS, WIDE), B...  3.96 us
  transfers between devices with their start and end apart: 9, of which 8 were waited for; matrix products, arithmetic and copies ran while one was open for 0% of the time, Pallas kernels for 4%

profile of v10, /device:TPU:1, one launch (start us, length us, event | category | flops | bytes accessed | tf_op | source)
XLA Modules:
  0.0 171.6 jit_solution(3737421250169356835)
XLA Ops:
  0.6 1.6 dispatch.1
  2.3 34.2 %all_to_all.20 = bf16[160,4,128]{2,1,0:T(4,128)(2,1)S(1)} all-to-all(bf16[160,4,128]{2,1,0:T(4,128)(2,1)S(1)} %bitcast.20), channel_id=1, replica_groups=mesh['z'=16,'core'=2,'y'=4,'x'=4] {'core','z'}, dimensions={0} | all-to-all | bytes 327680 | tf_op jit(solution)/shard_map/all_to_all | solution.py:414
  36.5 1.6 spread_rows.1
  38.1 0.0 copy-start.4
  38.1 0.0 copy-start.5
  38.1 0.0 copy-start
  38.1 6.9 %all-to-all-start.1 = ((bf16[16,640,128]{2,1,0:T(8,128)(2,1)}), bf16[16,640,128]{2,1,0:T(8,128)(2,1)S(1)}, u32[]{:S(2)}, u32[]{:S(2)}) async-start(bf16[16,640,128]{2,1,0:T(8,128)(2,1)} %spread_rows.1), calls=%async_computation.1 | async-start | bytes 5242880 | tf_op jit(solution)/shard_map/all_to_all | solution.py:414
  45.0 0.0 copy-start.3
  45.1 0.0 copy-done.4
  45.1 0.0 copy-done.5
  45.1 1.9 %collective-permute-start.2 = (bf16[128,256]{1,0:T(8,128)(2,1)S(1)}, bf16[128,256]{1,0:T(8,128)(2,1)S(1)}, u32[]{:S(2)}, u32[]{:S(2)}) collective-permute-start(bf16[128,256]{1,0:T(8,128)(2,1)S(1)} %pad_maximum_fusion.3), channel_id=1, source_target_pairs={{48,16},{80,48},{112,80},{144,112},{176,144},{208,176},{240,208},{... | collective-permute-start | bytes 196616 | tf_op jit(solution)/shard_map/ppermute | solution.py:406
  47.0 1.9 %collective-permute-start.1 = (bf16[128,256]{1,0:T(8,128)(2,1)S(1)}, bf16[128,256]{1,0:T(8,128)(2,1)S(1)}, u32[]{:S(2)}, u32[]{:S(2)}) collective-permute-start(bf16[128,256]{1,0:T(8,128)(2,1)S(1)} %pad_maximum_fusion.3), channel_id=1, source_target_pairs={{16,0},{48,32},{80,64},{112,96},{144,128},{176,160},{208,192},{240... | collective-permute-start | bytes 196616 | tf_op jit(solution)/shard_map/ppermute | solution.py:406
  49.0 1.4 collective-permute-done.2
  50.4 2.5 %collective-permute-done.1 = bf16[128,256]{1,0:T(8,128)(2,1)S(1)} collective-permute-done((bf16[128,256]{1,0:T(8,128)(2,1)S(1)}, bf16[128,256]{1,0:T(8,128)(2,1)S(1)}, u32[]{:S(2)}, u32[]{:S(2)}) %collective-permute-start.1) | collective-permute-done | bytes 65568 | tf_op jit(solution)/shard_map/ppermute | solution.py:406
  52.9 1.9 %collective-permute-start.3 = (bf16[2,128,256]{2,1,0:T(8,128)(2,1)S(1)}, bf16[2,128,256]{2,1,0:T(8,128)(2,1)S(1)}, u32[]{:S(2)}, u32[]{:S(2)}) collective-permute-start(bf16[2,128,256]{2,1,0:T(8,128)(2,1)S(1)} %pad_maximum_fusion.2), channel_id=1, source_target_pairs={{144,16},{176,48},{208,80},{0,128},{32,160},{64,192},{96,224},{128... | collective-permute-start | bytes 393224 | tf_op jit(solution)/shard_map/ppermute | solution.py:406
  54.8 10.5 %collective-permute-done.3 = bf16[2,128,256]{2,1,0:T(8,128)(2,1)S(1)} collective-permute-done((bf16[2,128,256]{2,1,0:T(8,128)(2,1)S(1)}, bf16[2,128,256]{2,1,0:T(8,128)(2,1)S(1)}, u32[]{:S(2)}, u32[]{:S(2)}) %collective-permute-start.3) | collective-permute-done | bytes 131104 | tf_op jit(solution)/shard_map/ppermute | solution.py:406
  65.4 1.9 %collective-permute-start.4 = (bf16[4,128,256]{2,1,0:T(8,128)(2,1)S(1)}, bf16[4,128,256]{2,1,0:T(8,128)(2,1)S(1)}, u32[]{:S(2)}, u32[]{:S(2)}) collective-permute-start(bf16[4,128,256]{2,1,0:T(8,128)(2,1)S(1)} %pad_maximum_fusion.1), channel_id=1, source_target_pairs={{80,16},{0,64},{32,96},{64,128},{96,160},{128,192},{160,224},{192,... | collective-permute-start | bytes 786440 | tf_op jit(solution)/shard_map/ppermute | solution.py:406
  67.3 6.4 %collective-permute-done.4 = bf16[4,128,256]{2,1,0:T(8,128)(2,1)S(1)} collective-permute-done((bf16[4,128,256]{2,1,0:T(8,128)(2,1)S(1)}, bf16[4,128,256]{2,1,0:T(8,128)(2,1)S(1)}, u32[]{:S(2)}, u32[]{:S(2)}) %collective-permute-start.4) | collective-permute-done | bytes 262176 | tf_op jit(solution)/shard_map/ppermute | solution.py:406
  73.7 0.1 pad_maximum_fusion.keys_ref
  73.8 2.1 %collective-permute-start.5 = (bf16[8,128,256]{2,1,0:T(8,128)(2,1)S(1)}, bf16[8,128,256]{2,1,0:T(8,128)(2,1)}, u32[]{:S(2)}, u32[]{:S(2)}) collective-permute-start(bf16[8,128,256]{2,1,0:T(8,128)(2,1)S(1)} %pad_maximum_fusion.keys_ref), channel_id=1, source_target_pairs={{0,32},{32,64},{64,96},{96,128},{128,160},{160,192},{192,224},{224... | collective-permute-start | bytes 1572872 | tf_op jit(solution)/shard_map/ppermute | solution.py:406
  75.8 0.0 copy-done
  75.8 1.9 %collective-permute-start = (bf16[128,128]{1,0:T(8,128)(2,1)S(1)}, bf16[128,128]{1,0:T(8,128)(2,1)S(1)}, u32[]{:S(2)}, u32[]{:S(2)}) collective-permute-start(bf16[128,128]{1,0:T(8,128)(2,1)S(1)} %bitcast.23), channel_id=1, source_target_pairs={{16,0},{0,16},{48,32},{32,48},{80,64},{64,80},{112,96},{96,112},{1... | collective-permute-start | bytes 98312 | tf_op jit(solution)/shard_map/ppermute | solution.py:406
  77.8 1.2 collective-permute-done.swapped_ref
  78.9 1.5 attend_early.1.refs_0_
  80.5 0.7 collective-permute-done.5.keys_ref
  81.2 3.0 %attend_late.1 = (f32[256,256]{1,0:T(8,128)S(1)}, f32[256,256]{1,0:T(8,128)S(1)}) custom-call(s32[1]{0:T(128)} %bitcast.8.z_ref, s32[1]{0:T(128)} %bitcast.9.core_ref, bf16[128,128]{1,0:T(8,128)(2,1)S(1)} %bitcast.25, bf16[128,128]{1,0:T(8,128)(2,1)S(1)} %collective-permute-done.swapped_ref, bf16[8,128,256]{2,1,0:T(8,128)(2,1)} %collective-permute-done.5.keys_ref, ...), custom_call_target="tpu_custom_call" | custom-call | tf_op jit(solution)/shard_map/attend_late/pallas_call | solution.py:337
  84.1 1.9 %collective-permute-start.6 = (f32[256,256]{1,0:T(8,128)S(1)}, f32[256,256]{1,0:T(8,128)S(1)}, u32[]{:S(2)}, u32[]{:S(2)}) collective-permute-start(f32[256,256]{1,0:T(8,128)S(1)} %get-tuple-element.9), channel_id=1, source_target_pairs={{16,0},{0,16},{48,32},{32,48},{80,64},{64,80},{112,96},{96,112},{1... | collective-permute-start | bytes 786440 | tf_op jit(solution)/shard_map/ppermute | solution.py:406
  86.7 0.9 collective-permute-done.6.other_ref
  87.6 0.0 copy-done.3
  87.6 1.7 project.1.proj_ref
  89.2 0.0 all-to-all-done.1.x_ref
  89.2 4.0 %ffn.1 = bf16[16,768,128]{2,1,0:T(8,128)(2,1)S(1)} custom-call(bf16[16,640,128]{2,1,0:T(8,128)(2,1)S(1)} %all-to-all-done.1.x_ref, bf16[2048,256]{1,0:T(8,128)(2,1)} %bitcast.30, bf16[2048,256]{1,0:T(8,128)(2,1)} %bitcast.31, bf16[256,2048]{1,0:T(8,128)(2,1)} %bitcast.32, bf16[16,128,128]{2,1,0:T(8,128)(2,1)S(1)} %project.1.proj_ref), custom_call_target="tpu_custom_call" | custom-call | tf_op jit(solution)/shard_map/ffn/pallas_call | solution.py:184
  93.2 45.7 %all_to_all.21.in_ref = bf16[16,768,128]{2,1,0:T(8,128)(2,1)S(1)} all-to-all(bf16[16,768,128]{2,1,0:T(8,128)(2,1)S(1)} %ffn.1), channel_id=1, replica_groups=mesh['z'=16,'core'=2,'y'=4,'x'=4] {'y','x'}, dimensions={0} | all-to-all | bytes 6291456 | tf_op jit(solution)/shard_map/all_to_all | solution.py:414
  138.9 0.0 copy-start.1
  138.9 0.0 copy-start.2
  138.9 1.0 reduce_terms.1
  139.9 13.2 %all-to-all-start.3 = ((bf16[160,4,128]{2,1,0:T(4,128)(2,1)}), bf16[160,4,128]{2,1,0:T(4,128)(2,1)S(1)}, u32[]{:S(2)}, u32[]{:S(2)}) async-start(bf16[160,4,128]{2,1,0:T(4,128)(2,1)} %bitcast.16), calls=%async_computation.3 | async-start | bytes 327680 | tf_op jit(solution)/shard_map/all_to_all | solution.py:414
  153.1 0.0 copy-done.1
  153.1 0.0 copy-done.2
  153.1 0.6 weigh.1
  153.7 17.0 %all-to-all-done.3 = bf16[160,4,128]{2,1,0:T(4,128)(2,1)S(1)} async-done(((bf16[160,4,128]{2,1,0:T(4,128)(2,1)}), bf16[160,4,128]{2,1,0:T(4,128)(2,1)S(1)}, u32[]{:S(2)}, u32[]{:S(2)}) %all-to-all-start.3) | async-done | bytes 163872 | tf_op jit(solution)/shard_map/all_to_all | solution.py:414
  170.7 0.9 combine.1
  (4 shorter events, 0.1 us)
Async XLA Ops:
  38.1 7.0 %copy-start.4 = (bf16[128,1,128]{2,0,1:T(8,128)(2,1)S(1)}, bf16[128,1,128]{2,0,1:T(8,128)(2,1)}, u32[]{:S(2)}) copy-start(bf16[128,1,128]{2,0,1:T(8,128)(2,1)} %param.15) | copy-start | bytes 98308
  38.1 7.0 %copy-start.5 = (bf16[128,1,128]{2,0,1:T(8,128)(2,1)S(1)}, bf16[128,1,128]{2,0,1:T(8,128)(2,1)}, u32[]{:S(2)}) copy-start(bf16[128,1,128]{2,0,1:T(8,128)(2,1)} %param.14) | copy-start | bytes 98308
  38.1 37.7 %copy-start = (bf16[128,1,128]{2,0,1:T(8,128)(2,1)S(1)}, bf16[128,1,128]{2,0,1:T(8,128)(2,1)}, u32[]{:S(2)}) copy-start(bf16[128,1,128]{2,0,1:T(8,128)(2,1)} %param.13) | copy-start | bytes 98308
  38.1 51.1 %all-to-all-start.1 = ((bf16[16,640,128]{2,1,0:T(8,128)(2,1)}), bf16[16,640,128]{2,1,0:T(8,128)(2,1)S(1)}, u32[]{:S(2)}, u32[]{:S(2)}) async-start(bf16[16,640,128]{2,1,0:T(8,128)(2,1)} %spread_rows.1), calls=%async_computation.1 | async-start | bytes 5242880 | tf_op jit(solution)/shard_map/all_to_all | solution.py:414
  45.0 42.5 %copy-start.3 = (f32[128]{0:T(128)S(1)}, f32[128]{0:T(128)}, u32[]{:S(2)}) copy-start(f32[128]{0:T(128)} %param.17) | copy-start | bytes 1540
  45.1 5.3 %collective-permute-start.2 = (bf16[128,256]{1,0:T(8,128)(2,1)S(1)}, bf16[128,256]{1,0:T(8,128)(2,1)S(1)}, u32[]{:S(2)}, u32[]{:S(2)}) collective-permute-start(bf16[128,256]{1,0:T(8,128)(2,1)S(1)} %pad_maximum_fusion.3), channel_id=1, source_target_pairs={{48,16},{80,48},{112,80},{144,112},{176,144},{208,176},{240,208},{... | collective-permute-start | bytes 196616 | tf_op jit(solution)/shard_map/ppermute | solution.py:406
  47.0 5.9 %collective-permute-start.1 = (bf16[128,256]{1,0:T(8,128)(2,1)S(1)}, bf16[128,256]{1,0:T(8,128)(2,1)S(1)}, u32[]{:S(2)}, u32[]{:S(2)}) collective-permute-start(bf16[128,256]{1,0:T(8,128)(2,1)S(1)} %pad_maximum_fusion.3), channel_id=1, source_target_pairs={{16,0},{48,32},{80,64},{112,96},{144,128},{176,160},{208,192},{240... | collective-permute-start | bytes 196616 | tf_op jit(solution)/shard_map/ppermute | solution.py:406
  52.9 12.4 %collective-permute-start.3 = (bf16[2,128,256]{2,1,0:T(8,128)(2,1)S(1)}, bf16[2,128,256]{2,1,0:T(8,128)(2,1)S(1)}, u32[]{:S(2)}, u32[]{:S(2)}) collective-permute-start(bf16[2,128,256]{2,1,0:T(8,128)(2,1)S(1)} %pad_maximum_fusion.2), channel_id=1, source_target_pairs={{144,16},{176,48},{208,80},{0,128},{32,160},{64,192},{96,224},{128... | collective-permute-start | bytes 393224 | tf_op jit(solution)/shard_map/ppermute | solution.py:406
  65.4 8.3 %collective-permute-start.4 = (bf16[4,128,256]{2,1,0:T(8,128)(2,1)S(1)}, bf16[4,128,256]{2,1,0:T(8,128)(2,1)S(1)}, u32[]{:S(2)}, u32[]{:S(2)}) collective-permute-start(bf16[4,128,256]{2,1,0:T(8,128)(2,1)S(1)} %pad_maximum_fusion.1), channel_id=1, source_target_pairs={{80,16},{0,64},{32,96},{64,128},{96,160},{128,192},{160,224},{192,... | collective-permute-start | bytes 786440 | tf_op jit(solution)/shard_map/ppermute | solution.py:406
  73.8 7.4 %collective-permute-start.5 = (bf16[8,128,256]{2,1,0:T(8,128)(2,1)S(1)}, bf16[8,128,256]{2,1,0:T(8,128)(2,1)}, u32[]{:S(2)}, u32[]{:S(2)}) collective-permute-start(bf16[8,128,256]{2,1,0:T(8,128)(2,1)S(1)} %pad_maximum_fusion.keys_ref), channel_id=1, source_target_pairs={{0,32},{32,64},{64,96},{96,128},{128,160},{160,192},{192,224},{224... | collective-permute-start | bytes 1572872 | tf_op jit(solution)/shard_map/ppermute | solution.py:406
  75.8 3.1 %collective-permute-start = (bf16[128,128]{1,0:T(8,128)(2,1)S(1)}, bf16[128,128]{1,0:T(8,128)(2,1)S(1)}, u32[]{:S(2)}, u32[]{:S(2)}) collective-permute-start(bf16[128,128]{1,0:T(8,128)(2,1)S(1)} %bitcast.23), channel_id=1, source_target_pairs={{16,0},{0,16},{48,32},{32,48},{80,64},{64,80},{112,96},{96,112},{1... | collective-permute-start | bytes 98312 | tf_op jit(solution)/shard_map/ppermute | solution.py:406
  84.1 3.4 %collective-permute-start.6 = (f32[256,256]{1,0:T(8,128)S(1)}, f32[256,256]{1,0:T(8,128)S(1)}, u32[]{:S(2)}, u32[]{:S(2)}) collective-permute-start(f32[256,256]{1,0:T(8,128)S(1)} %get-tuple-element.9), channel_id=1, source_target_pairs={{16,0},{0,16},{48,32},{32,48},{80,64},{64,80},{112,96},{96,112},{1... | collective-permute-start | bytes 786440 | tf_op jit(solution)/shard_map/ppermute | solution.py:406
  138.9 14.2 %copy-start.1 = (s32[128,4]{0,1:T(4,128)S(1)}, s32[128,4]{0,1:T(4,128)}, u32[]{:S(2)}) copy-start(s32[128,4]{0,1:T(4,128)} %param.21) | copy-start | bytes 6148
  138.9 14.2 %copy-start.2 = (f32[128,4]{0,1:T(4,128)S(1)}, f32[128,4]{0,1:T(4,128)}, u32[]{:S(2)}) copy-start(f32[128,4]{0,1:T(4,128)} %param.22) | copy-start | bytes 6148
  139.9 30.8 %all-to-all-start.3 = ((bf16[160,4,128]{2,1,0:T(4,128)(2,1)}), bf16[160,4,128]{2,1,0:T(4,128)(2,1)S(1)}, u32[]{:S(2)}, u32[]{:S(2)}) async-start(bf16[160,4,128]{2,1,0:T(4,128)(2,1)} %bitcast.16), calls=%async_computation.3 | async-start | bytes 327680 | tf_op jit(solution)/shard_map/all_to_all | solution.py:414

commit v11 on v10

--- a/solution.py
+++ b/solution.py
@@ -16,7 +16,6 @@
 
 Z, CORE, Y, X = 16, 2, 4, 4
 EP = ("z", "core")
-EP_SENT = ("core", "z")
 TP = ("y", "x")
 N_EP = Z * CORE
 N_TP = Y * X
@@ -45,8 +44,7 @@
 
 
 def routing(ids, values=None):
-    block = lax.broadcasted_iota(jnp.int32, (N_EP, TOK), 0)
-    expert = CORE * (block % Z) + block // Z
+    expert = lax.broadcasted_iota(jnp.int32, (N_EP, TOK), 0)
     named = jnp.zeros((N_EP, TOK), F32)
     weight = jnp.zeros((N_EP, TOK), F32)
     for k in range(ids.shape[0]):
@@ -66,7 +64,7 @@
     row = lax.broadcasted_iota(jnp.int32, (ROWS, N_EP), 0)
     first = lax.broadcasted_iota(jnp.int32, (ROWS, N_EP), 1) * CAP
     owner = jnp.where((row >= first) & (row < first + CAP), 1.0, 0.0).astype(BF16)
-    parts = [slot, block.astype(F32)]
+    parts = [slot, expert.astype(F32)]
     if values is not None:
         for _ in range(3):
             parts.append(weight.astype(BF16).astype(F32))
@@ -415,7 +413,7 @@
 
 
 def exchanged_rows(rows):
-    return exchanged(rows.reshape(ROWS // QUARTER, QUARTER, WIDE), EP_SENT).reshape(ROWS, WIDE)
+    return exchanged(rows.reshape(ROWS // QUARTER, QUARTER, WIDE), EP).reshape(ROWS, WIDE)
 
 
 def collect_keys(keys, values, core_at):

time: 172 us -> 172 us (level)
    ppermute x7, starting transfers between devices: 13.6 us -> 19.8 us  [moved(): return lax.ppermute(array, EP, flat)]
    all_to_all x2, starting transfers between devices: 20.1 us -> 15.3 us  [exchanged(): return lax.all_to_all(array, axes, split_axis=0, concat_axis=0, tiled=True)]
where the time goes in v11:
time: 172 us; the launch traced here: 171 us
  blocking collectives  79.4 us (46%)
  waiting for transfers between devices  39.4 us (23%)
  starting transfers between devices  35.1 us (20%)
  Pallas kernels  15.9 us (9%)
    all_to_all x2, blocking collectives, exchanged(): return lax.all_to_all(array, axes, split_axis=0, concat_axis=0, tiled=True)  79.4 us
    ppermute x7, waiting for transfers between devices, moved(): return lax.ppermute(array, EP, flat)  22.9 us
    ppermute x7, starting transfers between devices, moved(): return lax.ppermute(array, EP, flat)  19.8 us
    all_to_all x2, waiting for transfers between devices, exchanged(): return lax.all_to_all(array, axes, split_axis=0, concat_axis=0, tiled=True)  16.5 us
    all_to_all x2, starting transfers between devices, exchanged(): return lax.all_to_all(array, axes, split_axis=0, concat_axis=0, tiled=True)  15.3 us
    pallas_call x2, Pallas kernels, attend(): pl.pallas_call(functools.partial(attend_kernel, late), out_shape=tuple((j...  4.49 us
    pallas_call x1, Pallas kernels, ffn(): pl.pallas_call(ffn_kernel, out_shape=pltpu.VMEM((N_TP, OUT_ROWS, WIDE), B...  3.96 us
  transfers between devices with their start and end apart: 9, of which 8 were waited for; matrix products, arithmetic and copies ran while one was open for 0% of the time, Pallas kernels for 4%

profile of v11, /device:TPU:1, one launch (start us, length us, event | category | flops | bytes accessed | tf_op | source)
XLA Modules:
  0.0 171.4 jit_solution(14406716554054213795)
XLA Ops:
  0.6 1.6 dispatch.1
  2.3 33.7 %all_to_all.20 = bf16[160,4,128]{2,1,0:T(4,128)(2,1)S(1)} all-to-all(bf16[160,4,128]{2,1,0:T(4,128)(2,1)S(1)} %bitcast.20), channel_id=1, replica_groups=mesh['z'=16,'core'=2,'y'=4,'x'=4] {'z','core'}, dimensions={0} | all-to-all | bytes 327680 | tf_op jit(solution)/shard_map/all_to_all | solution.py:412
  35.9 1.6 spread_rows.1
  37.6 0.0 copy-start.4
  37.6 0.0 copy-start.5
  37.6 0.0 copy-start
  37.6 6.9 %all-to-all-start.1 = ((bf16[16,640,128]{2,1,0:T(8,128)(2,1)}), bf16[16,640,128]{2,1,0:T(8,128)(2,1)S(1)}, u32[]{:S(2)}, u32[]{:S(2)}) async-start(bf16[16,640,128]{2,1,0:T(8,128)(2,1)} %spread_rows.1), calls=%async_computation.1 | async-start | bytes 5242880 | tf_op jit(solution)/shard_map/all_to_all | solution.py:412
  44.5 0.0 copy-start.3
  44.5 0.0 copy-done.4
  44.5 0.0 copy-done.5
  44.6 1.9 %collective-permute-start.2 = (bf16[128,256]{1,0:T(8,128)(2,1)S(1)}, bf16[128,256]{1,0:T(8,128)(2,1)S(1)}, u32[]{:S(2)}, u32[]{:S(2)}) collective-permute-start(bf16[128,256]{1,0:T(8,128)(2,1)S(1)} %pad_maximum_fusion.3), channel_id=1, source_target_pairs={{48,16},{80,48},{112,80},{144,112},{176,144},{208,176},{240,208},{... | collective-permute-start | bytes 196616 | tf_op jit(solution)/shard_map/ppermute | solution.py:404
  46.5 2.6 %collective-permute-start.1 = (bf16[128,256]{1,0:T(8,128)(2,1)S(1)}, bf16[128,256]{1,0:T(8,128)(2,1)S(1)}, u32[]{:S(2)}, u32[]{:S(2)}) collective-permute-start(bf16[128,256]{1,0:T(8,128)(2,1)S(1)} %pad_maximum_fusion.3), channel_id=1, source_target_pairs={{16,0},{48,32},{80,64},{112,96},{144,128},{176,160},{208,192},{240... | collective-permute-start | bytes 196616 | tf_op jit(solution)/shard_map/ppermute | solution.py:404
  49.1 0.4 collective-permute-done.2
  49.6 2.8 %collective-permute-done.1 = bf16[128,256]{1,0:T(8,128)(2,1)S(1)} collective-permute-done((bf16[128,256]{1,0:T(8,128)(2,1)S(1)}, bf16[128,256]{1,0:T(8,128)(2,1)S(1)}, u32[]{:S(2)}, u32[]{:S(2)}) %collective-permute-start.1) | collective-permute-done | bytes 65568 | tf_op jit(solution)/shard_map/ppermute | solution.py:404
  52.4 1.9 %collective-permute-start.3 = (bf16[2,128,256]{2,1,0:T(8,128)(2,1)S(1)}, bf16[2,128,256]{2,1,0:T(8,128)(2,1)S(1)}, u32[]{:S(2)}, u32[]{:S(2)}) collective-permute-start(bf16[2,128,256]{2,1,0:T(8,128)(2,1)S(1)} %pad_maximum_fusion.2), channel_id=1, source_target_pairs={{144,16},{176,48},{208,80},{0,128},{32,160},{64,192},{96,224},{128... | collective-permute-start | bytes 393224 | tf_op jit(solution)/shard_map/ppermute | solution.py:404
  54.3 10.6 %collective-permute-done.3 = bf16[2,128,256]{2,1,0:T(8,128)(2,1)S(1)} collective-permute-done((bf16[2,128,256]{2,1,0:T(8,128)(2,1)S(1)}, bf16[2,128,256]{2,1,0:T(8,128)(2,1)S(1)}, u32[]{:S(2)}, u32[]{:S(2)}) %collective-permute-start.3) | collective-permute-done | bytes 131104 | tf_op jit(solution)/shard_map/ppermute | solution.py:404
  65.0 1.9 %collective-permute-start.4 = (bf16[4,128,256]{2,1,0:T(8,128)(2,1)S(1)}, bf16[4,128,256]{2,1,0:T(8,128)(2,1)S(1)}, u32[]{:S(2)}, u32[]{:S(2)}) collective-permute-start(bf16[4,128,256]{2,1,0:T(8,128)(2,1)S(1)} %pad_maximum_fusion.1), channel_id=1, source_target_pairs={{80,16},{0,64},{32,96},{64,128},{96,160},{128,192},{160,224},{192,... | collective-permute-start | bytes 786440 | tf_op jit(solution)/shard_map/ppermute | solution.py:404
  66.9 6.4 %collective-permute-done.4 = bf16[4,128,256]{2,1,0:T(8,128)(2,1)S(1)} collective-permute-done((bf16[4,128,256]{2,1,0:T(8,128)(2,1)S(1)}, bf16[4,128,256]{2,1,0:T(8,128)(2,1)S(1)}, u32[]{:S(2)}, u32[]{:S(2)}) %collective-permute-start.4) | collective-permute-done | bytes 262176 | tf_op jit(solution)/shard_map/ppermute | solution.py:404
  73.3 0.1 pad_maximum_fusion.keys_ref
  73.3 7.6 %collective-permute-start.5 = (bf16[8,128,256]{2,1,0:T(8,128)(2,1)S(1)}, bf16[8,128,256]{2,1,0:T(8,128)(2,1)}, u32[]{:S(2)}, u32[]{:S(2)}) collective-permute-start(bf16[8,128,256]{2,1,0:T(8,128)(2,1)S(1)} %pad_maximum_fusion.keys_ref), channel_id=1, source_target_pairs={{0,32},{32,64},{64,96},{96,128},{128,160},{160,192},{192,224},{224... | collective-permute-start | bytes 1572872 | tf_op jit(solution)/shard_map/ppermute | solution.py:404
  80.9 0.0 copy-done
  81.0 1.9 %collective-permute-start = (bf16[128,128]{1,0:T(8,128)(2,1)S(1)}, bf16[128,128]{1,0:T(8,128)(2,1)S(1)}, u32[]{:S(2)}, u32[]{:S(2)}) collective-permute-start(bf16[128,128]{1,0:T(8,128)(2,1)S(1)} %bitcast.23), channel_id=1, source_target_pairs={{16,0},{0,16},{48,32},{32,48},{80,64},{64,80},{112,96},{96,112},{1... | collective-permute-start | bytes 98312 | tf_op jit(solution)/shard_map/ppermute | solution.py:404
  82.9 1.2 collective-permute-done.swapped_ref
  84.0 1.5 attend_early.1.refs_0_
  85.6 0.7 collective-permute-done.5.keys_ref
  86.3 3.0 %attend_late.1 = (f32[256,256]{1,0:T(8,128)S(1)}, f32[256,256]{1,0:T(8,128)S(1)}) custom-call(s32[1]{0:T(128)} %bitcast.8.z_ref, s32[1]{0:T(128)} %bitcast.9.core_ref, bf16[128,128]{1,0:T(8,128)(2,1)S(1)} %bitcast.25, bf16[128,128]{1,0:T(8,128)(2,1)S(1)} %collective-permute-done.swapped_ref, bf16[8,128,256]{2,1,0:T(8,128)(2,1)} %collective-permute-done.5.keys_ref, ...), custom_call_target="tpu_custom_call" | custom-call | tf_op jit(solution)/shard_map/attend_late/pallas_call | solution.py:335
  89.2 1.9 %collective-permute-start.6 = (f32[256,256]{1,0:T(8,128)S(1)}, f32[256,256]{1,0:T(8,128)S(1)}, u32[]{:S(2)}, u32[]{:S(2)}) collective-permute-start(f32[256,256]{1,0:T(8,128)S(1)} %get-tuple-element.9), channel_id=1, source_target_pairs={{16,0},{0,16},{48,32},{32,48},{80,64},{64,80},{112,96},{96,112},{1... | collective-permute-start | bytes 786440 | tf_op jit(solution)/shard_map/ppermute | solution.py:404
  91.8 0.9 collective-permute-done.6.other_ref
  92.7 0.0 copy-done.3
  92.7 1.7 project.1.proj_ref
  94.3 0.0 all-to-all-done.1.x_ref
  94.3 4.0 %ffn.1 = bf16[16,768,128]{2,1,0:T(8,128)(2,1)S(1)} custom-call(bf16[16,640,128]{2,1,0:T(8,128)(2,1)S(1)} %all-to-all-done.1.x_ref, bf16[2048,256]{1,0:T(8,128)(2,1)} %bitcast.30, bf16[2048,256]{1,0:T(8,128)(2,1)} %bitcast.31, bf16[256,2048]{1,0:T(8,128)(2,1)} %bitcast.32, bf16[16,128,128]{2,1,0:T(8,128)(2,1)S(1)} %project.1.proj_ref), custom_call_target="tpu_custom_call" | custom-call | tf_op jit(solution)/shard_map/ffn/pallas_call | solution.py:182
  98.3 45.7 %all_to_all.21.in_ref = bf16[16,768,128]{2,1,0:T(8,128)(2,1)S(1)} all-to-all(bf16[16,768,128]{2,1,0:T(8,128)(2,1)S(1)} %ffn.1), channel_id=1, replica_groups=mesh['z'=16,'core'=2,'y'=4,'x'=4] {'y','x'}, dimensions={0} | all-to-all | bytes 6291456 | tf_op jit(solution)/shard_map/all_to_all | solution.py:412
  144.0 0.0 copy-start.1
  144.0 0.0 copy-start.2
  144.0 1.0 reduce_terms.1
  145.0 8.4 %all-to-all-start.3 = ((bf16[160,4,128]{2,1,0:T(4,128)(2,1)}), bf16[160,4,128]{2,1,0:T(4,128)(2,1)S(1)}, u32[]{:S(2)}, u32[]{:S(2)}) async-start(bf16[160,4,128]{2,1,0:T(4,128)(2,1)} %bitcast.16), calls=%async_computation.3 | async-start | bytes 327680 | tf_op jit(solution)/shard_map/all_to_all | solution.py:412
  153.4 0.0 copy-done.1
  153.4 0.0 copy-done.2
  153.4 0.6 weigh.1
  154.0 16.5 %all-to-all-done.3 = bf16[160,4,128]{2,1,0:T(4,128)(2,1)S(1)} async-done(((bf16[160,4,128]{2,1,0:T(4,128)(2,1)}), bf16[160,4,128]{2,1,0:T(4,128)(2,1)S(1)}, u32[]{:S(2)}, u32[]{:S(2)}) %all-to-all-start.3) | async-done | bytes 163872 | tf_op jit(solution)/shard_map/all_to_all | solution.py:412
  170.6 0.9 combine.1
  (4 shorter events, 0.1 us)
Async XLA Ops:
  37.6 7.0 %copy-start.4 = (bf16[128,1,128]{2,0,1:T(8,128)(2,1)S(1)}, bf16[128,1,128]{2,0,1:T(8,128)(2,1)}, u32[]{:S(2)}) copy-start(bf16[128,1,128]{2,0,1:T(8,128)(2,1)} %param.15) | copy-start | bytes 98308
  37.6 7.0 %copy-start.5 = (bf16[128,1,128]{2,0,1:T(8,128)(2,1)S(1)}, bf16[128,1,128]{2,0,1:T(8,128)(2,1)}, u32[]{:S(2)}) copy-start(bf16[128,1,128]{2,0,1:T(8,128)(2,1)} %param.14) | copy-start | bytes 98308
  37.6 43.3 %copy-start = (bf16[128,1,128]{2,0,1:T(8,128)(2,1)S(1)}, bf16[128,1,128]{2,0,1:T(8,128)(2,1)}, u32[]{:S(2)}) copy-start(bf16[128,1,128]{2,0,1:T(8,128)(2,1)} %param.13) | copy-start | bytes 98308
  37.6 56.7 %all-to-all-start.1 = ((bf16[16,640,128]{2,1,0:T(8,128)(2,1)}), bf16[16,640,128]{2,1,0:T(8,128)(2,1)S(1)}, u32[]{:S(2)}, u32[]{:S(2)}) async-start(bf16[16,640,128]{2,1,0:T(8,128)(2,1)} %spread_rows.1), calls=%async_computation.1 | async-start | bytes 5242880 | tf_op jit(solution)/shard_map/all_to_all | solution.py:412
  44.5 48.1 %copy-start.3 = (f32[128]{0:T(128)S(1)}, f32[128]{0:T(128)}, u32[]{:S(2)}) copy-start(f32[128]{0:T(128)} %param.17) | copy-start | bytes 1540
  44.6 5.0 %collective-permute-start.2 = (bf16[128,256]{1,0:T(8,128)(2,1)S(1)}, bf16[128,256]{1,0:T(8,128)(2,1)S(1)}, u32[]{:S(2)}, u32[]{:S(2)}) collective-permute-start(bf16[128,256]{1,0:T(8,128)(2,1)S(1)} %pad_maximum_fusion.3), channel_id=1, source_target_pairs={{48,16},{80,48},{112,80},{144,112},{176,144},{208,176},{240,208},{... | collective-permute-start | bytes 196616 | tf_op jit(solution)/shard_map/ppermute | solution.py:404
  46.5 5.9 %collective-permute-start.1 = (bf16[128,256]{1,0:T(8,128)(2,1)S(1)}, bf16[128,256]{1,0:T(8,128)(2,1)S(1)}, u32[]{:S(2)}, u32[]{:S(2)}) collective-permute-start(bf16[128,256]{1,0:T(8,128)(2,1)S(1)} %pad_maximum_fusion.3), channel_id=1, source_target_pairs={{16,0},{48,32},{80,64},{112,96},{144,128},{176,160},{208,192},{240... | collective-permute-start | bytes 196616 | tf_op jit(solution)/shard_map/ppermute | solution.py:404
  52.4 12.5 %collective-permute-start.3 = (bf16[2,128,256]{2,1,0:T(8,128)(2,1)S(1)}, bf16[2,128,256]{2,1,0:T(8,128)(2,1)S(1)}, u32[]{:S(2)}, u32[]{:S(2)}) collective-permute-start(bf16[2,128,256]{2,1,0:T(8,128)(2,1)S(1)} %pad_maximum_fusion.2), channel_id=1, source_target_pairs={{144,16},{176,48},{208,80},{0,128},{32,160},{64,192},{96,224},{128... | collective-permute-start | bytes 393224 | tf_op jit(solution)/shard_map/ppermute | solution.py:404
  65.0 8.3 %collective-permute-start.4 = (bf16[4,128,256]{2,1,0:T(8,128)(2,1)S(1)}, bf16[4,128,256]{2,1,0:T(8,128)(2,1)S(1)}, u32[]{:S(2)}, u32[]{:S(2)}) collective-permute-start(bf16[4,128,256]{2,1,0:T(8,128)(2,1)S(1)} %pad_maximum_fusion.1), channel_id=1, source_target_pairs={{80,16},{0,64},{32,96},{64,128},{96,160},{128,192},{160,224},{192,... | collective-permute-start | bytes 786440 | tf_op jit(solution)/shard_map/ppermute | solution.py:404
  73.3 12.9 %collective-permute-start.5 = (bf16[8,128,256]{2,1,0:T(8,128)(2,1)S(1)}, bf16[8,128,256]{2,1,0:T(8,128)(2,1)}, u32[]{:S(2)}, u32[]{:S(2)}) collective-permute-start(bf16[8,128,256]{2,1,0:T(8,128)(2,1)S(1)} %pad_maximum_fusion.keys_ref), channel_id=1, source_target_pairs={{0,32},{32,64},{64,96},{96,128},{128,160},{160,192},{192,224},{224... | collective-permute-start | bytes 1572872 | tf_op jit(solution)/shard_map/ppermute | solution.py:404
  81.0 3.1 %collective-permute-start = (bf16[128,128]{1,0:T(8,128)(2,1)S(1)}, bf16[128,128]{1,0:T(8,128)(2,1)S(1)}, u32[]{:S(2)}, u32[]{:S(2)}) collective-permute-start(bf16[128,128]{1,0:T(8,128)(2,1)S(1)} %bitcast.23), channel_id=1, source_target_pairs={{16,0},{0,16},{48,32},{32,48},{80,64},{64,80},{112,96},{96,112},{1... | collective-permute-start | bytes 98312 | tf_op jit(solution)/shard_map/ppermute | solution.py:404
  89.2 3.4 %collective-permute-start.6 = (f32[256,256]{1,0:T(8,128)S(1)}, f32[256,256]{1,0:T(8,128)S(1)}, u32[]{:S(2)}, u32[]{:S(2)}) collective-permute-start(f32[256,256]{1,0:T(8,128)S(1)} %get-tuple-element.9), channel_id=1, source_target_pairs={{16,0},{0,16},{48,32},{32,48},{80,64},{64,80},{112,96},{96,112},{1... | collective-permute-start | bytes 786440 | tf_op jit(solution)/shard_map/ppermute | solution.py:404
  144.0 9.4 %copy-start.1 = (s32[128,4]{0,1:T(4,128)S(1)}, s32[128,4]{0,1:T(4,128)}, u32[]{:S(2)}) copy-start(s32[128,4]{0,1:T(4,128)} %param.21) | copy-start | bytes 6148
  144.0 9.5 %copy-start.2 = (f32[128,4]{0,1:T(4,128)S(1)}, f32[128,4]{0,1:T(4,128)}, u32[]{:S(2)}) copy-start(f32[128,4]{0,1:T(4,128)} %param.22) | copy-start | bytes 6148
  145.0 25.5 %all-to-all-start.3 = ((bf16[160,4,128]{2,1,0:T(4,128)(2,1)}), bf16[160,4,128]{2,1,0:T(4,128)(2,1)S(1)}, u32[]{:S(2)}, u32[]{:S(2)}) async-start(bf16[160,4,128]{2,1,0:T(4,128)(2,1)} %bitcast.16), calls=%async_computation.3 | async-start | bytes 327680 | tf_op jit(solution)/shard_map/all_to_all | solution.py:412
